TPU v7x, 32 devices: a whole 2x2x4 slice. The times are simulated.
32 devices in a mesh: sp: 8 (over z, x), tp: 4 (over y, core).
Axes of the slice: x: 2, y: 2, z: 4, core: 2. Of those that a mesh axis runs over, the one named last changes fastest.
Arguments:
- latent: bfloat16 [8192, 2048], P(('sp', 'tp')), may hold values from -8 to 8
- context: bfloat16 [512, 2048], P('sp'), may hold values from -8 to 8
- latent_condition: bfloat16 [2048], replicated, may hold values from -4 to 4
- context_condition: bfloat16 [2048], replicated, may hold values from -4 to 4
- shift_weight: bfloat16 [2048, 2048], P('sp', 'tp'), may hold values from -0.125 to 0.125
- scale_weight: bfloat16 [2048, 2048], P('sp', 'tp'), may hold values from -0.125 to 0.125
- gate_weight: bfloat16 [2048, 2048], P('sp', 'tp'), may hold values from -0.125 to 0.125
- norm_gain: float32 [2048], replicated, may hold values from 0.1 to 1.9
- query_weight: bfloat16 [2048, 512], replicated, may hold values from -0.125 to 0.125
- key_weight: bfloat16 [2048, 512], replicated, may hold values from -0.125 to 0.125
- value_weight: bfloat16 [2048, 1024], replicated, may hold values from -0.125 to 0.125
- outgate_weight: bfloat16 [2048, 1024], replicated, may hold values from -0.125 to 0.125
- down_weight: bfloat16 [2048, 32], replicated, may hold values from -0.125 to 0.125
- up_weight: bfloat16 [32, 512], replicated, may hold values from -2 to 2
- decay_bias: float32 [512], replicated, as said below
- out_weight: bfloat16 [1024, 2048], replicated, may hold values from -0.1875 to 0.1875
- post_gain: float32 [2048], replicated, may hold values from 0.1 to 1.9
Outputs:
- updated: bfloat16 [8192, 2048], P(('sp', 'tp'))
Inputs may be any that keep to these rules, and one draw needn't show every extreme that they name: decay_bias is at least 0; counting heads from 0, the channels of heads 1, 3, 5, … are at least log(512) + 2, those of heads 0, 2, 4, … at most 1.5.
All inputs are finite; a program needn't handle non-finite values.
Results may differ from a plain program's by a relative error of at most 0.0035.
The roundings to bfloat16 on the way count: a program that leaves them out, or rounds other values in their place, can miss the bound.
Values may be sent and summed in bfloat16 or wider, within the bound.
A program may use at most 192 MiB of HBM per device.

v0:
```python
import functools

import jax
import jax.numpy as jnp
from jax import lax
from jax.experimental import pallas as pl
from jax.experimental.pallas import tpu as pltpu
from jax.sharding import PartitionSpec as P

HEADS = 16
DK = 32
DV = 64
LANES = 128
GROUP = LANES // DK
GV = GROUP * DV
GROUPS = HEADS // GROUP
MESH = pl.DeviceIdType.MESH
TILE = 64
PAD = 16

epsilon = 1e-06
decay_temper = 16.0
highest = lax.Precision.HIGHEST
f32 = jnp.float32
bf16 = jnp.bfloat16


def rms_factor(values):
    return lax.rsqrt(jnp.mean(values * values, axis=-1, keepdims=True) + epsilon)


def stored(values):
    return lax.optimization_barrier(values.astype(bf16))


def modulated(tokens, norm_gain, shift_row, scale_row):
    values = tokens.astype(f32)
    return (values * rms_factor(values) * norm_gain * (1.0 + scale_row) + shift_row).astype(bf16)


def project(normed, weight):
    return jnp.dot(normed, weight, preferred_element_type=f32)


def dot_nt(a, b):
    return lax.dot_general(a, b, (((1,), (1,)), ((), ())), preferred_element_type=f32)


def dot_tn(a, b):
    return lax.dot_general(a, b, (((0,), (0,)), ((), ())), preferred_element_type=f32)


def lower_ones(rows):
    t = lax.broadcasted_iota(jnp.int32, (rows, rows), 0)
    s = lax.broadcasted_iota(jnp.int32, (rows, rows), 1)
    return jnp.where(t >= s, 1.0, 0.0).astype(bf16)


def running_sum(lower, log_rows):
    high = log_rows.astype(bf16)
    rest = log_rows - high.astype(f32)
    mid = rest.astype(bf16)
    low = (rest - mid.astype(f32)).astype(bf16)
    dot = functools.partial(jnp.dot, preferred_element_type=f32)
    return dot(lower, high) + dot(lower, mid) + dot(lower, low)


def same_head(rows, row_size, cols, col_size):
    r = lax.broadcasted_iota(jnp.int32, (rows, cols), 0) // row_size
    c = lax.broadcasted_iota(jnp.int32, (rows, cols), 1) // col_size
    return r == c


def spread_kernel(sp_count, tp_count, part_ref, out_ref, held, local_sem, send_sems, recv_sems):
    count = sp_count * tp_count
    sp, tp = lax.axis_index("sp"), lax.axis_index("tp")
    mine = sp * tp_count + tp
    barrier = pltpu.get_barrier_semaphore()

    def place(step):
        peer = lax.rem(mine + step, count)
        return (peer // tp_count, lax.rem(peer, tp_count))

    def greet(step, carry):
        pl.semaphore_signal(barrier, inc=1, device_id=place(step), device_id_type=MESH)
        return carry

    lax.fori_loop(1, count, greet, 0)
    pl.semaphore_wait(barrier, count - 1)

    def copy(step, slot):
        return pltpu.make_async_remote_copy(
            src_ref=part_ref,
            dst_ref=held.at[slot],
            send_sem=send_sems.at[step],
            recv_sem=recv_sems.at[slot],
            device_id=place(step),
            device_id_type=MESH,
        )

    def send(step, carry):
        copy(step, mine).start()
        return carry

    def finish(step, carry):
        source = lax.rem(mine + count - step, count)
        copy(step, source).wait_recv()
        return carry

    def drain(step, carry):
        copy(step, mine).wait_send()
        return carry

    lax.fori_loop(1, count, send, 0)
    own = pltpu.make_async_copy(part_ref, held.at[mine], local_sem)
    own.start()
    own.wait()
    lax.fori_loop(1, count, finish, 0)
    width = part_ref.shape[1]
    for t in range(tp_count):
        total = held[t]
        for s in range(1, sp_count):
            total = total + held[s * tp_count + t]
        out_ref[:, t * width : (t + 1) * width] = total
    lax.fori_loop(1, count, drain, 0)


def segment_kernel(count, k_ref, v_ref, log_ref, out_ref, held, *, rows, ctx_rows):
    unit = DV * GROUPS // count
    per_group = count // GROUPS
    diag = same_head(GV, DV, LANES, DK)
    for which, (start, length, valid) in enumerate(
        ((0, rows, rows), (rows, k_ref.shape[0] - rows, ctx_rows))
    ):
        lower = lower_ones(length)
        for g in range(GROUPS):
            lanes = slice(g * LANES, (g + 1) * LANES)
            log_rows = log_ref[start : start + length, lanes]
            keys = k_ref[start : start + length, lanes].astype(f32)
            if valid < length:
                keep = lax.broadcasted_iota(jnp.int32, (length, LANES), 0) < valid
                log_rows = jnp.where(keep, log_rows, 0.0)
                keys = jnp.where(keep, keys, 0.0)
            inclusive = running_sum(lower, log_rows)
            total = inclusive[length - 1 : length, :]
            k_fwd = (keys * jnp.exp(total - inclusive)).astype(bf16)
            k_bwd = (keys * jnp.exp(inclusive - log_rows)).astype(bf16)
            values = v_ref[start : start + length, g * GV : (g + 1) * GV]
            for side, weighted in enumerate((k_fwd, k_bwd)):
                full = jnp.where(diag, dot_tn(values, weighted), 0.0)
                state = full[0:DV]
                for h in range(1, GROUP):
                    state = state + full[h * DV : (h + 1) * DV]
                row = (2 * which + side) * unit
                for r in range(per_group):
                    held[g * per_group + r, row : row + unit, :] = state[
                        r * unit : (r + 1) * unit
                    ]
            high = total.astype(bf16).astype(f32)
            row = 4 * unit + 2 * which
            for r in range(per_group):
                held[g * per_group + r, row : row + 1, :] = high
                held[g * per_group + r, row + 1 : row + 2, :] = total - high
    out_ref[...] = held[...].astype(bf16)


def chain_kernel(count, x_ref, out_ref, held, sent):
    unit = DV * GROUPS // count
    held[...] = x_ref[...].astype(f32)

    def decayed(i, state, which, side):
        at = 4 * unit + 2 * which
        total = held[i, at : at + 1, :] + held[i, at + 1 : at + 2, :]
        row = (2 * which + side) * unit
        return jnp.exp(total) * state + held[i, row : row + unit, :]

    def context_step(i, states):
        return (decayed(i, states[0], 1, 0), decayed(count - 1 - i, states[1], 1, 1))

    def latent_step(i, states):
        last = count - 1 - i
        sent[i, 0:unit, :] = states[0]
        sent[last, unit : 2 * unit, :] = states[1]
        return (decayed(i, states[0], 0, 0), decayed(last, states[1], 0, 1))

    zero = jnp.zeros((unit, LANES), f32)
    states = lax.fori_loop(0, count, context_step, (zero, zero))
    lax.fori_loop(0, count, latent_step, states)
    out_ref[...] = sent[...].astype(bf16)


def mixer_kernel(count, q_ref, k_ref, v_ref, og_ref, log_ref, start_ref, out_ref, enter, *, rows):
    unit = DV * GROUPS // count
    per_group = count // GROUPS
    blocks = rows // TILE
    diag = same_head(GV, DV, LANES, DK)
    diag2 = jnp.concatenate([diag, diag], axis=1)
    k_keep = same_head(GROUP * TILE, TILE, LANES, DK)
    v_keep = same_head(GROUP * TILE, TILE, GV, DV)
    head_mean = jnp.where(same_head(GV, DV, GV, DV), 1.0 / DV, 0.0).astype(bf16)
    t_index = lax.broadcasted_iota(jnp.int32, (TILE, GROUP * TILE), 0)
    s_index = lax.broadcasted_iota(jnp.int32, (TILE, GROUP * TILE), 1) % TILE
    lower = lower_ones(TILE)
    for g in range(GROUPS):
        for r in range(per_group):
            for side in range(2):
                enter[r * unit : (r + 1) * unit, side * LANES : (side + 1) * LANES] = start_ref[
                    g * per_group + r, side * unit : (side + 1) * unit, :
                ].astype(f32)
        start = jnp.where(diag2, jnp.concatenate([enter[...]] * GROUP, axis=0), 0.0)
        lanes = slice(g * LANES, (g + 1) * LANES)
        v_lanes = slice(g * GV, (g + 1) * GV)
        parts = []
        for b in range(blocks):
            at = slice(b * TILE, (b + 1) * TILE)
            log_rows = log_ref[at, lanes]
            inclusive = running_sum(lower, log_rows)
            before = inclusive - log_rows
            total = inclusive[TILE - 1 : TILE, :]
            middle = inclusive[TILE // 2 - 1 : TILE // 2, :]
            queries = q_ref[at, lanes].astype(f32) * DK ** (-0.5)
            keys = k_ref[at, lanes].astype(f32)
            values = v_ref[at, v_lanes]
            scores = []
            for q_log, k_log in ((inclusive - middle, middle - inclusive), (middle - before, before - middle)):
                k_side = (keys * jnp.exp(k_log)).astype(bf16)
                k_stack = jnp.where(k_keep, jnp.concatenate([k_side] * GROUP, axis=0), 0.0).astype(bf16)
                scores.append(dot_nt((queries * jnp.exp(q_log)).astype(bf16), k_stack))
            both = jnp.where(t_index >= s_index, scores[0], 0.0) + jnp.where(
                t_index <= s_index, scores[1], 0.0
            )
            v_stack = jnp.where(v_keep, jnp.concatenate([values] * GROUP, axis=0), 0.0).astype(bf16)
            within = jnp.dot(both.astype(bf16), v_stack, preferred_element_type=f32)
            q_across = jnp.concatenate(
                [queries * jnp.exp(inclusive), queries * jnp.exp(total - before)], axis=1
            ).astype(bf16)
            k_both = jnp.concatenate(
                [keys * jnp.exp(total - inclusive), keys * jnp.exp(before)], axis=1
            ).astype(bf16)
            summary = jnp.where(diag2, dot_tn(values, k_both), 0.0)
            parts.append((within, q_across, summary, jnp.exp(total)))
        forward = [start[:, :LANES]]
        for b in range(blocks - 1):
            forward.append(parts[b][3] * forward[b] + parts[b][2][:, :LANES])
        backward = [start[:, LANES:]]
        for b in range(blocks - 1, 0, -1):
            backward.insert(0, parts[b][3] * backward[0] + parts[b][2][:, LANES:])
        for b in range(blocks):
            at = slice(b * TILE, (b + 1) * TILE)
            entering = jnp.concatenate([forward[b], backward[b]], axis=1).astype(bf16)
            mixed = parts[b][0] + dot_nt(parts[b][1], entering)
            square = mixed * mixed
            high = square.astype(bf16)
            rest = (square - high.astype(f32)).astype(bf16)
            mean = jnp.dot(high, head_mean, preferred_element_type=f32) + jnp.dot(
                rest, head_mean, preferred_element_type=f32
            )
            gate = og_ref[at, v_lanes].astype(f32)
            silu = gate / (1.0 + jnp.exp(-gate))
            out_ref[at, v_lanes] = (mixed * lax.rsqrt(mean + epsilon) * silu).astype(bf16)


def shards(
    latent,
    context,
    latent_condition,
    context_condition,
    shift_weight,
    scale_weight,
    gate_weight,
    norm_gain,
    query_weight,
    key_weight,
    value_weight,
    outgate_weight,
    down_weight,
    up_weight,
    decay_bias,
    out_weight,
    post_gain,
):
    axes = ("sp", "tp")
    sp_count, tp_count = lax.axis_size("sp"), lax.axis_size("tp")
    count = sp_count * tp_count
    rows, width = latent.shape
    conditions = jnp.stack([latent_condition, context_condition])
    cond_act = jax.nn.silu(conditions.astype(f32)).astype(bf16)
    row_share = shift_weight.shape[0]
    cond_rows = lax.dynamic_slice_in_dim(cond_act, lax.axis_index("sp") * row_share, row_share, 1)
    part = jnp.concatenate(
        [project(cond_rows, w) for w in (shift_weight, scale_weight, gate_weight)], axis=0
    )
    part = jnp.pad(part, ((0, 2), (0, 0)))
    mods = pl.pallas_call(
        functools.partial(spread_kernel, sp_count, tp_count),
        out_shape=jax.ShapeDtypeStruct((part.shape[0], width), f32),
        in_specs=[pl.BlockSpec(memory_space=pltpu.VMEM)],
        out_specs=pl.BlockSpec(memory_space=pltpu.VMEM),
        scratch_shapes=[
            pltpu.VMEM((count, *part.shape), f32),
            pltpu.SemaphoreType.DMA,
            pltpu.SemaphoreType.DMA((count,)),
            pltpu.SemaphoreType.DMA((count,)),
        ],
        compiler_params=pltpu.CompilerParams(
            collective_id=0, has_side_effects=True, vmem_limit_bytes=16 * 1024 * 1024
        ),
        name="spread",
    )(part)

    ctx_rows = context.shape[0] // tp_count
    ctx_pad = -(-ctx_rows // PAD) * PAD
    ctx_mine = lax.dynamic_slice_in_dim(context, lax.axis_index("tp") * ctx_rows, ctx_rows, 0)
    ctx_mine = jnp.pad(ctx_mine, ((0, ctx_pad - ctx_rows), (0, 0)))
    normed = modulated(latent, norm_gain, mods[0], mods[2])
    ctx_normed = modulated(ctx_mine, norm_gain, mods[1], mods[3])
    every = jnp.concatenate([normed, ctx_normed], axis=0)
    key_rows = project(every, key_weight).astype(bf16)
    value_rows = project(every, value_weight).astype(bf16)
    low_rank = project(every, down_weight).astype(bf16)
    log_decay = jax.nn.log_sigmoid(project(low_rank, up_weight) + decay_bias) / decay_temper
    query_rows = project(every, query_weight).astype(bf16)
    outgate_rows = project(every, outgate_weight).astype(bf16)

    unit = DV * GROUPS // count
    sent, back = (count, 4 * unit + 4, LANES), (count, 2 * unit, LANES)
    limit = pltpu.CompilerParams(vmem_limit_bytes=16 * 1024 * 1024)
    segments = pl.pallas_call(
        functools.partial(segment_kernel, count, rows=rows, ctx_rows=ctx_rows),
        out_shape=jax.ShapeDtypeStruct(sent, bf16),
        scratch_shapes=[pltpu.VMEM(sent, f32)],
        compiler_params=limit,
        name="segments",
    )(key_rows, value_rows, log_decay)
    exchanged = lax.all_to_all(segments, axes, 0, 0, tiled=True)
    starts = pl.pallas_call(
        functools.partial(chain_kernel, count),
        out_shape=jax.ShapeDtypeStruct(back, bf16),
        scratch_shapes=[pltpu.VMEM(sent, f32), pltpu.VMEM(back, f32)],
        compiler_params=limit,
        name="chain",
    )(exchanged)
    starts = lax.all_to_all(starts, axes, 0, 0, tiled=True)
    gated = pl.pallas_call(
        functools.partial(mixer_kernel, count, rows=rows),
        out_shape=jax.ShapeDtypeStruct((rows, HEADS * DV), bf16),
        scratch_shapes=[pltpu.VMEM((DV, 2 * LANES), f32)],
        compiler_params=limit,
        name="mixer",
    )(query_rows, key_rows, value_rows, outgate_rows, log_decay, starts)
    branch = stored(project(gated, out_weight)).astype(f32)
    result = latent.astype(f32) + mods[4] * (branch * rms_factor(branch)) * post_gain
    return result.astype(bf16)


def solution(mesh):
    placed = (
        P(("sp", "tp"), None),
        P("sp", None),
        P(),
        P(),
        P("sp", "tp"),
        P("sp", "tp"),
        P("sp", "tp"),
        P(),
        P(),
        P(),
        P(),
        P(),
        P(),
        P(),
        P(),
        P(),
        P(),
    )
    return jax.shard_map(
        shards, mesh=mesh, in_specs=placed, out_specs=P(("sp", "tp"), None), check_vma=False
    )
```

profile of v0, /device:TPU:0, one launch (start us, length us, event | category | flops | bytes accessed | tf_op | source)
XLA Modules:
  0.0 85.2 jit_solution(8867631450658729148)
XLA Ops:
  0.0 1.1 %fusion.12 = f32[16]{0:T(128)S(1)} fusion(bf16[64,2048]{1,0:T(8,128)(2,1)} %param.18, s32[]{:T(128)S(6)} %select_n.12), kind=kLoop, calls=%fused_computation.28 | loop fusion | flops 98288 | bytes 65604 | tf_op jit(solution)/shard_map/reduce_sum | solution.py:29
  1.1 1.5 %fusion.3 = f32[256]{0:T(256)S(1)} fusion(bf16[256,2048]{1,0:T(8,128)(2,1)} %param.17), kind=kLoop, calls=%fused_computation.9 | loop fusion | flops 1572608 | bytes 1049600 | tf_op jit(solution)/shard_map/reduce_sum | solution.py:29
  2.7 0.7 stack.9
  3.4 0.7 stack.10
  4.1 1.1 %fusion.20 = f32[2,512]{1,0:T(2,128)S(1)} fusion(bf16[256,512]{1,0:T(8,128)(2,1)} %param.21, f32[2,2048]{1,0:T(2,128)S(1)} %maximum_convert_fusion, s32[]{:T(128)S(6)} %select_n.11), kind=kOutput, calls=%fused_computation.45 | convolution fusion | flops 526848 | bytes 268292 | tf_op jit(solution)/shard_map/dot_general | solution.py:42
  5.2 1.1 %fusion.18 = f32[2,512]{1,0:T(2,128)S(1)} fusion(bf16[256,512]{1,0:T(8,128)(2,1)} %param.22, f32[2,2048]{1,0:T(2,128)S(1)} %maximum_convert_fusion, s32[]{:T(128)S(6)} %select_n.11), kind=kOutput, calls=%fused_computation.44 | convolution fusion | flops 526848 | bytes 268292 | tf_op jit(solution)/shard_map/dot_general | solution.py:42
  6.3 1.1 %fusion.22 = f32[2,512]{1,0:T(2,128)S(1)} fusion(bf16[256,512]{1,0:T(8,128)(2,1)} %param.23, f32[2,2048]{1,0:T(2,128)S(1)} %maximum_convert_fusion, s32[]{:T(128)S(6)} %select_n.11), kind=kOutput, calls=%fused_computation.46 | convolution fusion | flops 526848 | bytes 268292 | tf_op jit(solution)/shard_map/dot_general | solution.py:42
  7.4 16.6 %spread.1 = f32[8,2048]{1,0:T(8,128)S(1)} custom-call(f32[8,512]{1,0:T(8,128)S(1)} %select_maximum_fusion.part_ref), custom_call_target="tpu_custom_call" | custom-call | tf_op jit(solution)/shard_map/spread/pallas_call | solution.py:294
  24.0 0.6 fusion.24
  24.7 0.9 %fusion.16 = bf16[16,2048]{1,0:T(8,128)(2,1)S(1)} fusion(f32[2048]{0:T(1024)S(1)} %bitcast.19, f32[2048]{0:T(1024)S(1)} %bitcast.20, f32[2048]{0:T(1024)S(1)} %copy-done.11, f32[16]{0:T(128)S(1)} %add_rsqrt_fusion.2, bf16[64,2048]{1,0:T(8,128)(2,1)} %param.18, s32[]{:T(128)S(6)} %select_n.12), kind=kLoop, calls=%fused_computation.32 | loop fusion | flops 196608 | bytes 155716 | tf_op jit(solution)/shard_map/convert_element_type | solution.py:38
  25.6 0.5 fusion.7
  26.1 0.7 convolution_convert_fusion.3.k_ref
  26.9 0.2 copy-done.9
  27.1 1.6 %copy-done.14 = bf16[2048,1024]{1,0:T(8,128)(2,1)S(1)} copy-done((bf16[2048,1024]{1,0:T(8,128)(2,1)S(1)}, bf16[2048,1024]{1,0:T(8,128)(2,1)}, u32[]{:S(2)}) %copy-start.14) | copy-done | bytes 4194328
  28.7 1.3 %convolution_convert_fusion.2.v_ref = bf16[272,1024]{1,0:T(8,128)(2,1)S(1)} fusion(bf16[2048,1024]{1,0:T(8,128)(2,1)S(1)} %copy-done.14, bf16[16,2048]{1,0:T(8,128)(2,1)S(1)} %fusion.16, bf16[256,2048]{1,0:T(8,128)(2,1)S(1)} %fusion.7), kind=kOutput, calls=%fused_computation.17 | convolution fusion | flops 1143357440 | bytes 5865472 | tf_op jit(solution)/shard_map/dot_general | solution.py:42
  30.0 2.2 %fusion.11.log_ref = f32[272,512]{1,0:T(8,128)S(1)} fusion(bf16[32,512]{1,0:T(8,128)(2,1)} %param.30, bf16[2048,32]{0,1:T(8,128)(2,1)} %param.29, f32[512]{0:T(512)} %param.31, bf16[16,2048]{1,0:T(8,128)(2,1)S(1)} %fusion.16, bf16[256,2048]{1,0:T(8,128)(2,1)} %copy-done.9), kind=kOutput, calls=%fused_computation.25 | convolution fusion | flops 48194048 | bytes 1837056 | tf_op jit(solution)/shard_map/dot_general | solution.py:42
  32.3 2.4 %segments.1 = bf16[32,36,128]{2,1,0:T(8,128)(2,1)S(1)} custom-call(bf16[272,512]{1,0:T(8,128)(2,1)S(1)} %convolution_convert_fusion.3.k_ref, bf16[272,1024]{1,0:T(8,128)(2,1)S(1)} %convolution_convert_fusion.2.v_ref, f32[272,512]{1,0:T(8,128)S(1)} %fusion.11.log_ref), custom_call_target="tpu_custom_call" | custom-call | tf_op jit(solution)/shard_map/segments/pallas_call | solution.py:328
  34.7 0.7 copy-done.1
  35.4 8.5 %all-to-all-start = ((bf16[32,36,128]{2,1,0:T(8,128)(2,1)}), bf16[32,36,128]{2,1,0:T(8,128)(2,1)S(1)}, u32[]{:S(2)}, u32[]{:S(2)}) async-start(bf16[32,36,128]{2,1,0:T(8,128)(2,1)} %copy-done.1), calls=%async_computation | async-start | bytes 655360 | tf_op jit(solution)/shard_map/all_to_all | solution.py:335
  43.9 4.7 %convolution_convert_fusion.1.og_ref = bf16[272,1024]{1,0:T(8,128)(2,1)} fusion(bf16[2048,1024]{1,0:T(8,128)(2,1)} %param.28, bf16[16,2048]{1,0:T(8,128)(2,1)} %copy-done.10, bf16[256,2048]{1,0:T(8,128)(2,1)} %copy-done.9), kind=kOutput, calls=%fused_computation.16 | convolution fusion | flops 1143357440 | bytes 5865472 | tf_op jit(solution)/shard_map/dot_general | solution.py:42
  48.6 7.4 %all-to-all-done.x_ref = bf16[32,36,128]{2,1,0:T(8,128)(2,1)S(1)} async-done(((bf16[32,36,128]{2,1,0:T(8,128)(2,1)}), bf16[32,36,128]{2,1,0:T(8,128)(2,1)S(1)}, u32[]{:S(2)}, u32[]{:S(2)}) %all-to-all-start) | async-done | bytes 294944 | tf_op jit(solution)/shard_map/all_to_all | solution.py:335
  56.0 0.9 %chain.1 = bf16[32,16,128]{2,1,0:T(8,128)(2,1)S(1)} custom-call(bf16[32,36,128]{2,1,0:T(8,128)(2,1)S(1)} %all-to-all-done.x_ref), custom_call_target="tpu_custom_call" | custom-call | tf_op jit(solution)/shard_map/chain/pallas_call | solution.py:336
  56.9 0.6 copy-done.5
  57.5 3.5 %all-to-all-start.1 = ((bf16[32,16,128]{2,1,0:T(8,128)(2,1)}), bf16[32,16,128]{2,1,0:T(8,128)(2,1)}, u32[]{:S(2)}, u32[]{:S(2)}) async-start(bf16[32,16,128]{2,1,0:T(8,128)(2,1)} %copy-done.5), calls=%async_computation.1 | async-start | bytes 262144 | tf_op jit(solution)/shard_map/all_to_all | solution.py:343
  61.0 3.4 %convolution_convert_fusion.4.q_ref = bf16[272,512]{1,0:T(8,128)(2,1)} fusion(bf16[2048,512]{1,0:T(8,128)(2,1)} %param.25, bf16[16,2048]{1,0:T(8,128)(2,1)} %copy-done.10, bf16[256,2048]{1,0:T(8,128)(2,1)} %copy-done.9), kind=kOutput, calls=%fused_computation.21 | convolution fusion | flops 572792832 | bytes 3489792 | tf_op jit(solution)/shard_map/dot_general | solution.py:42
  64.4 4.6 %all-to-all-done.1.start_ref = bf16[32,16,128]{2,1,0:T(8,128)(2,1)} async-done(((bf16[32,16,128]{2,1,0:T(8,128)(2,1)}), bf16[32,16,128]{2,1,0:T(8,128)(2,1)}, u32[]{:S(2)}, u32[]{:S(2)}) %all-to-all-start.1) | async-done | bytes 131104 | tf_op jit(solution)/shard_map/all_to_all | solution.py:343
  69.0 1.1 %copy-done.4 = bf16[272,1024]{1,0:T(8,128)(2,1)S(1)} copy-done((bf16[272,1024]{1,0:T(8,128)(2,1)S(1)}, bf16[272,1024]{1,0:T(8,128)(2,1)}, u32[]{:S(2)}) %copy-start.4) | copy-done | bytes 557080
  70.0 1.0 %copy-done.6 = bf16[272,512]{1,0:T(8,128)(2,1)S(1)} copy-done((bf16[272,512]{1,0:T(8,128)(2,1)S(1)}, bf16[272,512]{1,0:T(8,128)(2,1)}, u32[]{:S(2)}) %copy-start.6) | copy-done | bytes 278552
  71.0 8.8 %mixer.1 = bf16[256,1024]{1,0:T(8,128)(2,1)S(1)} custom-call(bf16[272,512]{1,0:T(8,128)(2,1)S(1)} %copy-done.6, bf16[272,512]{1,0:T(8,128)(2,1)S(1)} %copy-done.3, bf16[272,1024]{1,0:T(8,128)(2,1)S(1)} %convolution_convert_fusion.2.v_ref, bf16[272,1024]{1,0:T(8,128)(2,1)S(1)} %copy-done.4, f32[272,512]{1,0:T(8,128)S(1)} %fusion.11.log_ref, ...), custom_call_target="tpu_custom_call" | custom-call | tf_op jit(solution)/shard_map/mixer/pallas_call | solution.py:344
  79.8 3.5 %convolution_convert_fusion = bf16[256,2048]{1,0:T(8,128)(2,1)S(1)} fusion(bf16[256,1024]{1,0:T(8,128)(2,1)S(1)} %mixer.1, bf16[1024,2048]{1,0:T(8,128)(2,1)} %param.32), kind=kOutput, calls=%fused_computation.5 | convolution fusion | flops 1074266112 | bytes 5767168 | tf_op jit(solution)/shard_map/dot_general | solution.py:42
  83.3 0.3 fusion
  83.7 1.5 %fusion.8 = bf16[256,2048]{1,0:T(8,128)(2,1)} fusion(bf16[256,2048]{1,0:T(8,128)(2,1)S(1)} %convolution_convert_fusion, bf16[256,2048]{1,0:T(8,128)(2,1)S(1)} %copy-done.8, f32[2048]{0:T(1024)S(1)} %copy-done.13, f32[256]{0:T(256)S(1)} %add_rsqrt_fusion, f32[2048]{0:T(1024)S(1)} %bitcast.16), kind=kLoop, calls=%fused_computation.14 | loop fusion | flops 3670016 | bytes 3163136 | tf_op jit(solution)/shard_map/convert_element_type | solution.py:353
  (29 shorter events, 0.1 us)
Async XLA Ops:
  0.0 26.1 %copy-start = (bf16[2048,512]{1,0:T(8,128)(2,1)S(1)}, bf16[2048,512]{1,0:T(8,128)(2,1)}, u32[]{:S(2)}) copy-start(bf16[2048,512]{1,0:T(8,128)(2,1)} %param.26) | copy-start | bytes 6291460
  0.0 25.6 %copy-start.7 = (bf16[256,2048]{1,0:T(8,128)(2,1)S(1)}, bf16[256,2048]{1,0:T(8,128)(2,1)}, u32[]{:S(2)}) copy-start(bf16[256,2048]{1,0:T(8,128)(2,1)} %param.17) | copy-start | bytes 3145732
  0.0 24.7 %copy-start.11 = (f32[2048]{0:T(1024)S(1)}, f32[2048]{0:T(1024)}, u32[]{:S(2)}) copy-start(f32[2048]{0:T(1024)} %param.24) | copy-start | bytes 24580
  25.6 4.4 %copy-start.10 = (bf16[16,2048]{1,0:T(8,128)(2,1)}, bf16[16,2048]{1,0:T(8,128)(2,1)S(1)}, u32[]{:S(2)}) copy-start(bf16[16,2048]{1,0:T(8,128)(2,1)S(1)} %fusion.16) | copy-start | bytes 196612
  26.1 1.0 %copy-start.9 = (bf16[256,2048]{1,0:T(8,128)(2,1)}, bf16[256,2048]{1,0:T(8,128)(2,1)S(1)}, u32[]{:S(2)}) copy-start(bf16[256,2048]{1,0:T(8,128)(2,1)S(1)} %fusion.7) | copy-start | bytes 3145732
  26.1 2.6 %copy-start.14 = (bf16[2048,1024]{1,0:T(8,128)(2,1)S(1)}, bf16[2048,1024]{1,0:T(8,128)(2,1)}, u32[]{:S(2)}) copy-start(bf16[2048,1024]{1,0:T(8,128)(2,1)} %param.27) | copy-start | bytes 12582916
  28.7 3.6 %copy-start.2 = (bf16[272,512]{1,0:T(8,128)(2,1)}, bf16[272,512]{1,0:T(8,128)(2,1)S(1)}, u32[]{:S(2)}) copy-start(bf16[272,512]{1,0:T(8,128)(2,1)S(1)} %convolution_convert_fusion.3.k_ref) | copy-start | bytes 835588
  34.7 0.7 copy-start.1
  35.4 20.6 %all-to-all-start = ((bf16[32,36,128]{2,1,0:T(8,128)(2,1)}), bf16[32,36,128]{2,1,0:T(8,128)(2,1)S(1)}, u32[]{:S(2)}, u32[]{:S(2)}) async-start(bf16[32,36,128]{2,1,0:T(8,128)(2,1)} %copy-done.1), calls=%async_computation | async-start | bytes 655360 | tf_op jit(solution)/shard_map/all_to_all | solution.py:335
  56.9 0.6 copy-start.5
  57.5 11.5 %all-to-all-start.1 = ((bf16[32,16,128]{2,1,0:T(8,128)(2,1)}), bf16[32,16,128]{2,1,0:T(8,128)(2,1)}, u32[]{:S(2)}, u32[]{:S(2)}) async-start(bf16[32,16,128]{2,1,0:T(8,128)(2,1)} %copy-done.5), calls=%async_computation.1 | async-start | bytes 262144 | tf_op jit(solution)/shard_map/all_to_all | solution.py:343
  61.0 8.0 %copy-start.3 = (bf16[272,512]{1,0:T(8,128)(2,1)S(1)}, bf16[272,512]{1,0:T(8,128)(2,1)}, u32[]{:S(2)}) copy-start(bf16[272,512]{1,0:T(8,128)(2,1)} %copy-done.2) | copy-start | bytes 835588
  69.0 1.1 %copy-start.4 = (bf16[272,1024]{1,0:T(8,128)(2,1)S(1)}, bf16[272,1024]{1,0:T(8,128)(2,1)}, u32[]{:S(2)}) copy-start(bf16[272,1024]{1,0:T(8,128)(2,1)} %convolution_convert_fusion.1.og_ref) | copy-start | bytes 1671172
  70.0 1.0 %copy-start.6 = (bf16[272,512]{1,0:T(8,128)(2,1)S(1)}, bf16[272,512]{1,0:T(8,128)(2,1)}, u32[]{:S(2)}) copy-start(bf16[272,512]{1,0:T(8,128)(2,1)} %convolution_convert_fusion.4.q_ref) | copy-start | bytes 835588
  79.8 3.9 %copy-start.8 = (bf16[256,2048]{1,0:T(8,128)(2,1)S(1)}, bf16[256,2048]{1,0:T(8,128)(2,1)}, u32[]{:S(2)}) copy-start(bf16[256,2048]{1,0:T(8,128)(2,1)} %param.17) | copy-start | bytes 3145732
  79.8 3.9 %copy-start.12 = (f32[1,2048]{1,0:T(1,128)S(1)}, f32[1,2048]{1,0:T(1,128)}, u32[]{:S(2)}) copy-start(f32[1,2048]{1,0:T(1,128)} %get-tuple-element.5) | copy-start | bytes 24580
  79.8 3.9 %copy-start.13 = (f32[2048]{0:T(1024)S(1)}, f32[2048]{0:T(1024)}, u32[]{:S(2)}) copy-start(f32[2048]{0:T(1024)} %param.33) | copy-start | bytes 24580
where the time goes:
time: 85.8 us; the launch traced here: 85.2 us
  Pallas kernels  28.7 us (33%)
  matrix products  19.2 us (22%)
  starting transfers between devices  12 us (14%)
  waiting for transfers between devices  11.9 us (14%)
  local copies, waits for them, and re-layouts  6.61 us (8%)
  other arithmetic  6.55 us (8%)
    dot_general x9, matrix products, project(): return jnp.dot(normed, weight, preferred_element_type=f32)  19.2 us
    pallas_call x1, Pallas kernels, shards(): pl.pallas_call(functools.partial(spread_kernel, sp_count, tp_count), out_...  16.6 us
    pallas_call x1, Pallas kernels, shards(): pl.pallas_call(functools.partial(mixer_kernel, count, rows=rows), out_sha...  8.76 us
    all_to_all x1, starting transfers between devices, shards(): exchanged = lax.all_to_all(segments, axes, 0, 0, tiled=True)  8.53 us
    all_to_all x1, waiting for transfers between devices, shards(): exchanged = lax.all_to_all(segments, axes, 0, 0, tiled=True)  7.36 us
    unnamed x30, local copies, waits for them, and re-layouts  5.22 us
    all_to_all x1, waiting for transfers between devices, shards(): starts = lax.all_to_all(starts, axes, 0, 0, tiled=True)  4.55 us
    all_to_all x1, starting transfers between devices, shards(): starts = lax.all_to_all(starts, axes, 0, 0, tiled=True)  3.46 us
  transfers between devices with their start and end apart: 2, of which 2 were waited for; matrix products, arithmetic and copies ran while one was open for 10% of the time, Pallas kernels for 0%

commit v1 on v0

v1 whole, which is shorter than its diff:
```python
import functools
from types import SimpleNamespace

import jax
import jax.numpy as jnp
from jax import lax
from jax.experimental import pallas as pl
from jax.experimental.pallas import tpu as pltpu
from jax.sharding import PartitionSpec as P

HEADS = 16
DK = 32
DV = 64
LANES = 128
SUB = 8
GROUP = LANES // DK
GV = GROUP * DV
GROUPS = HEADS // GROUP
CREW = DV // SUB
MESH = pl.DeviceIdType.MESH
TILE = 64
COLS = 256
STRIP = 16
VMEM_LIMIT = 60 * 1024 * 1024

NAMES = (
    "latent",
    "context",
    "latent_condition",
    "context_condition",
    "shift_weight",
    "scale_weight",
    "gate_weight",
    "norm_gain",
    "query_weight",
    "key_weight",
    "value_weight",
    "outgate_weight",
    "down_weight",
    "up_weight",
    "decay_bias",
    "out_weight",
    "post_gain",
)
MODULATION = ("shift_weight", "scale_weight", "gate_weight")
LATER = (
    "down_weight",
    "up_weight",
    "key_weight",
    "value_weight",
    "query_weight",
    "outgate_weight",
    "out_weight",
)

epsilon = 1e-06
decay_temper = 16.0
f32 = jnp.float32
bf16 = jnp.bfloat16


def dot(a, b):
    return jnp.dot(a, b, preferred_element_type=f32)


def dot_nt(a, b):
    return lax.dot_general(a, b, (((1,), (1,)), ((), ())), preferred_element_type=f32)


def dot_tn(a, b):
    return lax.dot_general(a, b, (((0,), (0,)), ((), ())), preferred_element_type=f32)


def iota(shape, axis):
    return lax.broadcasted_iota(jnp.int32, shape, axis)


def lower_ones(rows):
    return jnp.where(iota((rows, rows), 0) >= iota((rows, rows), 1), 1.0, 0.0).astype(bf16)


def running_sum(lower, log_rows):
    high = log_rows.astype(bf16)
    rest = log_rows - high.astype(f32)
    mid = rest.astype(bf16)
    low = (rest - mid.astype(f32)).astype(bf16)
    return dot(lower, high) + dot(lower, mid) + dot(lower, low)


def log_decays(values):
    return (jnp.minimum(values, 0.0) - jnp.log1p(jnp.exp(-jnp.abs(values)))) / decay_temper


def rms_factor(values):
    return lax.rsqrt(jnp.mean(values * values, axis=-1, keepdims=True) + epsilon)


def per_head(full, head):
    out = full[(GROUP - 1) * DV :]
    for h in range(GROUP - 2, -1, -1):
        out = jnp.where(head == h, full[h * DV : (h + 1) * DV], out)
    return out


def stacked(values, head):
    zero = jnp.zeros_like(values)
    return jnp.concatenate([jnp.where(head == h, values, zero) for h in range(GROUP)], axis=0)


def block_kernel(sp_count, tp_count, *refs):
    hbm = SimpleNamespace(**dict(zip((*NAMES, "out"), refs)))
    vm = SimpleNamespace(**refs[-2])
    sem = SimpleNamespace(**refs[-1])

    count = sp_count * tp_count
    crews = count // CREW
    sp, tp = lax.axis_index("sp"), lax.axis_index("tp")
    me = sp * tp_count + tp
    crew, post = me // CREW, lax.rem(me, CREW)
    rows, width = hbm.latent.shape
    blocks = rows // TILE
    chunks = hbm.shift_weight.shape[1] // LANES
    row_share = hbm.shift_weight.shape[0]
    ctx_rows = vm.context.shape[0]
    ctx_group = lax.rem(tp, GROUPS)

    def place(flat):
        return (flat // tp_count, lax.rem(flat, tp_count))

    def remote(src, dst, send, recv, flat):
        return pltpu.make_async_remote_copy(
            src_ref=src,
            dst_ref=dst,
            send_sem=send,
            recv_sem=recv,
            device_id=place(flat),
            device_id_type=MESH,
        )

    def others(body, total):
        def step(i, carry):
            body(i)
            return carry

        lax.fori_loop(1, total, step, 0)

    def load(slot, src, dst):
        return pltpu.make_async_copy(src, dst, sem.load.at[slot])

    ctx_at = (tp // GROUPS) * ctx_rows
    first = [
        load(0, hbm.shift_weight, vm.shift_weight),
        load(1, hbm.scale_weight, vm.scale_weight),
        load(2, hbm.gate_weight, vm.gate_weight),
        load(3, hbm.context.at[pl.ds(pl.multiple_of(ctx_at, 8), ctx_rows)], vm.context),
        load(4, hbm.latent, vm.latent),
    ]
    later = {
        name: load(5 + i, getattr(hbm, name), getattr(vm, name)) for i, name in enumerate(LATER)
    }
    for copy in first:
        copy.start()

    barrier = pltpu.get_barrier_semaphore()
    others(
        lambda i: pl.semaphore_signal(
            barrier, inc=1, device_id=place(lax.rem(me + i, count)), device_id_type=MESH
        ),
        count,
    )

    mine = pl.ds(pl.multiple_of(sp * row_share, LANES), row_share)
    pick = iota((STRIP, row_share), 0) == 0
    raw = jnp.where(
        pick, hbm.latent_condition[:, mine].astype(f32), hbm.context_condition[:, mine].astype(f32)
    )
    cond = (raw / (1.0 + jnp.exp(-raw))).astype(bf16)
    for copy in later.values():
        copy.start()
    for which in range(3):
        first[which].wait()
        weight = (vm.shift_weight, vm.scale_weight, vm.gate_weight)[which]
        part = dot(cond, weight[...])
        for c in range(chunks):
            at = slice(c * LANES, (c + 1) * LANES)
            vm.part[c, which : which + 1, :] = part[0:1, at]
            vm.part[c, 3 + which : 4 + which, :] = part[1:2, at]
    pl.semaphore_wait(barrier, count - 1)

    def to_reducer(c):
        return remote(
            vm.part.at[c], vm.parts.at[crew], sem.part_send.at[c], sem.part_recv.at[crew], c * CREW + post
        )

    for c in range(chunks):

        @pl.when(crew != c)
        def _():
            to_reducer(c).start()

    first[3].wait()
    xc = vm.context[...].astype(f32)
    vm.ctx_scaled[...] = xc * rms_factor(xc)
    first[4].wait()

    def scale_strip(i, carry):
        at = pl.ds(pl.multiple_of(i * STRIP, STRIP), STRIP)
        x = vm.latent[at, :].astype(f32)
        vm.scaled[at, :] = x * rms_factor(x)
        return carry

    lax.fori_loop(0, rows // STRIP, scale_strip, 0)

    def spread(flat, slot):
        return remote(
            vm.total, vm.totals.at[slot], sem.total_send.at[flat], sem.total_recv.at[slot], flat
        )

    @pl.when(crew < chunks)
    def _():
        vm.parts[crew] = vm.part[crew]

        def arrived(i):
            source = lax.rem(crew + i, crews)
            remote(
                vm.part.at[0],
                vm.parts.at[source],
                sem.part_send.at[0],
                sem.part_recv.at[source],
                source * CREW + post,
            ).wait_recv()

        others(arrived, crews)
        total = vm.parts[0]
        for i in range(1, crews):
            total = total + vm.parts[i]
        vm.total[...] = total
        vm.totals[me] = total
        others(lambda i: spread(lax.rem(me + i, count), me).start(), count)

    def total_in(f, carry):
        @pl.when(f != me)
        def _():
            spread(f, f).wait_recv()

        return carry

    lax.fori_loop(0, chunks * CREW, total_in, 0)
    for t in range(tp_count):
        for c in range(chunks):
            tile = vm.totals[c * CREW + t]
            for x in range(1, CREW // tp_count):
                tile = tile + vm.totals[c * CREW + x * tp_count + t]
            at = (t * chunks + c) * LANES
            vm.mods[:, at : at + LANES] = tile

    gain = hbm.norm_gain[...] * (1.0 + vm.mods[4:5, :])
    ctx_normed = (vm.ctx_scaled[...] * gain + vm.mods[3:4, :]).astype(bf16)
    later["down_weight"].wait()
    later["up_weight"].wait()
    later["key_weight"].wait()
    later["value_weight"].wait()
    head_k = iota((DV, 2 * LANES), 1) % LANES // DK
    key_at = pl.ds(pl.multiple_of(ctx_group * LANES, LANES), LANES)
    val_at = pl.ds(pl.multiple_of(ctx_group * GV, GV), GV)
    low = dot(ctx_normed, vm.down_weight[...]).astype(bf16)
    log_rows = log_decays(dot(low, vm.up_weight[:, key_at]) + hbm.decay_bias[:, key_at])
    keys = dot(ctx_normed, vm.key_weight[:, key_at]).astype(bf16).astype(f32)
    values = dot(ctx_normed, vm.value_weight[:, val_at]).astype(bf16)
    inclusive = running_sum(lower_ones(ctx_rows), log_rows)
    closing = inclusive[ctx_rows - 1 : ctx_rows, :]
    both = jnp.concatenate(
        [keys * jnp.exp(closing - inclusive), keys * jnp.exp(inclusive - log_rows)], axis=1
    ).astype(bf16)
    state = per_head(dot_tn(values, both), head_k)
    for j in range(CREW):
        at = slice(j * SUB, (j + 1) * SUB)
        vm.ctx_out[j] = jnp.concatenate([state[at, :LANES], state[at, LANES:]], axis=0).astype(bf16)
    vm.ctx_log[...] = closing

    def ctx_copies(flat, slot):
        return (
            remote(
                vm.ctx_out.at[lax.rem(flat, CREW)],
                vm.ctx_in.at[slot],
                sem.ctx_send.at[flat],
                sem.ctx_recv.at[slot],
                flat,
            ),
            remote(
                vm.ctx_log, vm.ctx_logs.at[slot], sem.ctx_log_send.at[flat], sem.ctx_log_recv.at[slot], flat
            ),
        )

    def ctx_start(i):
        for copy in ctx_copies(lax.rem(me + i, count), me):
            copy.start()

    others(ctx_start, count)
    vm.ctx_in[me] = vm.ctx_out[post]
    vm.ctx_logs[me] = closing

    gain = hbm.norm_gain[...] * (1.0 + vm.mods[1:2, :])
    shift = vm.mods[0:1, :]

    def norm_strip(i, carry):
        at = pl.ds(pl.multiple_of(i * STRIP, STRIP), STRIP)
        vm.normed[at, :] = (vm.scaled[at, :] * gain + shift).astype(bf16)
        return carry

    lax.fori_loop(0, rows // STRIP, norm_strip, 0)

    def project(weight, out):
        for n in range(0, weight.shape[1], COLS):
            at = slice(n, n + COLS)
            out[:, at] = dot(vm.normed[...], weight[:, at]).astype(bf16)

    low = dot(vm.normed[...], vm.down_weight[...]).astype(bf16)
    log_all = log_decays(dot(low, vm.up_weight[...]) + hbm.decay_bias[...])
    lower = lower_ones(TILE)
    ends = []
    for b in range(blocks):
        at = slice(b * TILE, (b + 1) * TILE)
        log_rows = log_all[at]
        inclusive = running_sum(lower, log_rows)
        vm.inclusive[at, :] = inclusive
        vm.before[at, :] = inclusive - log_rows
        ends.append(inclusive[TILE - 1 : TILE, :])
        vm.closing[b : b + 1, :] = ends[b]
    segment_log = functools.reduce(lambda a, b: a + b, ends)
    for g in range(GROUPS):
        vm.log_out[g : g + 1, :] = segment_log[:, g * LANES : (g + 1) * LANES]

    def mate(i):
        return lax.rem(post + i, CREW)

    def log_copy(p, slot):
        return remote(
            vm.log_out, vm.logs.at[slot], sem.log_send.at[p], sem.log_recv.at[slot], crew * CREW + p
        )

    others(lambda i: log_copy(mate(i), post).start(), CREW)
    vm.logs[post] = vm.log_out[...]
    project(vm.key_weight, vm.key)

    def seg_copy(p, slot, g):
        return remote(
            vm.seg_out.at[g, p],
            vm.seg_in.at[g, slot],
            sem.seg_send.at[g, p],
            sem.seg_recv.at[g, slot],
            crew * CREW + p,
        )

    for g in range(GROUPS):
        lanes = slice(g * LANES, (g + 1) * LANES)
        v_lanes = slice(g * GV, (g + 1) * GV)
        vm.value[:, v_lanes] = dot(vm.normed[...], vm.value_weight[:, v_lanes]).astype(bf16)
        decays = [jnp.exp(vm.closing[b : b + 1, lanes]) for b in range(blocks)]
        for b in range(blocks):
            at = slice(b * TILE, (b + 1) * TILE)
            keys = vm.key[at, lanes].astype(f32)
            both = jnp.concatenate(
                [
                    keys * jnp.exp(vm.closing[b : b + 1, lanes] - vm.inclusive[at, lanes]),
                    keys * jnp.exp(vm.before[at, lanes]),
                ],
                axis=1,
            ).astype(bf16)
            vm.summary[g, b] = per_head(dot_tn(vm.value[at, v_lanes], both), head_k)
        forward = vm.summary[g, 0, :, :LANES]
        for b in range(1, blocks):
            forward = decays[b] * forward + vm.summary[g, b, :, :LANES]
        backward = vm.summary[g, blocks - 1, :, LANES:]
        for b in range(blocks - 2, -1, -1):
            backward = decays[b] * backward + vm.summary[g, b, :, LANES:]
        for j in range(CREW):
            at = slice(j * SUB, (j + 1) * SUB)
            vm.seg_out[g, j] = jnp.concatenate([forward[at], backward[at]], axis=0).astype(bf16)
        others(lambda i: seg_copy(mate(i), post, g).start(), CREW)
        vm.seg_in[g, post] = vm.seg_out[g, post]

    head_k1 = iota((TILE, LANES), 1) // DK
    head_v = iota((TILE, GV), 1) // DV
    t_index = iota((TILE, GROUP * TILE), 0)
    s_index = iota((TILE, GROUP * TILE), 1) % TILE

    def inside(g):
        lanes = slice(g * LANES, (g + 1) * LANES)
        v_lanes = slice(g * GV, (g + 1) * GV)
        for b in range(blocks):
            at = slice(b * TILE, (b + 1) * TILE)
            inclusive, before = vm.inclusive[at, lanes], vm.before[at, lanes]
            closing = inclusive[TILE - 1 : TILE, :]
            middle = inclusive[TILE // 2 - 1 : TILE // 2, :]
            queries = vm.query[at, lanes].astype(f32) * DK ** (-0.5)
            keys = vm.key[at, lanes].astype(f32)
            scores = []
            for q_log, k_log in (
                (inclusive - middle, middle - inclusive),
                (middle - before, before - middle),
            ):
                k_stack = stacked((keys * jnp.exp(k_log)).astype(bf16), head_k1)
                scores.append(dot_nt((queries * jnp.exp(q_log)).astype(bf16), k_stack))
            both = jnp.where(t_index >= s_index, scores[0], 0.0) + jnp.where(
                t_index <= s_index, scores[1], 0.0
            )
            v_stack = stacked(vm.value[at, v_lanes], head_v)
            vm.within[at, v_lanes] = dot(both.astype(bf16), v_stack)
            vm.q_across[g, at, :] = jnp.concatenate(
                [queries * jnp.exp(inclusive), queries * jnp.exp(closing - before)], axis=1
            ).astype(bf16)

    later["query_weight"].wait()
    project(vm.query_weight, vm.query)
    inside(0)

    def log_in(i):
        log_copy(mate(i), mate(i)).wait_recv()

    others(log_in, CREW)
    decays = [[jnp.exp(vm.logs[p, g : g + 1, :]) for g in range(GROUPS)] for p in range(CREW)]
    crew_log = vm.logs[0]
    for p in range(1, CREW):
        crew_log = crew_log + vm.logs[p]
    side = GROUPS * SUB
    vm.crew_out[side : side + SUB, :] = crew_log
    for g in range(GROUPS):
        others(lambda i: seg_copy(mate(i), mate(i), g).wait_recv(), CREW)
        forward = vm.seg_in[g, 0].astype(f32)[:SUB]
        for p in range(1, CREW):
            forward = decays[p][g] * forward + vm.seg_in[g, p].astype(f32)[:SUB]
        backward = vm.seg_in[g, CREW - 1].astype(f32)[SUB:]
        for p in range(CREW - 2, -1, -1):
            backward = decays[p][g] * backward + vm.seg_in[g, p].astype(f32)[SUB:]
        vm.crew_out[g * SUB : (g + 1) * SUB, :] = forward
        at = side + SUB + g * SUB
        vm.crew_out[at : at + SUB, :] = backward

    def crew_copy(c, slot, ahead):
        part = pl.ds(0, side + SUB) if ahead else pl.ds(side, side + SUB)
        return remote(
            vm.crew_out.at[part],
            vm.crew_in.at[slot, part],
            sem.crew_send.at[c],
            sem.crew_recv.at[slot],
            c * CREW + post,
        )

    def crew_start(i):
        c = lax.rem(crew + i, crews)

        @pl.when(c > crew)
        def _():
            crew_copy(c, crew, True).start()

        @pl.when(c < crew)
        def _():
            crew_copy(c, crew, False).start()

    others(crew_start, crews)
    for g in range(1, GROUPS):
        inside(g)

    def ctx_arrived(i):
        flat = lax.rem(me + i, count)
        for copy in ctx_copies(flat, flat):
            copy.wait_recv()

    others(ctx_arrived, count)
    parts = count // GROUPS
    zero = jnp.zeros((SUB, LANES), f32)

    def ctx_chain(i, carry):
        out = []
        for g in range(GROUPS):
            a = i * GROUPS + g
            z = (parts - 1 - i) * GROUPS + g
            out.append(jnp.exp(vm.ctx_logs[a]) * carry[2 * g] + vm.ctx_in[a].astype(f32)[:SUB])
            out.append(jnp.exp(vm.ctx_logs[z]) * carry[2 * g + 1] + vm.ctx_in[z].astype(f32)[SUB:])
        return tuple(out)

    carry = lax.fori_loop(0, parts, ctx_chain, (zero,) * (2 * GROUPS))

    def from_before(c, states):
        crew_copy(c, c, True).wait_recv()
        return tuple(
            jnp.exp(vm.crew_in[c, side + g : side + g + 1, :]) * states[g]
            + vm.crew_in[c, g * SUB : (g + 1) * SUB, :]
            for g in range(GROUPS)
        )

    def from_after(i, states):
        c = crews - 1 - i
        crew_copy(c, c, False).wait_recv()
        at = side + SUB
        return tuple(
            jnp.exp(vm.crew_in[c, side + g : side + g + 1, :]) * states[g]
            + vm.crew_in[c, at + g * SUB : at + (g + 1) * SUB, :]
            for g in range(GROUPS)
        )

    forward = lax.fori_loop(0, crew, from_before, tuple(carry[0::2]))
    backward = lax.fori_loop(0, crews - 1 - crew, from_after, tuple(carry[1::2]))
    for g in range(GROUPS):
        state = forward[g]
        entering = []
        for p in range(CREW):
            entering.append(state)
            state = decays[p][g] * state + vm.seg_in[g, p].astype(f32)[:SUB]
        state = backward[g]
        for p in range(CREW - 1, -1, -1):
            vm.enter_out[p, g] = jnp.concatenate([entering[p], state], axis=0).astype(bf16)
            state = decays[p][g] * state + vm.seg_in[g, p].astype(f32)[SUB:]

    def enter_copy(p, slot):
        return remote(
            vm.enter_out.at[p],
            vm.enter_in.at[slot],
            sem.enter_send.at[p],
            sem.enter_recv.at[slot],
            crew * CREW + p,
        )

    others(lambda i: enter_copy(mate(i), post).start(), CREW)
    vm.enter_in[post] = vm.enter_out[post]

    later["outgate_weight"].wait()
    project(vm.outgate_weight, vm.outgate)
    head_mean = jnp.where(iota((GV, GV), 0) // DV == iota((GV, GV), 1) // DV, 1.0 / DV, 0.0).astype(bf16)

    others(lambda i: enter_copy(mate(i), mate(i)).wait_recv(), CREW)
    for g in range(GROUPS):
        lanes = slice(g * LANES, (g + 1) * LANES)
        v_lanes = slice(g * GV, (g + 1) * GV)
        units = [vm.enter_in[j, g].astype(f32) for j in range(CREW)]
        decays = [jnp.exp(vm.closing[b : b + 1, lanes]) for b in range(blocks)]
        forward = [jnp.concatenate([u[:SUB] for u in units], axis=0)]
        for b in range(blocks - 1):
            forward.append(decays[b] * forward[b] + vm.summary[g, b, :, :LANES])
        backward = [jnp.concatenate([u[SUB:] for u in units], axis=0)]
        for b in range(blocks - 1, 0, -1):
            backward.insert(0, decays[b] * backward[0] + vm.summary[g, b, :, LANES:])
        for b in range(blocks):
            at = slice(b * TILE, (b + 1) * TILE)
            entering = jnp.concatenate([forward[b], backward[b]], axis=1)
            across = dot_nt(vm.q_across[g, at, :], stacked(entering, head_k).astype(bf16))
            mixed = vm.within[at, v_lanes] + across
            square = mixed * mixed
            high = square.astype(bf16)
            rest = (square - high.astype(f32)).astype(bf16)
            mean = dot(high, head_mean) + dot(rest, head_mean)
            gate = vm.outgate[at, v_lanes].astype(f32)
            silu = gate / (1.0 + jnp.exp(-gate))
            vm.gated[at, v_lanes] = (mixed * lax.rsqrt(mean + epsilon) * silu).astype(bf16)

    later["out_weight"].wait()
    for n in range(0, width, COLS):
        at = slice(n, n + COLS)
        vm.branch[:, at] = dot(vm.gated[...], vm.out_weight[:, at]).astype(bf16)
    gain = vm.mods[2:3, :] * hbm.post_gain[...]

    def store(i):
        at = pl.ds(pl.multiple_of(i * TILE, TILE), TILE)
        return pltpu.make_async_copy(vm.updated.at[at], hbm.out.at[at], sem.store.at[i])

    def final_block(b, carry):
        for s in range(TILE // STRIP):
            at = pl.ds(pl.multiple_of(b * TILE + s * STRIP, STRIP), STRIP)
            branch = vm.branch[at, :].astype(f32)
            vm.updated[at, :] = (
                vm.latent[at, :].astype(f32) + gain * (branch * rms_factor(branch))
            ).astype(bf16)
        store(b).start()
        return carry

    lax.fori_loop(0, blocks, final_block, 0)

    for c in range(chunks):

        @pl.when(crew != c)
        def _():
            to_reducer(c).wait_send()

    @pl.when(crew < chunks)
    def _():
        others(lambda i: spread(lax.rem(me + i, count), me).wait_send(), count)

    def ctx_sent(i):
        for copy in ctx_copies(lax.rem(me + i, count), me):
            copy.wait_send()

    others(ctx_sent, count)

    def mate_sent(i):
        log_copy(mate(i), post).wait_send()
        enter_copy(mate(i), post).wait_send()
        for g in range(GROUPS):
            seg_copy(mate(i), post, g).wait_send()

    others(mate_sent, CREW)

    def crew_sent(i):
        crew_copy(lax.rem(crew + i, crews), crew, True).wait_send()

    others(crew_sent, crews)
    for b in range(blocks):
        store(b).wait()


def shards(*operands):
    values = dict(zip(NAMES, operands))
    latent, context = values["latent"], values["context"]
    sp_count, tp_count = lax.axis_size("sp"), lax.axis_size("tp")
    count = sp_count * tp_count
    crews = count // CREW
    rows, width = latent.shape
    args, specs = [], []
    for value in operands:
        vector = value.ndim == 1
        args.append(value.reshape(1, -1) if vector else value)
        specs.append(pl.BlockSpec(memory_space=pltpu.VMEM if vector else pl.ANY))
    ctx_rows = context.shape[0] * GROUPS // tp_count
    chunks = values["shift_weight"].shape[1] // LANES
    keyw, valw = values["key_weight"].shape[1], values["value_weight"].shape[1]
    blocks = rows // TILE
    side = GROUPS * SUB
    buffers = dict(
        latent=pltpu.VMEM((rows, width), bf16),
        context=pltpu.VMEM((ctx_rows, width), bf16),
        part=pltpu.VMEM((chunks, SUB, LANES), f32),
        parts=pltpu.VMEM((crews, SUB, LANES), f32),
        total=pltpu.VMEM((SUB, LANES), f32),
        totals=pltpu.VMEM((chunks * CREW, SUB, LANES), f32),
        mods=pltpu.VMEM((SUB, width), f32),
        scaled=pltpu.VMEM((rows, width), f32),
        ctx_scaled=pltpu.VMEM((ctx_rows, width), f32),
        normed=pltpu.VMEM((rows, width), bf16),
        ctx_out=pltpu.VMEM((CREW, 2 * SUB, LANES), bf16),
        ctx_in=pltpu.VMEM((count, 2 * SUB, LANES), bf16),
        ctx_log=pltpu.VMEM((1, LANES), f32),
        ctx_logs=pltpu.VMEM((count, 1, LANES), f32),
        key=pltpu.VMEM((rows, keyw), bf16),
        query=pltpu.VMEM((rows, keyw), bf16),
        value=pltpu.VMEM((rows, valw), bf16),
        outgate=pltpu.VMEM((rows, valw), bf16),
        gated=pltpu.VMEM((rows, valw), bf16),
        inclusive=pltpu.VMEM((rows, keyw), f32),
        before=pltpu.VMEM((rows, keyw), f32),
        closing=pltpu.VMEM((SUB, keyw), f32),
        log_out=pltpu.VMEM((SUB, LANES), f32),
        logs=pltpu.VMEM((CREW, SUB, LANES), f32),
        summary=pltpu.VMEM((GROUPS, blocks, DV, 2 * LANES), f32),
        seg_out=pltpu.VMEM((GROUPS, CREW, 2 * SUB, LANES), bf16),
        seg_in=pltpu.VMEM((GROUPS, CREW, 2 * SUB, LANES), bf16),
        crew_out=pltpu.VMEM((2 * side + SUB, LANES), f32),
        crew_in=pltpu.VMEM((crews, 2 * side + SUB, LANES), f32),
        enter_out=pltpu.VMEM((CREW, GROUPS, 2 * SUB, LANES), bf16),
        enter_in=pltpu.VMEM((CREW, GROUPS, 2 * SUB, LANES), bf16),
        q_across=pltpu.VMEM((GROUPS, rows, 2 * LANES), bf16),
        within=pltpu.VMEM((rows, valw), f32),
        branch=pltpu.VMEM((rows, width), bf16),
        updated=pltpu.VMEM((rows, width), bf16),
    )
    for name in MODULATION + LATER:
        buffers[name] = pltpu.VMEM(values[name].shape, bf16)
    dma = pltpu.SemaphoreType.DMA
    semaphores = dict(
        load=dma((12,)),
        store=dma((blocks,)),
        part_send=dma((chunks,)),
        part_recv=dma((crews,)),
        total_send=dma((count,)),
        total_recv=dma((chunks * CREW,)),
        ctx_send=dma((count,)),
        ctx_recv=dma((count,)),
        ctx_log_send=dma((count,)),
        ctx_log_recv=dma((count,)),
        log_send=dma((CREW,)),
        log_recv=dma((CREW,)),
        seg_send=dma((GROUPS, CREW)),
        seg_recv=dma((GROUPS, CREW)),
        crew_send=dma((crews,)),
        crew_recv=dma((crews,)),
        enter_send=dma((CREW,)),
        enter_recv=dma((CREW,)),
    )
    return pl.pallas_call(
        functools.partial(block_kernel, sp_count, tp_count),
        out_shape=jax.ShapeDtypeStruct((rows, width), bf16),
        in_specs=specs,
        out_specs=pl.BlockSpec(memory_space=pl.ANY),
        scratch_shapes=[buffers, semaphores],
        compiler_params=pltpu.CompilerParams(
            collective_id=0, has_side_effects=True, vmem_limit_bytes=VMEM_LIMIT
        ),
        name="block",
    )(*args)


def solution(mesh):
    placed = (
        P(("sp", "tp"), None),
        P("sp", None),
        P(),
        P(),
        P("sp", "tp"),
        P("sp", "tp"),
        P("sp", "tp"),
        P(),
        P(),
        P(),
        P(),
        P(),
        P(),
        P(),
        P(),
        P(),
        P(),
    )
    return jax.shard_map(
        shards, mesh=mesh, in_specs=placed, out_specs=P(("sp", "tp"), None), check_vma=False
    )
```

time: 85.8 us -> 50.9 us (0.59)
  matrix products: 19.2 us -> 0 us
  Pallas kernels: 28.7 us -> 43.8 us
  starting transfers between devices: 12 us -> 0 us
  waiting for transfers between devices: 11.9 us -> 0 us
  other arithmetic: 6.55 us -> 0 us
    dot_general x9 -> x0, matrix products: 19.2 us -> none  [project(): return jnp.dot(normed, weight, preferred_element_type=f32)]
    pallas_call x4 -> x1, Pallas kernels: 28.7 us -> 43.8 us  [shards(): pl.pallas_call(functools.partial(block_kernel, sp_count, tp_count), out_s...]
    all_to_all x2 -> x0, starting transfers between devices: 12 us -> none  [the longest x1 8.53 us: shards(): exchanged = lax.all_to_all(segments, axes, 0, 0, tiled=True)]
    all_to_all x2 -> x0, waiting for transfers between devices: 11.9 us -> none  [the longest x1 7.36 us: shards(): exchanged = lax.all_to_all(segments, axes, 0, 0, tiled=True)]
    convert_element_type x4 -> x0, other arithmetic: 2.96 us -> none  [the longest x1 1.54 us: shards(): return result.astype(bf16)]
    reduce_sum x3 -> x0, other arithmetic: 2.94 us -> none  [rms_factor(): jnp.mean(values * values, axis=-1, keepdims=True) + epsilon]
    reshape x0 -> x2, local copies, waits for them, and re-layouts: none -> 2.57 us  [shards(): args.append(value.reshape(1, -1) if vector else value)]
    another operation x2 -> x0, local copies, waits for them, and re-layouts: 1.39 us -> none  [shards(): conditions = jnp.stack([latent_condition, context_condition])]
  transfers between devices with their start and end apart: 2 -> 0, of which waited for: 2 -> 0; matrix products, arithmetic and copies ran while one was open for 10% -> 0% of each run, Pallas kernels for 0% -> 0%
where the time goes in v1:
time: 50.9 us; the launch traced here: 50.6 us
  Pallas kernels  43.8 us (86%)
  local copies, waits for them, and re-layouts  6.78 us (13%)
    pallas_call x1, Pallas kernels, shards(): pl.pallas_call(functools.partial(block_kernel, sp_count, tp_count), out_s...  43.8 us
    unnamed x2, local copies, waits for them, and re-layouts  4.21 us
    reshape x2, local copies, waits for them, and re-layouts, shards(): args.append(value.reshape(1, -1) if vector else value)  2.57 us

profile of v1, /device:TPU:0, one launch (start us, length us, event | category | flops | bytes accessed | tf_op | source)
XLA Modules:
  0.0 50.6 jit_solution(8855583154516992862)
XLA Ops:
  0.0 1.3 %reshape.15.refs_2_ = bf16[1,2048]{1,0:T(2,128)(2,1)} reshape(bf16[2048]{0:T(1024)(128)(2,1)} %param.19) | data formatting | bytes 8192 | tf_op jit(solution)/shard_map/reshape | solution.py:621
  1.3 1.3 %reshape.16.refs_3_ = bf16[1,2048]{1,0:T(2,128)(2,1)} reshape(bf16[2048]{0:T(1024)(128)(2,1)} %param.20) | data formatting | bytes 8192 | tf_op jit(solution)/shard_map/reshape | solution.py:621
  2.6 1.9 %copy.18.refs_12_ = bf16[2048,32]{1,0:T(8,128)(2,1)} copy(bf16[2048,32]{0,1:T(8,128)(2,1)} %param.29) | data formatting | bytes 262144 | tf_op args[12]
  4.5 43.8 %block.1 = bf16[256,2048]{1,0:T(8,128)(2,1)} custom-call(bf16[256,2048]{1,0:T(8,128)(2,1)} %refs_0_.1, bf16[64,2048]{1,0:T(8,128)(2,1)} %refs_1_.1, bf16[1,2048]{1,0:T(2,128)(2,1)} %reshape.15.refs_2_, bf16[1,2048]{1,0:T(2,128)(2,1)} %reshape.16.refs_3_, bf16[256,512]{1,0:T(8,128)(2,1)} %refs_4_.1, bf16[256,512]{1,0:T(8,128)(2,1)} %refs_5_.1, ...), custom_call_target="tpu_custom_call" | custom-call | tf_op jit(solution)/shard_map/block/pallas_call | solution.py:688
  48.3 2.3 %copy.20 = bf16[256,2048]{1,0:T(8,128)(2,1)} copy(bf16[256,2048]{1,0:T(8,128)(2,1)} %block.1) | data formatting | bytes 2097152

commit v2 on v1

v2 whole, which is shorter than its diff:
```python
import functools
from types import SimpleNamespace

import jax
import jax.numpy as jnp
from jax import lax
from jax.experimental import pallas as pl
from jax.experimental.pallas import tpu as pltpu
from jax.sharding import PartitionSpec as P

HEADS = 16
DK = 32
DV = 64
LANES = 128
SUB = 8
GROUP = LANES // DK
GV = GROUP * DV
GROUPS = HEADS // GROUP
CREW = DV // SUB
MESH = pl.DeviceIdType.MESH
TILE = 64
COLS = 256
STRIP = 16
VMEM_LIMIT = 60 * 1024 * 1024

NAMES = (
    "latent",
    "context",
    "latent_condition",
    "context_condition",
    "shift_weight",
    "scale_weight",
    "gate_weight",
    "norm_gain",
    "query_weight",
    "key_weight",
    "value_weight",
    "outgate_weight",
    "down_weight",
    "up_weight",
    "decay_bias",
    "out_weight",
    "post_gain",
)
FIRST = (
    "latent_condition",
    "context_condition",
    "shift_weight",
    "scale_weight",
    "gate_weight",
    "context",
    "latent",
)
LATER = (
    "norm_gain",
    "decay_bias",
    "post_gain",
    "down_weight",
    "up_weight",
    "key_weight",
    "value_weight",
    "query_weight",
    "outgate_weight",
    "out_weight",
)

epsilon = 1e-06
decay_temper = 16.0
f32 = jnp.float32
bf16 = jnp.bfloat16


def dot(a, b):
    return jnp.dot(a, b, preferred_element_type=f32)


def dot_nt(a, b):
    return lax.dot_general(a, b, (((1,), (1,)), ((), ())), preferred_element_type=f32)


def dot_tn(a, b):
    return lax.dot_general(a, b, (((0,), (0,)), ((), ())), preferred_element_type=f32)


def iota(shape, axis):
    return lax.broadcasted_iota(jnp.int32, shape, axis)


def lower_ones(rows):
    return jnp.where(iota((rows, rows), 0) >= iota((rows, rows), 1), 1.0, 0.0).astype(bf16)


def running_sum(lower, log_rows):
    high = log_rows.astype(bf16)
    rest = log_rows - high.astype(f32)
    mid = rest.astype(bf16)
    low = (rest - mid.astype(f32)).astype(bf16)
    return dot(lower, high) + dot(lower, mid) + dot(lower, low)


def log_decays(values):
    return (jnp.minimum(values, 0.0) - jnp.log1p(jnp.exp(-jnp.abs(values)))) / decay_temper


def rms_factor(values):
    return lax.rsqrt(jnp.mean(values * values, axis=-1, keepdims=True) + epsilon)


def per_head(full, head):
    out = full[(GROUP - 1) * DV :]
    for h in range(GROUP - 2, -1, -1):
        out = jnp.where(head == h, full[h * DV : (h + 1) * DV], out)
    return out


def stacked(values, head):
    zero = jnp.zeros_like(values)
    return jnp.concatenate([jnp.where(head == h, values, zero) for h in range(GROUP)], axis=0)


def reduction(chunks, crews):
    reducers = min(2, chunks, crews)
    return reducers, chunks // reducers


def block_kernel(sp_count, tp_count, *refs):
    hbm = SimpleNamespace(**dict(zip((*NAMES, "out"), refs)))
    vm = SimpleNamespace(**refs[-2])
    sem = SimpleNamespace(**refs[-1])

    count = sp_count * tp_count
    crews = count // CREW
    sp, tp = lax.axis_index("sp"), lax.axis_index("tp")
    me = sp * tp_count + tp
    crew, post = me // CREW, lax.rem(me, CREW)
    rows, width = hbm.latent.shape
    blocks = rows // TILE
    row_share = hbm.shift_weight.shape[0]
    chunks = hbm.shift_weight.shape[1] // LANES
    reducers, share = reduction(chunks, crews)
    first_reducer = (crews - reducers) // 2
    ctx_rows = vm.context.shape[0]
    ctx_group = lax.rem(tp, GROUPS)

    def place(flat):
        return (flat // tp_count, lax.rem(flat, tp_count))

    def remote(src, dst, send, recv, flat):
        return pltpu.make_async_remote_copy(
            src_ref=src,
            dst_ref=dst,
            send_sem=send,
            recv_sem=recv,
            device_id=place(flat),
            device_id_type=MESH,
        )

    def others(body, total):
        def step(i, carry):
            body(i)
            return carry

        lax.fori_loop(1, total, step, 0)

    def mate(i):
        return lax.rem(post + i, CREW)

    def mates(body):
        for i in range(1, CREW):
            body(mate(i))

    ctx_at = pl.multiple_of((tp // GROUPS) * ctx_rows, SUB)
    hbm.context = hbm.context.at[pl.ds(ctx_at, ctx_rows)]
    loads = {
        name: pltpu.make_async_copy(getattr(hbm, name), getattr(vm, name), sem.load.at[i])
        for i, name in enumerate(FIRST + LATER)
    }
    for name in FIRST:
        loads[name].start()

    barrier = pltpu.get_barrier_semaphore()
    others(
        lambda i: pl.semaphore_signal(
            barrier, inc=1, device_id=place(lax.rem(me + i, count)), device_id_type=MESH
        ),
        count,
    )

    loads["latent_condition"].wait()
    loads["context_condition"].wait()
    vm.cond[0:1, :] = vm.latent_condition[...].astype(f32).reshape(1, width)
    vm.cond[1:2, :] = vm.context_condition[...].astype(f32).reshape(1, width)
    mine = pl.ds(pl.multiple_of(sp * row_share, LANES), row_share)
    pick = iota((STRIP, row_share), 0) == 0
    raw = jnp.where(pick, vm.cond[0:1, mine], vm.cond[1:2, mine])
    cond = (raw / (1.0 + jnp.exp(-raw))).astype(bf16)
    for name in LATER:
        loads[name].start()
    for which, name in enumerate(("shift_weight", "scale_weight", "gate_weight")):
        loads[name].wait()
        part = dot(cond, getattr(vm, name)[...])
        for c in range(chunks):
            at = slice(c * LANES, (c + 1) * LANES)
            r, row = c // share, c % share
            if which == 2:
                vm.gate_part[r, row] = part[0:1, at]
            else:
                vm.part[r, row * 4 + which : row * 4 + which + 1, :] = part[0:1, at]
                vm.part[r, row * 4 + 2 + which : row * 4 + 3 + which, :] = part[1:2, at]
    pl.semaphore_wait(barrier, count - 1)

    def to_reducer(r, slot):
        flat = (first_reducer + r) * CREW + post
        return (
            remote(vm.part.at[r], vm.parts.at[slot], sem.part_send.at[r], sem.part_recv.at[slot], flat),
            remote(
                vm.gate_part.at[r],
                vm.gate_parts.at[slot],
                sem.gate_part_send.at[r],
                sem.gate_part_recv.at[slot],
                flat,
            ),
        )

    for which in range(2):
        for r in range(reducers):

            @pl.when(crew != first_reducer + r)
            def _():
                to_reducer(r, crew)[which].start()

    loads["context"].wait()
    xc = vm.context[...].astype(f32)
    vm.ctx_scaled[...] = xc * rms_factor(xc)
    loads["latent"].wait()

    def scale_strip(i, carry):
        at = pl.ds(pl.multiple_of(i * TILE, TILE), TILE)
        x = vm.latent[at, :].astype(f32)
        vm.scaled[at, :] = x * rms_factor(x)
        return carry

    lax.fori_loop(0, rows // TILE, scale_strip, 0)

    reduced = reducers * CREW

    def spread(flat, slot):
        return remote(
            vm.total, vm.totals.at[slot], sem.total_send.at[flat], sem.total_recv.at[slot], flat
        )

    def gate_spread(flat, slot):
        return remote(
            vm.gate_total,
            vm.gate_totals.at[slot],
            sem.gate_send.at[flat],
            sem.gate_recv.at[slot],
            flat,
        )

    def reduce_here(which, mine, held, total, totals, copy):
        for r in range(reducers):
            home = first_reducer + r

            @pl.when(crew == home)
            def _():
                slot = r * CREW + post
                out = mine[r]
                for c in range(crews):
                    if c != home:
                        to_reducer(r, c)[which].wait_recv()
                        out = out + held[c]
                total[...] = out
                totals[slot] = out
                for c in sorted(range(crews), key=lambda c: -abs(c - home)):

                    def send(i, carry):
                        flat = c * CREW + mate(i)
                        copy(flat, slot).start()
                        return carry

                    lax.fori_loop(0 if c != home else 1, CREW, send, 0)

    def arrivals(copy):
        def arrived(i, carry):
            @pl.when(first_reducer * CREW + i != me)
            def _():
                copy(me, i).wait_recv()

            return carry

        lax.fori_loop(0, reduced, arrived, 0)

    def sent(copy):
        @pl.when((crew >= first_reducer) & (crew < first_reducer + reducers))
        def _():
            others(lambda i: copy(lax.rem(me + i, count), 0).wait_send(), count)

    reduce_here(0, vm.part, vm.parts, vm.total, vm.totals, spread)
    loads_needed = ("norm_gain", "decay_bias", "post_gain", "down_weight", "up_weight", "key_weight")
    for name in loads_needed + ("value_weight",):
        loads[name].wait()
    arrivals(spread)
    for r in range(reducers):
        for t in range(tp_count):
            tile = vm.totals[r * CREW + t]
            for x in range(1, CREW // tp_count):
                tile = tile + vm.totals[r * CREW + x * tp_count + t]
            for s in range(share):
                at = (t * chunks + r * share + s) * LANES
                vm.mods[0:4, at : at + LANES] = tile[s * 4 : s * 4 + 4]

    gain = vm.norm_gain[...] * (1.0 + vm.mods[3:4, :])
    ctx_normed = (vm.ctx_scaled[...] * gain + vm.mods[2:3, :]).astype(bf16)
    head_k = iota((DV, 2 * LANES), 1) % LANES // DK
    key_at = pl.ds(pl.multiple_of(ctx_group * LANES, LANES), LANES)
    val_at = pl.ds(pl.multiple_of(ctx_group * GV, GV), GV)
    low = dot_nt(ctx_normed, vm.down_weight[...]).astype(bf16)
    log_rows = log_decays(dot(low, vm.up_weight[:, key_at]) + vm.decay_bias[:, key_at])
    keys = dot(ctx_normed, vm.key_weight[:, key_at]).astype(bf16).astype(f32)
    values = dot(ctx_normed, vm.value_weight[:, val_at]).astype(bf16)
    inclusive = running_sum(lower_ones(ctx_rows), log_rows)
    closing = inclusive[ctx_rows - 1 : ctx_rows, :]
    both = jnp.concatenate(
        [keys * jnp.exp(closing - inclusive), keys * jnp.exp(inclusive - log_rows)], axis=1
    ).astype(bf16)
    state = per_head(dot_tn(values, both), head_k)
    for j in range(CREW):
        at = slice(j * SUB, (j + 1) * SUB)
        vm.ctx_out[j] = jnp.concatenate([state[at, :LANES], state[at, LANES:]], axis=0).astype(bf16)
    vm.ctx_log[...] = closing

    def ctx_copies(p, slot):
        flat = crew * CREW + p
        return (
            remote(vm.ctx_out.at[p], vm.ctx_in.at[slot], sem.ctx_send.at[p], sem.ctx_recv.at[slot], flat),
            remote(
                vm.ctx_log, vm.ctx_logs.at[slot], sem.ctx_log_send.at[p], sem.ctx_log_recv.at[slot], flat
            ),
        )

    def ctx_start(p):
        for copy in ctx_copies(p, post):
            copy.start()

    mates(ctx_start)
    vm.ctx_in[post] = vm.ctx_out[post]
    vm.ctx_logs[post] = closing

    gain = vm.norm_gain[...] * (1.0 + vm.mods[1:2, :])
    shift = vm.mods[0:1, :]
    for i in range(rows // STRIP):
        at = slice(i * STRIP, (i + 1) * STRIP)
        vm.normed[at, :] = (vm.scaled[at, :] * gain + shift).astype(bf16)

    def project(weight, out):
        for n in range(0, weight.shape[1], COLS):
            at = slice(n, n + COLS)
            out[:, at] = dot(vm.normed[...], weight[:, at]).astype(bf16)

    low = dot_nt(vm.normed[...], vm.down_weight[...]).astype(bf16)
    log_all = log_decays(dot(low, vm.up_weight[...]) + vm.decay_bias[...])
    lower = lower_ones(TILE)
    offset = None
    for b in range(blocks):
        at = slice(b * TILE, (b + 1) * TILE)
        log_rows = log_all[at]
        inclusive = running_sum(lower, log_rows)
        end = inclusive[TILE - 1 : TILE, :]
        vm.inclusive[at, :] = inclusive
        vm.before[at, :] = inclusive - log_rows
        vm.closing[b : b + 1, :] = end
        vm.offset[b : b + 1, :] = jnp.zeros_like(end) if offset is None else offset
        offset = end if offset is None else offset + end
    vm.offset[blocks : blocks + 1, :] = offset
    for g in range(GROUPS):
        vm.log_out[g : g + 1, :] = offset[:, g * LANES : (g + 1) * LANES]
    project(vm.key_weight, vm.key)
    project(vm.value_weight, vm.value)

    def log_copy(p, slot):
        return remote(
            vm.log_out, vm.logs.at[slot], sem.log_send.at[p], sem.log_recv.at[slot], crew * CREW + p
        )

    mates(lambda p: log_copy(p, post).start())
    vm.logs[post] = vm.log_out[...]

    def ctx_in(p):
        for copy in ctx_copies(p, p):
            copy.wait_recv()

    mates(ctx_in)
    for g in range(GROUPS):
        posts = list(range(g, CREW, GROUPS))
        logs = [vm.ctx_logs[p] for p in posts]
        tiles = [vm.ctx_in[p].astype(f32) for p in posts]
        forward, backward, log_sum = tiles[0][:SUB], tiles[-1][SUB:], logs[0]
        for i in range(1, len(posts)):
            forward = jnp.exp(logs[i]) * forward + tiles[i][:SUB]
            backward = jnp.exp(logs[-1 - i]) * backward + tiles[-1 - i][SUB:]
            log_sum = log_sum + logs[i]
        vm.ctx_crews_out[g] = jnp.concatenate([forward, backward], axis=0).astype(bf16)
        vm.ctx_crews_log[g : g + 1, :] = log_sum

    def ctx_crew_copies(c, slot):
        flat = c * CREW + post
        return (
            remote(
                vm.ctx_crews_out,
                vm.ctx_crews.at[slot],
                sem.ctx_crew_send.at[c],
                sem.ctx_crew_recv.at[slot],
                flat,
            ),
            remote(
                vm.ctx_crews_log,
                vm.ctx_crews_logs.at[slot],
                sem.ctx_crew_log_send.at[c],
                sem.ctx_crew_log_recv.at[slot],
                flat,
            ),
        )

    def ctx_crew_start(i):
        for copy in ctx_crew_copies(lax.rem(crew + i, crews), crew):
            copy.start()

    others(ctx_crew_start, crews)
    vm.ctx_crews[crew] = vm.ctx_crews_out[...]
    vm.ctx_crews_logs[crew] = vm.ctx_crews_log[...]

    def seg_copy(p, slot, g):
        return remote(
            vm.seg_out.at[g, p],
            vm.seg_in.at[g, slot],
            sem.seg_send.at[g, p],
            sem.seg_recv.at[g, slot],
            crew * CREW + p,
        )

    for g in range(GROUPS):
        lanes = slice(g * LANES, (g + 1) * LANES)
        v_lanes = slice(g * GV, (g + 1) * GV)
        whole = vm.offset[blocks : blocks + 1, lanes]
        both = []
        for b in range(blocks):
            at = slice(b * TILE, (b + 1) * TILE)
            keys = vm.key[at, lanes].astype(f32)
            start = vm.offset[b : b + 1, lanes]
            after = (whole - start) - vm.inclusive[at, lanes]
            both.append(
                jnp.concatenate(
                    [keys * jnp.exp(after), keys * jnp.exp(start + vm.before[at, lanes])], axis=1
                ).astype(bf16)
            )
        state = per_head(dot_tn(vm.value[:, v_lanes], jnp.concatenate(both, axis=0)), head_k)
        for j in range(CREW):
            at = slice(j * SUB, (j + 1) * SUB)
            vm.seg_out[g, j] = jnp.concatenate([state[at, :LANES], state[at, LANES:]], axis=0).astype(bf16)
        mates(lambda p: seg_copy(p, post, g).start())
        vm.seg_in[g, post] = vm.seg_out[g, post]

    mates(lambda p: log_copy(p, p).wait_recv())
    crew_log = vm.logs[0]
    for p in range(1, CREW):
        crew_log = crew_log + vm.logs[p]
    vm.crew_log[...] = crew_log

    def crew_log_copy(c, slot):
        return remote(
            vm.crew_log,
            vm.crew_logs.at[slot],
            sem.crew_log_send.at[c],
            sem.crew_log_recv.at[slot],
            c * CREW + post,
        )

    others(lambda i: crew_log_copy(lax.rem(crew + i, crews), crew).start(), crews)

    head_k1 = iota((TILE, LANES), 1) // DK
    head_v = iota((TILE, GV), 1) // DV
    t_index = iota((TILE, GROUP * TILE), 0)
    s_index = iota((TILE, GROUP * TILE), 1) % TILE

    def inside(g):
        lanes = slice(g * LANES, (g + 1) * LANES)
        v_lanes = slice(g * GV, (g + 1) * GV)
        whole = vm.offset[blocks : blocks + 1, lanes]
        for b in range(blocks):
            at = slice(b * TILE, (b + 1) * TILE)
            inclusive, before = vm.inclusive[at, lanes], vm.before[at, lanes]
            start = vm.offset[b : b + 1, lanes]
            closing = inclusive[TILE - 1 : TILE, :]
            middle = inclusive[TILE // 2 - 1 : TILE // 2, :]
            queries = vm.query[at, lanes].astype(f32) * DK ** (-0.5)
            keys = vm.key[at, lanes].astype(f32)
            scores = []
            for q_log, k_log in (
                (inclusive - middle, middle - inclusive),
                (middle - before, before - middle),
            ):
                k_stack = stacked((keys * jnp.exp(k_log)).astype(bf16), head_k1)
                scores.append(dot_nt((queries * jnp.exp(q_log)).astype(bf16), k_stack))
            both = jnp.where(t_index >= s_index, scores[0], 0.0) + jnp.where(
                t_index <= s_index, scores[1], 0.0
            )
            v_stack = stacked(vm.value[at, v_lanes], head_v)
            vm.within[at, v_lanes] = dot(both.astype(bf16), v_stack)
            vm.q_block[g, at, :] = jnp.concatenate(
                [queries * jnp.exp(inclusive), queries * jnp.exp(closing - before)], axis=1
            ).astype(bf16)
            vm.q_whole[g, at, :] = jnp.concatenate(
                [queries * jnp.exp(start + inclusive), queries * jnp.exp((whole - start) - before)], axis=1
            ).astype(bf16)

    def between(g):
        lanes = slice(g * LANES, (g + 1) * LANES)
        v_lanes = slice(g * GV, (g + 1) * GV)
        decays = [jnp.exp(vm.closing[b : b + 1, lanes]) for b in range(blocks)]
        left = []
        for b in range(blocks):
            at = slice(b * TILE, (b + 1) * TILE)
            keys = vm.key[at, lanes].astype(f32)
            both = jnp.concatenate(
                [
                    keys * jnp.exp(vm.closing[b : b + 1, lanes] - vm.inclusive[at, lanes]),
                    keys * jnp.exp(vm.before[at, lanes]),
                ],
                axis=1,
            ).astype(bf16)
            left.append(per_head(dot_tn(vm.value[at, v_lanes], both), head_k))
        forward = [jnp.zeros((DV, LANES), f32)]
        backward = [jnp.zeros((DV, LANES), f32)]
        for b in range(blocks - 1):
            forward.append(decays[b] * forward[b] + left[b][:, :LANES])
            back = blocks - 1 - b
            backward.insert(0, decays[back] * backward[0] + left[back][:, LANES:])
        for b in range(blocks):
            at = slice(b * TILE, (b + 1) * TILE)
            states = jnp.concatenate([forward[b], backward[b]], axis=1)
            across = dot_nt(vm.q_block[g, at, :], stacked(states, head_k).astype(bf16))
            vm.within[at, v_lanes] = vm.within[at, v_lanes] + across

    loads["query_weight"].wait()
    project(vm.query_weight, vm.query)
    inside(0)
    inside(1)

    decays = [[jnp.exp(vm.logs[p, g : g + 1, :]) for g in range(GROUPS)] for p in range(CREW)]
    for g in range(GROUPS):
        mates(lambda p: seg_copy(p, p, g).wait_recv())
    ends = []
    for g in range(GROUPS):
        forward = vm.seg_in[g, 0].astype(f32)[:SUB]
        for p in range(1, CREW):
            forward = decays[p][g] * forward + vm.seg_in[g, p].astype(f32)[:SUB]
        backward = vm.seg_in[g, CREW - 1].astype(f32)[SUB:]
        for p in range(CREW - 2, -1, -1):
            backward = decays[p][g] * backward + vm.seg_in[g, p].astype(f32)[SUB:]
        ends.append((forward, backward))
    for side in range(2):
        vm.crew_out[side] = jnp.concatenate([end[side] for end in ends], axis=0).astype(bf16)

    def crew_copy(c, slot, side):
        return remote(
            vm.crew_out.at[side],
            vm.crew_in.at[slot],
            sem.crew_send.at[c],
            sem.crew_recv.at[slot],
            c * CREW + post,
        )

    def crew_start(i):
        c = lax.rem(crew + i, crews)

        @pl.when(c > crew)
        def _():
            crew_copy(c, crew, 0).start()

        @pl.when(c < crew)
        def _():
            crew_copy(c, crew, 1).start()

    others(crew_start, crews)
    for g in range(2, GROUPS):
        inside(g)
    for g in range(GROUPS - 1):
        between(g)

    reduce_here(1, vm.gate_part, vm.gate_parts, vm.gate_total, vm.gate_totals, gate_spread)

    def ctx_arrived(i):
        c = lax.rem(crew + i, crews)
        for copy in ctx_crew_copies(c, c):
            copy.wait_recv()
        crew_log_copy(c, c).wait_recv()

    others(ctx_arrived, crews)
    zero = jnp.zeros((SUB, LANES), f32)
    forward, backward = [zero] * GROUPS, [zero] * GROUPS
    for a in range(crews):
        z = crews - 1 - a
        for g in range(GROUPS):
            forward[g] = (
                jnp.exp(vm.ctx_crews_logs[a, g : g + 1, :]) * forward[g]
                + vm.ctx_crews[a, g].astype(f32)[:SUB]
            )
            backward[g] = (
                jnp.exp(vm.ctx_crews_logs[z, g : g + 1, :]) * backward[g]
                + vm.ctx_crews[z, g].astype(f32)[SUB:]
            )

    def step_states(c, states):
        left = vm.crew_in[c].astype(f32)
        return tuple(
            jnp.exp(vm.crew_logs[c, g : g + 1, :]) * states[g] + left[g * SUB : (g + 1) * SUB]
            for g in range(GROUPS)
        )

    def from_before(c, states):
        crew_copy(c, c, 0).wait_recv()
        return step_states(c, states)

    def from_after(i, states):
        c = crews - 1 - i
        crew_copy(c, c, 1).wait_recv()
        return step_states(c, states)

    forward = lax.fori_loop(0, crew, from_before, tuple(forward))
    backward = lax.fori_loop(0, crews - 1 - crew, from_after, tuple(backward))

    def enter_copy(p, slot, g):
        return remote(
            vm.enter_out.at[g, p],
            vm.enter_in.at[g, slot],
            sem.enter_send.at[g, p],
            sem.enter_recv.at[g, slot],
            crew * CREW + p,
        )

    for g in range(GROUPS):
        state = forward[g]
        entering = []
        for p in range(CREW):
            entering.append(state)
            state = decays[p][g] * state + vm.seg_in[g, p].astype(f32)[:SUB]
        state = backward[g]
        for p in range(CREW - 1, -1, -1):
            vm.enter_out[g, p] = jnp.concatenate([entering[p], state], axis=0).astype(bf16)
            state = decays[p][g] * state + vm.seg_in[g, p].astype(f32)[SUB:]
        mates(lambda p: enter_copy(p, post, g).start())
        vm.enter_in[g, post] = vm.enter_out[g, post]

    loads["outgate_weight"].wait()
    for n in range(0, vm.outgate_weight.shape[1], COLS):
        at = slice(n, n + COLS)
        gate = dot(vm.normed[...], vm.outgate_weight[:, at]).astype(bf16).astype(f32)
        vm.silu[:, at] = gate / (1.0 + jnp.exp(-gate))
    between(GROUPS - 1)
    head_mean = jnp.where(iota((GV, GV), 0) // DV == iota((GV, GV), 1) // DV, 1.0 / DV, 0.0).astype(bf16)

    arrivals(gate_spread)
    for r in range(reducers):
        for t in range(tp_count):
            for s in range(share):
                row = vm.gate_totals[r * CREW + t, s]
                for x in range(1, CREW // tp_count):
                    row = row + vm.gate_totals[r * CREW + x * tp_count + t, s]
                at = (t * chunks + r * share + s) * LANES
                vm.mods[4:5, at : at + LANES] = row
    loads["out_weight"].wait()

    for r in range(reducers):

        @pl.when(crew != first_reducer + r)
        def _():
            for copy in to_reducer(r, crew):
                copy.wait_send()

    sent(spread)
    sent(gate_spread)

    def mate_sent(p):
        log_copy(p, post).wait_send()
        for copy in ctx_copies(p, post):
            copy.wait_send()
        for g in range(GROUPS):
            seg_copy(p, post, g).wait_send()

    mates(mate_sent)

    def crew_sent(i):
        c = lax.rem(crew + i, crews)
        for copy in ctx_crew_copies(c, crew):
            copy.wait_send()
        crew_log_copy(c, crew).wait_send()
        crew_copy(c, crew, 0).wait_send()

    others(crew_sent, crews)

    for g in range(GROUPS):
        v_lanes = slice(g * GV, (g + 1) * GV)
        mates(lambda p: enter_copy(p, p, g).wait_recv())
        units = [vm.enter_in[g, j].astype(f32) for j in range(CREW)]
        states = jnp.concatenate(
            [
                jnp.concatenate([u[:SUB] for u in units], axis=0),
                jnp.concatenate([u[SUB:] for u in units], axis=0),
            ],
            axis=1,
        )
        across = dot_nt(vm.q_whole[g], stacked(states, head_k).astype(bf16))
        mixed = vm.within[:, v_lanes] + across
        mean = dot((mixed * mixed).astype(bf16), head_mean)
        vm.gated[:, v_lanes] = (mixed * lax.rsqrt(mean + epsilon) * vm.silu[:, v_lanes]).astype(bf16)

    square = jnp.zeros((rows, LANES), f32)
    for n in range(0, width, COLS):
        at = slice(n, n + COLS)
        branch = dot(vm.gated[...], vm.out_weight[:, at]).astype(bf16)
        vm.branch[:, at] = branch
        branch = branch.astype(f32)
        branch = branch * branch
        for s in range(0, COLS, LANES):
            square = square + branch[:, s : s + LANES]
    factor = lax.rsqrt(jnp.sum(square, axis=1, keepdims=True) / width + epsilon)
    gain = vm.mods[4:5, :] * vm.post_gain[...]
    for i in range(rows // STRIP):
        at = slice(i * STRIP, (i + 1) * STRIP)
        hbm.out[at, :] = (
            vm.latent[at, :].astype(f32) + gain * (vm.branch[at, :].astype(f32) * factor[at])
        ).astype(bf16)

    for g in range(GROUPS):
        mates(lambda p: enter_copy(p, post, g).wait_send())


def shards(*operands):
    values = dict(zip(NAMES, operands))
    values["down_weight"] = values["down_weight"].T
    latent, context = values["latent"], values["context"]
    sp_count, tp_count = lax.axis_size("sp"), lax.axis_size("tp")
    count = sp_count * tp_count
    crews = count // CREW
    rows, width = latent.shape
    args, specs = [], []
    for name, value in values.items():
        vector = value.ndim == 1
        args.append(value.reshape(1, -1) if vector and value.dtype == f32 else value)
        specs.append(pl.BlockSpec(memory_space=pltpu.HBM))
    ctx_rows = context.shape[0] * GROUPS // tp_count
    chunks = values["shift_weight"].shape[1] // LANES
    reducers, share = reduction(chunks, crews)
    part_rows = -(-4 * share // SUB) * SUB
    keyw, valw = values["key_weight"].shape[1], values["value_weight"].shape[1]
    blocks = rows // TILE
    unit = (2 * SUB, LANES)
    buffers = dict(
        context=pltpu.VMEM((ctx_rows, width), bf16),
        cond=pltpu.VMEM((SUB, width), f32),
        part=pltpu.VMEM((reducers, part_rows, LANES), f32),
        parts=pltpu.VMEM((crews, part_rows, LANES), f32),
        total=pltpu.VMEM((part_rows, LANES), f32),
        totals=pltpu.VMEM((reducers * CREW, part_rows, LANES), f32),
        gate_part=pltpu.VMEM((reducers, share, 1, LANES), f32),
        gate_parts=pltpu.VMEM((crews, share, 1, LANES), f32),
        gate_total=pltpu.VMEM((share, 1, LANES), f32),
        gate_totals=pltpu.VMEM((reducers * CREW, share, 1, LANES), f32),
        mods=pltpu.VMEM((SUB, width), f32),
        scaled=pltpu.VMEM((rows, width), f32),
        ctx_scaled=pltpu.VMEM((ctx_rows, width), f32),
        normed=pltpu.VMEM((rows, width), bf16),
        ctx_out=pltpu.VMEM((CREW, *unit), bf16),
        ctx_in=pltpu.VMEM((CREW, *unit), bf16),
        ctx_log=pltpu.VMEM((1, LANES), f32),
        ctx_logs=pltpu.VMEM((CREW, 1, LANES), f32),
        ctx_crews_out=pltpu.VMEM((GROUPS, *unit), bf16),
        ctx_crews=pltpu.VMEM((crews, GROUPS, *unit), bf16),
        ctx_crews_log=pltpu.VMEM((SUB, LANES), f32),
        ctx_crews_logs=pltpu.VMEM((crews, SUB, LANES), f32),
        key=pltpu.VMEM((rows, keyw), bf16),
        query=pltpu.VMEM((rows, keyw), bf16),
        value=pltpu.VMEM((rows, valw), bf16),
        silu=pltpu.VMEM((rows, valw), f32),
        gated=pltpu.VMEM((rows, valw), bf16),
        inclusive=pltpu.VMEM((rows, keyw), f32),
        before=pltpu.VMEM((rows, keyw), f32),
        closing=pltpu.VMEM((blocks, keyw), f32),
        offset=pltpu.VMEM((blocks + 1, keyw), f32),
        log_out=pltpu.VMEM((SUB, LANES), f32),
        logs=pltpu.VMEM((CREW, SUB, LANES), f32),
        seg_out=pltpu.VMEM((GROUPS, CREW, *unit), bf16),
        seg_in=pltpu.VMEM((GROUPS, CREW, *unit), bf16),
        crew_out=pltpu.VMEM((2, GROUPS * SUB, LANES), bf16),
        crew_in=pltpu.VMEM((crews, GROUPS * SUB, LANES), bf16),
        crew_log=pltpu.VMEM((SUB, LANES), f32),
        crew_logs=pltpu.VMEM((crews, SUB, LANES), f32),
        enter_out=pltpu.VMEM((GROUPS, CREW, *unit), bf16),
        enter_in=pltpu.VMEM((GROUPS, CREW, *unit), bf16),
        q_block=pltpu.VMEM((GROUPS, rows, 2 * LANES), bf16),
        q_whole=pltpu.VMEM((GROUPS, rows, 2 * LANES), bf16),
        within=pltpu.VMEM((rows, valw), f32),
        branch=pltpu.VMEM((rows, width), bf16),
    )
    for name, value in zip(NAMES, args):
        if name not in buffers:
            buffers[name] = pltpu.VMEM(value.shape, value.dtype)
    dma = pltpu.SemaphoreType.DMA
    semaphores = dict(
        load=dma((len(NAMES),)),
        part_send=dma((reducers,)),
        part_recv=dma((crews,)),
        total_send=dma((count,)),
        total_recv=dma((reducers * CREW,)),
        gate_part_send=dma((reducers,)),
        gate_part_recv=dma((crews,)),
        gate_send=dma((count,)),
        gate_recv=dma((reducers * CREW,)),
        ctx_send=dma((CREW,)),
        ctx_recv=dma((CREW,)),
        ctx_log_send=dma((CREW,)),
        ctx_log_recv=dma((CREW,)),
        ctx_crew_send=dma((crews,)),
        ctx_crew_recv=dma((crews,)),
        ctx_crew_log_send=dma((crews,)),
        ctx_crew_log_recv=dma((crews,)),
        log_send=dma((CREW,)),
        log_recv=dma((CREW,)),
        seg_send=dma((GROUPS, CREW)),
        seg_recv=dma((GROUPS, CREW)),
        crew_send=dma((crews,)),
        crew_recv=dma((crews,)),
        crew_log_send=dma((crews,)),
        crew_log_recv=dma((crews,)),
        enter_send=dma((GROUPS, CREW)),
        enter_recv=dma((GROUPS, CREW)),
    )
    return pl.pallas_call(
        functools.partial(block_kernel, sp_count, tp_count),
        out_shape=pltpu.VMEM((rows, width), bf16),
        in_specs=specs,
        out_specs=pl.BlockSpec(memory_space=pltpu.VMEM),
        scratch_shapes=[buffers, semaphores],
        compiler_params=pltpu.CompilerParams(
            collective_id=0, has_side_effects=True, vmem_limit_bytes=VMEM_LIMIT
        ),
        name="block",
    )(*args)


def solution(mesh):
    placed = (
        P(("sp", "tp"), None),
        P("sp", None),
        P(),
        P(),
        P("sp", "tp"),
        P("sp", "tp"),
        P("sp", "tp"),
        P(),
        P(),
        P(),
        P(),
        P(),
        P(),
        P(),
        P(),
        P(),
        P(),
    )
    return jax.shard_map(
        shards, mesh=mesh, in_specs=placed, out_specs=P(("sp", "tp"), None), check_vma=False
    )
```

time: 50.9 us -> 36.7 us (0.72)
  Pallas kernels: 43.8 us -> 35.5 us
  local copies, waits for them, and re-layouts: 6.78 us -> 0.97 us
    pallas_call x1, Pallas kernels: 43.8 us -> 35.5 us  [shards(): pl.pallas_call(functools.partial(block_kernel, sp_count, tp_count), out_s...]
    unnamed x2 -> x1, local copies, waits for them, and re-layouts: 4.21 us -> 0.97 us
    reshape x2 -> x0, local copies, waits for them, and re-layouts: 2.57 us -> none  [shards(): args.append(value.reshape(1, -1) if vector else value)]
where the time goes in v2:
time: 36.7 us; the launch traced here: 36.5 us
  Pallas kernels  35.5 us (97%)
  local copies, waits for them, and re-layouts  0.97 us (3%)
    pallas_call x1, Pallas kernels, shards(): pl.pallas_call(functools.partial(block_kernel, sp_count, tp_count), out_s...  35.5 us
    unnamed x1, local copies, waits for them, and re-layouts  0.97 us

profile of v2, /device:TPU:0, one launch (start us, length us, event | category | flops | bytes accessed | tf_op | source)
XLA Modules:
  0.0 36.5 jit_solution(8027372564598241269)
XLA Ops:
  0.0 35.5 %block.1 = bf16[256,2048]{1,0:T(8,128)(2,1)S(1)} custom-call(bf16[256,2048]{1,0:T(8,128)(2,1)} %refs_0_.1, bf16[64,2048]{1,0:T(8,128)(2,1)} %refs_1_.1, bf16[2048]{0:T(1024)(128)(2,1)} %refs_2_.1, bf16[2048]{0:T(1024)(128)(2,1)} %refs_3_.1, bf16[256,512]{1,0:T(8,128)(2,1)} %refs_4_.1, bf16[256,512]{1,0:T(8,128)(2,1)} %refs_5_.1, bf16[256,512]{1,0:T(8,128)(2,1)} %refs_6_.1, ...), custom_call_target="tpu_custom_call" | custom-call | tf_op jit(solution)/shard_map/block/pallas_call | solution.py:839
  35.5 1.0 %copy.19 = bf16[256,2048]{1,0:T(8,128)(2,1)} copy(bf16[256,2048]{1,0:T(8,128)(2,1)S(1)} %block.1) | data formatting | bytes 2097152

commit v3 on v2

--- a/solution.py
+++ b/solution.py
@@ -17,6 +17,9 @@
 GV = GROUP * DV
 GROUPS = HEADS // GROUP
 CREW = DV // SUB
+CORES = 2
+OWNERS = CREW // CORES
+UNIT = DV // OWNERS
 MESH = pl.DeviceIdType.MESH
 TILE = 64
 COLS = 256
@@ -93,9 +96,7 @@
 def running_sum(lower, log_rows):
     high = log_rows.astype(bf16)
     rest = log_rows - high.astype(f32)
-    mid = rest.astype(bf16)
-    low = (rest - mid.astype(f32)).astype(bf16)
-    return dot(lower, high) + dot(lower, mid) + dot(lower, low)
+    return dot(lower, high) + dot(lower, rest.astype(bf16))
 
 
 def log_decays(values):
@@ -133,12 +134,16 @@
     sp, tp = lax.axis_index("sp"), lax.axis_index("tp")
     me = sp * tp_count + tp
     crew, post = me // CREW, lax.rem(me, CREW)
+    chip, core = post // CORES, lax.rem(post, CORES)
     rows, width = hbm.latent.shape
     blocks = rows // TILE
     row_share = hbm.shift_weight.shape[0]
     chunks = hbm.shift_weight.shape[1] // LANES
     reducers, share = reduction(chunks, crews)
     first_reducer = (crews - reducers) // 2
+    owner = core == CORES - 1
+    middle_crew = (crew >= first_reducer) & (crew < first_reducer + reducers)
+    reducer = owner & middle_crew
     ctx_rows = vm.context.shape[0]
     ctx_group = lax.rem(tp, GROUPS)
 
@@ -169,6 +174,17 @@
         for i in range(1, CREW):
             body(mate(i))
 
+    def owners(body):
+        for i in range(OWNERS):
+            at = lax.rem(chip + i, OWNERS)
+            if i == 0:
+                pl.when(jnp.logical_not(owner))(functools.partial(body, at))
+            else:
+                body(at)
+
+    def owner_of(at):
+        return at * CORES + CORES - 1
+
     ctx_at = pl.multiple_of((tp // GROUPS) * ctx_rows, SUB)
     hbm.context = hbm.context.at[pl.ds(ctx_at, ctx_rows)]
     loads = {
@@ -179,12 +195,24 @@
         loads[name].start()
 
     barrier = pltpu.get_barrier_semaphore()
-    others(
-        lambda i: pl.semaphore_signal(
-            barrier, inc=1, device_id=place(lax.rem(me + i, count)), device_id_type=MESH
-        ),
-        count,
-    )
+
+    def greet(flat):
+        pl.semaphore_signal(barrier, inc=1, device_id=place(flat), device_id_type=MESH)
+
+    for r in range(reducers):
+        for q in range(OWNERS):
+            flat = (first_reducer + r) * CREW + owner_of(q)
+
+            @pl.when(flat != me)
+            def _():
+                greet(flat)
+
+    @pl.when(reducer)
+    def _():
+        for c in range(crews):
+            for k in range(CORES):
+                if k < CORES - 1 or not first_reducer <= c < first_reducer + reducers:
+                    greet(c * CREW + chip * CORES + k)
 
     loads["latent_condition"].wait()
     loads["context_condition"].wait()
@@ -207,27 +235,33 @@
             else:
                 vm.part[r, row * 4 + which : row * 4 + which + 1, :] = part[0:1, at]
                 vm.part[r, row * 4 + 2 + which : row * 4 + 3 + which, :] = part[1:2, at]
-    pl.semaphore_wait(barrier, count - 1)
-
-    def to_reducer(r, slot):
-        flat = (first_reducer + r) * CREW + post
-        return (
-            remote(vm.part.at[r], vm.parts.at[slot], sem.part_send.at[r], sem.part_recv.at[slot], flat),
-            remote(
-                vm.gate_part.at[r],
-                vm.gate_parts.at[slot],
-                sem.gate_part_send.at[r],
-                sem.gate_part_recv.at[slot],
-                flat,
-            ),
-        )
+    @pl.when(reducer)
+    def _():
+        pl.semaphore_wait(barrier, count - 1)
+
+    @pl.when(jnp.logical_not(reducer))
+    def _():
+        pl.semaphore_wait(barrier, reducers)
+
+    def to_reducer(r, c, k, which):
+        part, parts = ((vm.part, vm.parts), (vm.gate_part, vm.gate_parts))[which]
+        return remote(
+            part.at[r],
+            parts.at[c, k],
+            sem.part_send.at[which, r],
+            sem.part_recv.at[which, c, k],
+            (first_reducer + r) * CREW + owner_of(chip),
+        )
+
+    def elsewhere(r):
+        return jnp.logical_not(owner & (crew == first_reducer + r))
 
     for which in range(2):
         for r in range(reducers):
 
-            @pl.when(crew != first_reducer + r)
+            @pl.when(elsewhere(r))
             def _():
-                to_reducer(r, crew)[which].start()
+                to_reducer(r, crew, core, which).start()
 
     loads["context"].wait()
     xc = vm.context[...].astype(f32)
@@ -242,7 +276,7 @@
 
     lax.fori_loop(0, rows // TILE, scale_strip, 0)
 
-    reduced = reducers * CREW
+    reduced = reducers * OWNERS
 
     def spread(flat, slot):
         return remote(
@@ -262,16 +296,20 @@
         for r in range(reducers):
             home = first_reducer + r
 
-            @pl.when(crew == home)
+            @pl.when(owner & (crew == home))
             def _():
-                slot = r * CREW + post
-                out = mine[r]
-                for c in range(crews):
-                    if c != home:
-                        to_reducer(r, c)[which].wait_recv()
-                        out = out + held[c]
-                total[...] = out
-                totals[slot] = out
+                slot = r * OWNERS + chip
+                for k in range(CORES):
+                    out = None
+                    for c in range(crews):
+                        if c == home and k == CORES - 1:
+                            term = mine[r]
+                        else:
+                            to_reducer(r, c, k, which).wait_recv()
+                            term = held[c, k]
+                        out = term if out is None else out + term
+                    total[k] = out
+                    totals[slot, k] = out
                 for c in sorted(range(crews), key=lambda c: -abs(c - home)):
 
                     def send(i, carry):
@@ -283,7 +321,7 @@
 
     def arrivals(copy):
         def arrived(i, carry):
-            @pl.when(first_reducer * CREW + i != me)
+            @pl.when((first_reducer + i // OWNERS) * CREW + owner_of(lax.rem(i, OWNERS)) != me)
             def _():
                 copy(me, i).wait_recv()
 
@@ -292,7 +330,7 @@
         lax.fori_loop(0, reduced, arrived, 0)
 
     def sent(copy):
-        @pl.when((crew >= first_reducer) & (crew < first_reducer + reducers))
+        @pl.when(reducer)
         def _():
             others(lambda i: copy(lax.rem(me + i, count), 0).wait_send(), count)
 
@@ -301,11 +339,16 @@
     for name in loads_needed + ("value_weight",):
         loads[name].wait()
     arrivals(spread)
+    def summed(totals, r, t):
+        out = None
+        for p in range(t, CREW, tp_count):
+            term = totals[r * OWNERS + p // CORES, p % CORES]
+            out = term if out is None else out + term
+        return out
+
     for r in range(reducers):
         for t in range(tp_count):
-            tile = vm.totals[r * CREW + t]
-            for x in range(1, CREW // tp_count):
-                tile = tile + vm.totals[r * CREW + x * tp_count + t]
+            tile = summed(vm.totals, r, t)
             for s in range(share):
                 at = (t * chunks + r * share + s) * LANES
                 vm.mods[0:4, at : at + LANES] = tile[s * 4 : s * 4 + 4]
@@ -325,27 +368,10 @@
         [keys * jnp.exp(closing - inclusive), keys * jnp.exp(inclusive - log_rows)], axis=1
     ).astype(bf16)
     state = per_head(dot_tn(values, both), head_k)
-    for j in range(CREW):
-        at = slice(j * SUB, (j + 1) * SUB)
+    for j in range(OWNERS):
+        at = slice(j * UNIT, (j + 1) * UNIT)
         vm.ctx_out[j] = jnp.concatenate([state[at, :LANES], state[at, LANES:]], axis=0).astype(bf16)
     vm.ctx_log[...] = closing
-
-    def ctx_copies(p, slot):
-        flat = crew * CREW + p
-        return (
-            remote(vm.ctx_out.at[p], vm.ctx_in.at[slot], sem.ctx_send.at[p], sem.ctx_recv.at[slot], flat),
-            remote(
-                vm.ctx_log, vm.ctx_logs.at[slot], sem.ctx_log_send.at[p], sem.ctx_log_recv.at[slot], flat
-            ),
-        )
-
-    def ctx_start(p):
-        for copy in ctx_copies(p, post):
-            copy.start()
-
-    mates(ctx_start)
-    vm.ctx_in[post] = vm.ctx_out[post]
-    vm.ctx_logs[post] = closing
 
     gain = vm.norm_gain[...] * (1.0 + vm.mods[1:2, :])
     shift = vm.mods[0:1, :]
@@ -378,65 +404,40 @@
     project(vm.key_weight, vm.key)
     project(vm.value_weight, vm.value)
 
-    def log_copy(p, slot):
+    def log_copy(o, p):
         return remote(
-            vm.log_out, vm.logs.at[slot], sem.log_send.at[p], sem.log_recv.at[slot], crew * CREW + p
-        )
-
-    mates(lambda p: log_copy(p, post).start())
-    vm.logs[post] = vm.log_out[...]
-
-    def ctx_in(p):
-        for copy in ctx_copies(p, p):
-            copy.wait_recv()
-
-    mates(ctx_in)
-    for g in range(GROUPS):
-        posts = list(range(g, CREW, GROUPS))
-        logs = [vm.ctx_logs[p] for p in posts]
-        tiles = [vm.ctx_in[p].astype(f32) for p in posts]
-        forward, backward, log_sum = tiles[0][:SUB], tiles[-1][SUB:], logs[0]
-        for i in range(1, len(posts)):
-            forward = jnp.exp(logs[i]) * forward + tiles[i][:SUB]
-            backward = jnp.exp(logs[-1 - i]) * backward + tiles[-1 - i][SUB:]
-            log_sum = log_sum + logs[i]
-        vm.ctx_crews_out[g] = jnp.concatenate([forward, backward], axis=0).astype(bf16)
-        vm.ctx_crews_log[g : g + 1, :] = log_sum
-
-    def ctx_crew_copies(c, slot):
-        flat = c * CREW + post
+            vm.log_out, vm.logs.at[p], sem.log_send.at[o], sem.log_recv.at[p], crew * CREW + owner_of(o)
+        )
+
+    def ctx_copies(o, p):
+        flat = crew * CREW + owner_of(o)
         return (
-            remote(
-                vm.ctx_crews_out,
-                vm.ctx_crews.at[slot],
-                sem.ctx_crew_send.at[c],
-                sem.ctx_crew_recv.at[slot],
-                flat,
-            ),
-            remote(
-                vm.ctx_crews_log,
-                vm.ctx_crews_logs.at[slot],
-                sem.ctx_crew_log_send.at[c],
-                sem.ctx_crew_log_recv.at[slot],
-                flat,
-            ),
-        )
-
-    def ctx_crew_start(i):
-        for copy in ctx_crew_copies(lax.rem(crew + i, crews), crew):
+            remote(vm.ctx_out.at[o], vm.ctx_in.at[p], sem.ctx_send.at[o], sem.ctx_recv.at[p], flat),
+            remote(vm.ctx_log, vm.ctx_logs.at[p], sem.ctx_log_send.at[o], sem.ctx_log_recv.at[p], flat),
+        )
+
+    def early_copies(o, p):
+        return (*ctx_copies(o, p), log_copy(o, p))
+
+    def early_start(o):
+        for copy in early_copies(o, post):
             copy.start()
 
-    others(ctx_crew_start, crews)
-    vm.ctx_crews[crew] = vm.ctx_crews_out[...]
-    vm.ctx_crews_logs[crew] = vm.ctx_crews_log[...]
-
-    def seg_copy(p, slot, g):
+    owners(early_start)
+
+    @pl.when(owner)
+    def _():
+        vm.ctx_in[post] = vm.ctx_out[chip]
+        vm.ctx_logs[post] = vm.ctx_log[...]
+        vm.logs[post] = vm.log_out[...]
+
+    def seg_copy(o, p, g):
         return remote(
-            vm.seg_out.at[g, p],
-            vm.seg_in.at[g, slot],
-            sem.seg_send.at[g, p],
-            sem.seg_recv.at[g, slot],
-            crew * CREW + p,
+            vm.seg_out.at[g, o],
+            vm.seg_in.at[g, p],
+            sem.seg_send.at[g, o],
+            sem.seg_recv.at[g, p],
+            crew * CREW + owner_of(o),
         )
 
     for g in range(GROUPS):
@@ -455,28 +456,18 @@
                 ).astype(bf16)
             )
         state = per_head(dot_tn(vm.value[:, v_lanes], jnp.concatenate(both, axis=0)), head_k)
-        for j in range(CREW):
-            at = slice(j * SUB, (j + 1) * SUB)
+        for j in range(OWNERS):
+            at = slice(j * UNIT, (j + 1) * UNIT)
             vm.seg_out[g, j] = jnp.concatenate([state[at, :LANES], state[at, LANES:]], axis=0).astype(bf16)
-        mates(lambda p: seg_copy(p, post, g).start())
-        vm.seg_in[g, post] = vm.seg_out[g, post]
-
-    mates(lambda p: log_copy(p, p).wait_recv())
-    crew_log = vm.logs[0]
-    for p in range(1, CREW):
-        crew_log = crew_log + vm.logs[p]
-    vm.crew_log[...] = crew_log
-
-    def crew_log_copy(c, slot):
-        return remote(
-            vm.crew_log,
-            vm.crew_logs.at[slot],
-            sem.crew_log_send.at[c],
-            sem.crew_log_recv.at[slot],
-            c * CREW + post,
-        )
-
-    others(lambda i: crew_log_copy(lax.rem(crew + i, crews), crew).start(), crews)
+        owners(lambda o: seg_copy(o, post, g).start())
+
+    @pl.when(owner)
+    def _():
+        for g in range(GROUPS):
+            vm.seg_in[g, post] = vm.seg_out[g, chip]
+
+    reduce_here(1, vm.gate_part, vm.gate_parts, vm.gate_total, vm.gate_totals, gate_spread)
+
 
     head_k1 = iota((TILE, LANES), 1) // DK
     head_v = iota((TILE, GV), 1) // DV
@@ -545,22 +536,54 @@
     loads["query_weight"].wait()
     project(vm.query_weight, vm.query)
     inside(0)
+
+    def ctx_crew_copies(c, slot):
+        flat = c * CREW + post
+        return (
+            remote(
+                vm.ctx_crews_out,
+                vm.ctx_crews.at[slot],
+                sem.ctx_crew_send.at[c],
+                sem.ctx_crew_recv.at[slot],
+                flat,
+            ),
+            remote(
+                vm.crew_log, vm.crew_logs.at[slot], sem.crew_log_send.at[c], sem.crew_log_recv.at[slot], flat
+            ),
+        )
+
+    @pl.when(owner)
+    def _():
+        def early_in(p):
+            for copy in early_copies(0, p):
+                copy.wait_recv()
+
+        mates(early_in)
+        crew_log = vm.logs[0]
+        for p in range(1, CREW):
+            crew_log = crew_log + vm.logs[p]
+        vm.crew_log[0] = crew_log
+        for g in range(GROUPS):
+            posts = list(range(g, CREW, GROUPS))
+            logs = [vm.ctx_logs[p] for p in posts]
+            tiles = [vm.ctx_in[p].astype(f32) for p in posts]
+            forward, backward, log_sum = tiles[0][:UNIT], tiles[-1][UNIT:], logs[0]
+            for i in range(1, len(posts)):
+                forward = jnp.exp(logs[i]) * forward + tiles[i][:UNIT]
+                backward = jnp.exp(logs[-1 - i]) * backward + tiles[-1 - i][UNIT:]
+                log_sum = log_sum + logs[i]
+            vm.ctx_crews_out[g] = jnp.concatenate([forward, backward], axis=0).astype(bf16)
+            vm.crew_log[1, g : g + 1, :] = log_sum
+
+        def ctx_crew_start(i):
+            for copy in ctx_crew_copies(lax.rem(crew + i, crews), crew):
+                copy.start()
+
+        others(ctx_crew_start, crews)
+        vm.ctx_crews[crew] = vm.ctx_crews_out[...]
+        vm.crew_logs[crew] = vm.crew_log[...]
+
     inside(1)
-
-    decays = [[jnp.exp(vm.logs[p, g : g + 1, :]) for g in range(GROUPS)] for p in range(CREW)]
-    for g in range(GROUPS):
-        mates(lambda p: seg_copy(p, p, g).wait_recv())
-    ends = []
-    for g in range(GROUPS):
-        forward = vm.seg_in[g, 0].astype(f32)[:SUB]
-        for p in range(1, CREW):
-            forward = decays[p][g] * forward + vm.seg_in[g, p].astype(f32)[:SUB]
-        backward = vm.seg_in[g, CREW - 1].astype(f32)[SUB:]
-        for p in range(CREW - 2, -1, -1):
-            backward = decays[p][g] * backward + vm.seg_in[g, p].astype(f32)[SUB:]
-        ends.append((forward, backward))
-    for side in range(2):
-        vm.crew_out[side] = jnp.concatenate([end[side] for end in ends], axis=0).astype(bf16)
 
     def crew_copy(c, slot, side):
         return remote(
@@ -571,149 +594,172 @@
             c * CREW + post,
         )
 
-    def crew_start(i):
-        c = lax.rem(crew + i, crews)
-
-        @pl.when(c > crew)
-        def _():
-            crew_copy(c, crew, 0).start()
-
-        @pl.when(c < crew)
-        def _():
-            crew_copy(c, crew, 1).start()
-
-    others(crew_start, crews)
+    def post_decay(p, g):
+        return jnp.exp(vm.logs[p, g : g + 1, :])
+
+    @pl.when(owner)
+    def _():
+        for g in range(GROUPS):
+            mates(lambda p: seg_copy(0, p, g).wait_recv())
+        at = slice(0, UNIT)
+        for g in range(GROUPS):
+            at = slice(g * UNIT, (g + 1) * UNIT)
+            forward = vm.seg_in[g, 0, :UNIT].astype(f32)
+            for p in range(1, CREW):
+                forward = post_decay(p, g) * forward + vm.seg_in[g, p, :UNIT].astype(f32)
+            backward = vm.seg_in[g, CREW - 1, UNIT:].astype(f32)
+            for p in range(CREW - 2, -1, -1):
+                backward = post_decay(p, g) * backward + vm.seg_in[g, p, UNIT:].astype(f32)
+            vm.crew_out[0, at, :] = forward.astype(bf16)
+            vm.crew_out[1, at, :] = backward.astype(bf16)
+
+        def crew_start(i):
+            c = lax.rem(crew + i, crews)
+
+            @pl.when(c > crew)
+            def _():
+                crew_copy(c, crew, 0).start()
+
+            @pl.when(c < crew)
+            def _():
+                crew_copy(c, crew, 1).start()
+
+        others(crew_start, crews)
+
     for g in range(2, GROUPS):
         inside(g)
-    for g in range(GROUPS - 1):
+    for g in range(GROUPS - 2):
         between(g)
 
-    reduce_here(1, vm.gate_part, vm.gate_parts, vm.gate_total, vm.gate_totals, gate_spread)
-
-    def ctx_arrived(i):
-        c = lax.rem(crew + i, crews)
-        for copy in ctx_crew_copies(c, c):
-            copy.wait_recv()
-        crew_log_copy(c, c).wait_recv()
-
-    others(ctx_arrived, crews)
-    zero = jnp.zeros((SUB, LANES), f32)
-    forward, backward = [zero] * GROUPS, [zero] * GROUPS
-    for a in range(crews):
-        z = crews - 1 - a
-        for g in range(GROUPS):
-            forward[g] = (
-                jnp.exp(vm.ctx_crews_logs[a, g : g + 1, :]) * forward[g]
-                + vm.ctx_crews[a, g].astype(f32)[:SUB]
-            )
-            backward[g] = (
-                jnp.exp(vm.ctx_crews_logs[z, g : g + 1, :]) * backward[g]
-                + vm.ctx_crews[z, g].astype(f32)[SUB:]
-            )
-
-    def step_states(c, states):
-        left = vm.crew_in[c].astype(f32)
-        return tuple(
-            jnp.exp(vm.crew_logs[c, g : g + 1, :]) * states[g] + left[g * SUB : (g + 1) * SUB]
-            for g in range(GROUPS)
-        )
-
-    def from_before(c, states):
-        crew_copy(c, c, 0).wait_recv()
-        return step_states(c, states)
-
-    def from_after(i, states):
-        c = crews - 1 - i
-        crew_copy(c, c, 1).wait_recv()
-        return step_states(c, states)
-
-    forward = lax.fori_loop(0, crew, from_before, tuple(forward))
-    backward = lax.fori_loop(0, crews - 1 - crew, from_after, tuple(backward))
-
-    def enter_copy(p, slot, g):
+    def enter_copy(p, o, g):
         return remote(
             vm.enter_out.at[g, p],
-            vm.enter_in.at[g, slot],
+            vm.enter_in.at[g, o],
             sem.enter_send.at[g, p],
-            sem.enter_recv.at[g, slot],
+            sem.enter_recv.at[g, o],
             crew * CREW + p,
         )
 
-    for g in range(GROUPS):
-        state = forward[g]
-        entering = []
-        for p in range(CREW):
-            entering.append(state)
-            state = decays[p][g] * state + vm.seg_in[g, p].astype(f32)[:SUB]
-        state = backward[g]
-        for p in range(CREW - 1, -1, -1):
-            vm.enter_out[g, p] = jnp.concatenate([entering[p], state], axis=0).astype(bf16)
-            state = decays[p][g] * state + vm.seg_in[g, p].astype(f32)[SUB:]
-        mates(lambda p: enter_copy(p, post, g).start())
-        vm.enter_in[g, post] = vm.enter_out[g, post]
+    @pl.when(owner)
+    def _():
+        def ctx_arrived(i):
+            c = lax.rem(crew + i, crews)
+            for copy in ctx_crew_copies(c, c):
+                copy.wait_recv()
+
+        others(ctx_arrived, crews)
+        zero = jnp.zeros((UNIT, LANES), f32)
+        forward, backward = [zero] * GROUPS, [zero] * GROUPS
+        for a in range(crews):
+            z = crews - 1 - a
+            for g in range(GROUPS):
+                forward[g] = (
+                    jnp.exp(vm.crew_logs[a, 1, g : g + 1, :]) * forward[g]
+                    + vm.ctx_crews[a, g, :UNIT].astype(f32)
+                )
+                backward[g] = (
+                    jnp.exp(vm.crew_logs[z, 1, g : g + 1, :]) * backward[g]
+                    + vm.ctx_crews[z, g, UNIT:].astype(f32)
+                )
+
+        def step_states(c, states):
+            left = vm.crew_in[c].astype(f32)
+            return tuple(
+                jnp.exp(vm.crew_logs[c, 0, g : g + 1, :]) * states[g] + left[g * UNIT : (g + 1) * UNIT]
+                for g in range(GROUPS)
+            )
+
+        def from_before(c, states):
+            crew_copy(c, c, 0).wait_recv()
+            return step_states(c, states)
+
+        def from_after(i, states):
+            c = crews - 1 - i
+            crew_copy(c, c, 1).wait_recv()
+            return step_states(c, states)
+
+        forward = lax.fori_loop(0, crew, from_before, tuple(forward))
+        backward = lax.fori_loop(0, crews - 1 - crew, from_after, tuple(backward))
+        for g in range(GROUPS):
+            state = forward[g]
+            for p in range(CREW):
+                vm.enter_out[g, p, :UNIT] = state.astype(bf16)
+                if p < CREW - 1:
+                    state = post_decay(p, g) * state + vm.seg_in[g, p, :UNIT].astype(f32)
+            state = backward[g]
+            for p in range(CREW - 1, -1, -1):
+                vm.enter_out[g, p, UNIT:] = state.astype(bf16)
+                if p > 0:
+                    state = post_decay(p, g) * state + vm.seg_in[g, p, UNIT:].astype(f32)
+            mates(lambda p: enter_copy(p, chip, g).start())
+        for g in range(GROUPS):
+            vm.enter_in[g, chip] = vm.enter_out[g, post]
 
     loads["outgate_weight"].wait()
     for n in range(0, vm.outgate_weight.shape[1], COLS):
         at = slice(n, n + COLS)
         gate = dot(vm.normed[...], vm.outgate_weight[:, at]).astype(bf16).astype(f32)
         vm.silu[:, at] = gate / (1.0 + jnp.exp(-gate))
-    between(GROUPS - 1)
+    for g in range(GROUPS - 2, GROUPS):
+        between(g)
     head_mean = jnp.where(iota((GV, GV), 0) // DV == iota((GV, GV), 1) // DV, 1.0 / DV, 0.0).astype(bf16)
 
     arrivals(gate_spread)
     for r in range(reducers):
         for t in range(tp_count):
+            tile = summed(vm.gate_totals, r, t)
             for s in range(share):
-                row = vm.gate_totals[r * CREW + t, s]
-                for x in range(1, CREW // tp_count):
-                    row = row + vm.gate_totals[r * CREW + x * tp_count + t, s]
                 at = (t * chunks + r * share + s) * LANES
-                vm.mods[4:5, at : at + LANES] = row
+                vm.mods[4:5, at : at + LANES] = tile[s]
     loads["out_weight"].wait()
 
-    for r in range(reducers):
-
-        @pl.when(crew != first_reducer + r)
-        def _():
-            for copy in to_reducer(r, crew):
-                copy.wait_send()
+    for which in range(2):
+        for r in range(reducers):
+
+            @pl.when(elsewhere(r))
+            def _():
+                to_reducer(r, crew, core, which).wait_send()
 
     sent(spread)
     sent(gate_spread)
 
-    def mate_sent(p):
-        log_copy(p, post).wait_send()
-        for copy in ctx_copies(p, post):
+    def to_owner_sent(o):
+        for copy in early_copies(o, post):
             copy.wait_send()
         for g in range(GROUPS):
-            seg_copy(p, post, g).wait_send()
-
-    mates(mate_sent)
-
-    def crew_sent(i):
-        c = lax.rem(crew + i, crews)
-        for copy in ctx_crew_copies(c, crew):
-            copy.wait_send()
-        crew_log_copy(c, crew).wait_send()
-        crew_copy(c, crew, 0).wait_send()
-
-    others(crew_sent, crews)
-
-    for g in range(GROUPS):
+            seg_copy(o, post, g).wait_send()
+
+    owners(to_owner_sent)
+
+    @pl.when(owner)
+    def _():
+        def crew_sent(i):
+            c = lax.rem(crew + i, crews)
+            for copy in ctx_crew_copies(c, crew):
+                copy.wait_send()
+            crew_copy(c, crew, 0).wait_send()
+
+        others(crew_sent, crews)
+
+    def finish(g):
         v_lanes = slice(g * GV, (g + 1) * GV)
-        mates(lambda p: enter_copy(p, p, g).wait_recv())
-        units = [vm.enter_in[g, j].astype(f32) for j in range(CREW)]
         states = jnp.concatenate(
             [
-                jnp.concatenate([u[:SUB] for u in units], axis=0),
-                jnp.concatenate([u[SUB:] for u in units], axis=0),
+                jnp.concatenate([vm.enter_in[g, o, :UNIT] for o in range(OWNERS)], axis=0),
+                jnp.concatenate([vm.enter_in[g, o, UNIT:] for o in range(OWNERS)], axis=0),
             ],
             axis=1,
         )
-        across = dot_nt(vm.q_whole[g], stacked(states, head_k).astype(bf16))
+        across = dot_nt(vm.q_whole[g], stacked(states, head_k))
         mixed = vm.within[:, v_lanes] + across
         mean = dot((mixed * mixed).astype(bf16), head_mean)
         vm.gated[:, v_lanes] = (mixed * lax.rsqrt(mean + epsilon) * vm.silu[:, v_lanes]).astype(bf16)
+
+    for half in range(0, GROUPS, 2):
+        for g in range(half, half + 2):
+            owners(lambda o: enter_copy(post, o, g).wait_recv())
+        for g in range(half, half + 2):
+            finish(g)
 
     square = jnp.zeros((rows, LANES), f32)
     for n in range(0, width, COLS):
@@ -732,8 +778,10 @@
             vm.latent[at, :].astype(f32) + gain * (vm.branch[at, :].astype(f32) * factor[at])
         ).astype(bf16)
 
-    for g in range(GROUPS):
-        mates(lambda p: enter_copy(p, post, g).wait_send())
+    @pl.when(owner)
+    def _():
+        for g in range(GROUPS):
+            mates(lambda p: enter_copy(p, chip, g).wait_send())
 
 
 def shards(*operands):
@@ -755,30 +803,28 @@
     part_rows = -(-4 * share // SUB) * SUB
     keyw, valw = values["key_weight"].shape[1], values["value_weight"].shape[1]
     blocks = rows // TILE
-    unit = (2 * SUB, LANES)
+    unit = (2 * UNIT, LANES)
     buffers = dict(
         context=pltpu.VMEM((ctx_rows, width), bf16),
         cond=pltpu.VMEM((SUB, width), f32),
         part=pltpu.VMEM((reducers, part_rows, LANES), f32),
-        parts=pltpu.VMEM((crews, part_rows, LANES), f32),
-        total=pltpu.VMEM((part_rows, LANES), f32),
-        totals=pltpu.VMEM((reducers * CREW, part_rows, LANES), f32),
+        parts=pltpu.VMEM((crews, CORES, part_rows, LANES), f32),
+        total=pltpu.VMEM((CORES, part_rows, LANES), f32),
+        totals=pltpu.VMEM((reducers * OWNERS, CORES, part_rows, LANES), f32),
         gate_part=pltpu.VMEM((reducers, share, 1, LANES), f32),
-        gate_parts=pltpu.VMEM((crews, share, 1, LANES), f32),
-        gate_total=pltpu.VMEM((share, 1, LANES), f32),
-        gate_totals=pltpu.VMEM((reducers * CREW, share, 1, LANES), f32),
+        gate_parts=pltpu.VMEM((crews, CORES, share, 1, LANES), f32),
+        gate_total=pltpu.VMEM((CORES, share, 1, LANES), f32),
+        gate_totals=pltpu.VMEM((reducers * OWNERS, CORES, share, 1, LANES), f32),
         mods=pltpu.VMEM((SUB, width), f32),
         scaled=pltpu.VMEM((rows, width), f32),
         ctx_scaled=pltpu.VMEM((ctx_rows, width), f32),
         normed=pltpu.VMEM((rows, width), bf16),
-        ctx_out=pltpu.VMEM((CREW, *unit), bf16),
+        ctx_out=pltpu.VMEM((OWNERS, *unit), bf16),
         ctx_in=pltpu.VMEM((CREW, *unit), bf16),
         ctx_log=pltpu.VMEM((1, LANES), f32),
         ctx_logs=pltpu.VMEM((CREW, 1, LANES), f32),
         ctx_crews_out=pltpu.VMEM((GROUPS, *unit), bf16),
         ctx_crews=pltpu.VMEM((crews, GROUPS, *unit), bf16),
-        ctx_crews_log=pltpu.VMEM((SUB, LANES), f32),
-        ctx_crews_logs=pltpu.VMEM((crews, SUB, LANES), f32),
         key=pltpu.VMEM((rows, keyw), bf16),
         query=pltpu.VMEM((rows, keyw), bf16),
         value=pltpu.VMEM((rows, valw), bf16),
@@ -790,14 +836,14 @@
         offset=pltpu.VMEM((blocks + 1, keyw), f32),
         log_out=pltpu.VMEM((SUB, LANES), f32),
         logs=pltpu.VMEM((CREW, SUB, LANES), f32),
-        seg_out=pltpu.VMEM((GROUPS, CREW, *unit), bf16),
+        seg_out=pltpu.VMEM((GROUPS, OWNERS, *unit), bf16),
         seg_in=pltpu.VMEM((GROUPS, CREW, *unit), bf16),
-        crew_out=pltpu.VMEM((2, GROUPS * SUB, LANES), bf16),
-        crew_in=pltpu.VMEM((crews, GROUPS * SUB, LANES), bf16),
-        crew_log=pltpu.VMEM((SUB, LANES), f32),
-        crew_logs=pltpu.VMEM((crews, SUB, LANES), f32),
+        crew_out=pltpu.VMEM((2, GROUPS * UNIT, LANES), bf16),
+        crew_in=pltpu.VMEM((crews, GROUPS * UNIT, LANES), bf16),
+        crew_log=pltpu.VMEM((2, SUB, LANES), f32),
+        crew_logs=pltpu.VMEM((crews, 2, SUB, LANES), f32),
         enter_out=pltpu.VMEM((GROUPS, CREW, *unit), bf16),
-        enter_in=pltpu.VMEM((GROUPS, CREW, *unit), bf16),
+        enter_in=pltpu.VMEM((GROUPS, OWNERS, *unit), bf16),
         q_block=pltpu.VMEM((GROUPS, rows, 2 * LANES), bf16),
         q_whole=pltpu.VMEM((GROUPS, rows, 2 * LANES), bf16),
         within=pltpu.VMEM((rows, valw), f32),
@@ -809,32 +855,28 @@
     dma = pltpu.SemaphoreType.DMA
     semaphores = dict(
         load=dma((len(NAMES),)),
-        part_send=dma((reducers,)),
-        part_recv=dma((crews,)),
+        part_send=dma((2, reducers)),
+        part_recv=dma((2, crews, CORES)),
         total_send=dma((count,)),
-        total_recv=dma((reducers * CREW,)),
-        gate_part_send=dma((reducers,)),
-        gate_part_recv=dma((crews,)),
+        total_recv=dma((reducers * OWNERS,)),
         gate_send=dma((count,)),
-        gate_recv=dma((reducers * CREW,)),
-        ctx_send=dma((CREW,)),
+        gate_recv=dma((reducers * OWNERS,)),
+        ctx_send=dma((OWNERS,)),
         ctx_recv=dma((CREW,)),
-        ctx_log_send=dma((CREW,)),
+        ctx_log_send=dma((OWNERS,)),
         ctx_log_recv=dma((CREW,)),
+        log_send=dma((OWNERS,)),
+        log_recv=dma((CREW,)),
+        seg_send=dma((GROUPS, OWNERS)),
+        seg_recv=dma((GROUPS, CREW)),
         ctx_crew_send=dma((crews,)),
         ctx_crew_recv=dma((crews,)),
-        ctx_crew_log_send=dma((crews,)),
-        ctx_crew_log_recv=dma((crews,)),
-        log_send=dma((CREW,)),
-        log_recv=dma((CREW,)),
-        seg_send=dma((GROUPS, CREW)),
-        seg_recv=dma((GROUPS, CREW)),
+        crew_log_send=dma((crews,)),
+        crew_log_recv=dma((crews,)),
         crew_send=dma((crews,)),
         crew_recv=dma((crews,)),
-        crew_log_send=dma((crews,)),
-        crew_log_recv=dma((crews,)),
         enter_send=dma((GROUPS, CREW)),
-        enter_recv=dma((GROUPS, CREW)),
+        enter_recv=dma((GROUPS, OWNERS)),
     )
     return pl.pallas_call(
         functools.partial(block_kernel, sp_count, tp_count),

time: 36.7 us -> 33 us (0.90)
  Pallas kernels: 35.5 us -> 31.9 us
    pallas_call x1, Pallas kernels: 35.5 us -> 31.9 us  [shards(): pl.pallas_call(functools.partial(block_kernel, sp_count, tp_count), out_s...]
where the time goes in v3:
time: 33 us; the launch traced here: 32.9 us
  Pallas kernels  31.9 us (97%)
  local copies, waits for them, and re-layouts  0.97 us (3%)
    pallas_call x1, Pallas kernels, shards(): pl.pallas_call(functools.partial(block_kernel, sp_count, tp_count), out_s...  31.9 us
    unnamed x1, local copies, waits for them, and re-layouts  0.97 us

profile of v3, /device:TPU:0, one launch (start us, length us, event | category | flops | bytes accessed | tf_op | source)
XLA Modules:
  0.0 32.9 jit_solution(9135351758773110600)
XLA Ops:
  0.0 31.9 %block.1 = bf16[256,2048]{1,0:T(8,128)(2,1)S(1)} custom-call(bf16[256,2048]{1,0:T(8,128)(2,1)} %refs_0_.1, bf16[64,2048]{1,0:T(8,128)(2,1)} %refs_1_.1, bf16[2048]{0:T(1024)(128)(2,1)} %refs_2_.1, bf16[2048]{0:T(1024)(128)(2,1)} %refs_3_.1, bf16[256,512]{1,0:T(8,128)(2,1)} %refs_4_.1, bf16[256,512]{1,0:T(8,128)(2,1)} %refs_5_.1, bf16[256,512]{1,0:T(8,128)(2,1)} %refs_6_.1, ...), custom_call_target="tpu_custom_call" | custom-call | tf_op jit(solution)/shard_map/block/pallas_call | solution.py:881
  31.9 1.0 %copy.19 = bf16[256,2048]{1,0:T(8,128)(2,1)} copy(bf16[256,2048]{1,0:T(8,128)(2,1)S(1)} %block.1) | data formatting | bytes 2097152

commit v4 on v3

--- a/solution.py
+++ b/solution.py
@@ -51,14 +51,14 @@
     "shift_weight",
     "scale_weight",
     "gate_weight",
+)
+LATER = (
     "context",
     "latent",
-)
-LATER = (
+    "down_weight",
     "norm_gain",
     "decay_bias",
     "post_gain",
-    "down_weight",
     "up_weight",
     "key_weight",
     "value_weight",
@@ -100,7 +100,7 @@
 
 
 def log_decays(values):
-    return (jnp.minimum(values, 0.0) - jnp.log1p(jnp.exp(-jnp.abs(values)))) / decay_temper
+    return (jnp.minimum(values, 0.0) - jnp.log(1.0 + jnp.exp(-jnp.abs(values)))) * (1.0 / decay_temper)
 
 
 def rms_factor(values):
@@ -133,8 +133,8 @@
     crews = count // CREW
     sp, tp = lax.axis_index("sp"), lax.axis_index("tp")
     me = sp * tp_count + tp
-    crew, post = me // CREW, lax.rem(me, CREW)
-    chip, core = post // CORES, lax.rem(post, CORES)
+    crew, post = lax.div(me, CREW), lax.rem(me, CREW)
+    chip, core = lax.div(post, CORES), lax.rem(post, CORES)
     rows, width = hbm.latent.shape
     blocks = rows // TILE
     row_share = hbm.shift_weight.shape[0]
@@ -148,7 +148,7 @@
     ctx_group = lax.rem(tp, GROUPS)
 
     def place(flat):
-        return (flat // tp_count, lax.rem(flat, tp_count))
+        return (lax.div(flat, jnp.int32(tp_count)), lax.rem(flat, jnp.int32(tp_count)))
 
     def remote(src, dst, send, recv, flat):
         return pltpu.make_async_remote_copy(
@@ -222,8 +222,6 @@
     pick = iota((STRIP, row_share), 0) == 0
     raw = jnp.where(pick, vm.cond[0:1, mine], vm.cond[1:2, mine])
     cond = (raw / (1.0 + jnp.exp(-raw))).astype(bf16)
-    for name in LATER:
-        loads[name].start()
     for which, name in enumerate(("shift_weight", "scale_weight", "gate_weight")):
         loads[name].wait()
         part = dot(cond, getattr(vm, name)[...])
@@ -235,6 +233,8 @@
             else:
                 vm.part[r, row * 4 + which : row * 4 + which + 1, :] = part[0:1, at]
                 vm.part[r, row * 4 + 2 + which : row * 4 + 3 + which, :] = part[1:2, at]
+    for name in LATER:
+        loads[name].start()
     @pl.when(reducer)
     def _():
         pl.semaphore_wait(barrier, count - 1)
@@ -242,6 +242,8 @@
     @pl.when(jnp.logical_not(reducer))
     def _():
         pl.semaphore_wait(barrier, reducers)
+
+    home_core = (CORES - 1, 0)
 
     def to_reducer(r, c, k, which):
         part, parts = ((vm.part, vm.parts), (vm.gate_part, vm.gate_parts))[which]
@@ -250,18 +252,20 @@
             parts.at[c, k],
             sem.part_send.at[which, r],
             sem.part_recv.at[which, c, k],
-            (first_reducer + r) * CREW + owner_of(chip),
-        )
-
-    def elsewhere(r):
-        return jnp.logical_not(owner & (crew == first_reducer + r))
-
-    for which in range(2):
+            (first_reducer + r) * CREW + chip * CORES + home_core[which],
+        )
+
+    def elsewhere(r, which):
+        return jnp.logical_not((core == home_core[which]) & (crew == first_reducer + r))
+
+    def send_parts(which):
         for r in range(reducers):
 
-            @pl.when(elsewhere(r))
+            @pl.when(elsewhere(r, which))
             def _():
                 to_reducer(r, crew, core, which).start()
+
+    send_parts(0)
 
     loads["context"].wait()
     xc = vm.context[...].astype(f32)
@@ -275,19 +279,21 @@
         return carry
 
     lax.fori_loop(0, rows // TILE, scale_strip, 0)
+    loads["down_weight"].wait()
+    vm.down[...] = vm.down_weight[...].T
 
     reduced = reducers * OWNERS
 
-    def spread(flat, slot):
+    def spread(flat, slot, step=0):
         return remote(
-            vm.total, vm.totals.at[slot], sem.total_send.at[flat], sem.total_recv.at[slot], flat
-        )
-
-    def gate_spread(flat, slot):
+            vm.total, vm.totals.at[slot], sem.total_send.at[step], sem.total_recv.at[slot], flat
+        )
+
+    def gate_spread(flat, slot, step=0):
         return remote(
             vm.gate_total,
             vm.gate_totals.at[slot],
-            sem.gate_send.at[flat],
+            sem.gate_send.at[step],
             sem.gate_recv.at[slot],
             flat,
         )
@@ -296,13 +302,13 @@
         for r in range(reducers):
             home = first_reducer + r
 
-            @pl.when(owner & (crew == home))
+            @pl.when((core == home_core[which]) & (crew == home))
             def _():
                 slot = r * OWNERS + chip
                 for k in range(CORES):
                     out = None
                     for c in range(crews):
-                        if c == home and k == CORES - 1:
+                        if c == home and k == home_core[which]:
                             term = mine[r]
                         else:
                             to_reducer(r, c, k, which).wait_recv()
@@ -313,32 +319,34 @@
                 for c in sorted(range(crews), key=lambda c: -abs(c - home)):
 
                     def send(i, carry):
-                        flat = c * CREW + mate(i)
-                        copy(flat, slot).start()
+                        copy(c * CREW + mate(i), slot, c * CREW + i).start()
                         return carry
 
                     lax.fori_loop(0 if c != home else 1, CREW, send, 0)
 
-    def arrivals(copy):
-        def arrived(i, carry):
-            @pl.when((first_reducer + i // OWNERS) * CREW + owner_of(lax.rem(i, OWNERS)) != me)
+    def arrivals(which, copy):
+        for i in range(reduced):
+            flat = (first_reducer + i // OWNERS) * CREW + i % OWNERS * CORES + home_core[which]
+
+            @pl.when(flat != me)
             def _():
                 copy(me, i).wait_recv()
 
-            return carry
-
-        lax.fori_loop(0, reduced, arrived, 0)
-
-    def sent(copy):
-        @pl.when(reducer)
-        def _():
-            others(lambda i: copy(lax.rem(me + i, count), 0).wait_send(), count)
+    def sent(which, copy):
+        for r in range(reducers):
+            home = first_reducer + r
+
+            @pl.when((core == home_core[which]) & (crew == home))
+            def _():
+                for step in range(count):
+                    if step != home * CREW:
+                        copy(me, 0, step).wait_send()
 
     reduce_here(0, vm.part, vm.parts, vm.total, vm.totals, spread)
-    loads_needed = ("norm_gain", "decay_bias", "post_gain", "down_weight", "up_weight", "key_weight")
+    loads_needed = ("norm_gain", "decay_bias", "post_gain", "up_weight", "key_weight")
     for name in loads_needed + ("value_weight",):
         loads[name].wait()
-    arrivals(spread)
+    arrivals(0, spread)
     def summed(totals, r, t):
         out = None
         for p in range(t, CREW, tp_count):
@@ -358,7 +366,7 @@
     head_k = iota((DV, 2 * LANES), 1) % LANES // DK
     key_at = pl.ds(pl.multiple_of(ctx_group * LANES, LANES), LANES)
     val_at = pl.ds(pl.multiple_of(ctx_group * GV, GV), GV)
-    low = dot_nt(ctx_normed, vm.down_weight[...]).astype(bf16)
+    low = dot(ctx_normed, vm.down[...]).astype(bf16)
     log_rows = log_decays(dot(low, vm.up_weight[:, key_at]) + vm.decay_bias[:, key_at])
     keys = dot(ctx_normed, vm.key_weight[:, key_at]).astype(bf16).astype(f32)
     values = dot(ctx_normed, vm.value_weight[:, val_at]).astype(bf16)
@@ -373,6 +381,19 @@
         vm.ctx_out[j] = jnp.concatenate([state[at, :LANES], state[at, LANES:]], axis=0).astype(bf16)
     vm.ctx_log[...] = closing
 
+    def ctx_copies(o, p):
+        flat = crew * CREW + owner_of(o)
+        return (
+            remote(vm.ctx_out.at[o], vm.ctx_in.at[p], sem.ctx_send.at[o], sem.ctx_recv.at[p], flat),
+            remote(vm.ctx_log, vm.ctx_logs.at[p], sem.ctx_log_send.at[o], sem.ctx_log_recv.at[p], flat),
+        )
+
+    def ctx_start(o):
+        for copy in ctx_copies(o, post):
+            copy.start()
+
+    owners(ctx_start)
+
     gain = vm.norm_gain[...] * (1.0 + vm.mods[1:2, :])
     shift = vm.mods[0:1, :]
     for i in range(rows // STRIP):
@@ -384,13 +405,19 @@
             at = slice(n, n + COLS)
             out[:, at] = dot(vm.normed[...], weight[:, at]).astype(bf16)
 
-    low = dot_nt(vm.normed[...], vm.down_weight[...]).astype(bf16)
-    log_all = log_decays(dot(low, vm.up_weight[...]) + vm.decay_bias[...])
+    def project_tile(weight, out, n):
+        at = slice(n, min(n + COLS, weight.shape[1]))
+        out[:, at] = dot(vm.normed[...], weight[:, at]).astype(bf16)
+
+    tiles = [(vm.key_weight, vm.key, n) for n in range(0, vm.key_weight.shape[1], COLS)]
+    tiles += [(vm.value_weight, vm.value, n) for n in range(0, vm.value_weight.shape[1], COLS)]
+    low = dot(vm.normed[...], vm.down[...]).astype(bf16)
+    project_tile(*tiles.pop(0))
     lower = lower_ones(TILE)
     offset = None
     for b in range(blocks):
         at = slice(b * TILE, (b + 1) * TILE)
-        log_rows = log_all[at]
+        log_rows = log_decays(dot(low[at], vm.up_weight[...]) + vm.decay_bias[...])
         inclusive = running_sum(lower, log_rows)
         end = inclusive[TILE - 1 : TILE, :]
         vm.inclusive[at, :] = inclusive
@@ -398,32 +425,25 @@
         vm.closing[b : b + 1, :] = end
         vm.offset[b : b + 1, :] = jnp.zeros_like(end) if offset is None else offset
         offset = end if offset is None else offset + end
+        if tiles:
+            project_tile(*tiles.pop(0))
     vm.offset[blocks : blocks + 1, :] = offset
     for g in range(GROUPS):
         vm.log_out[g : g + 1, :] = offset[:, g * LANES : (g + 1) * LANES]
-    project(vm.key_weight, vm.key)
-    project(vm.value_weight, vm.value)
+    while tiles:
+        project_tile(*tiles.pop(0))
+
+    send_parts(1)
 
     def log_copy(o, p):
         return remote(
             vm.log_out, vm.logs.at[p], sem.log_send.at[o], sem.log_recv.at[p], crew * CREW + owner_of(o)
         )
 
-    def ctx_copies(o, p):
-        flat = crew * CREW + owner_of(o)
-        return (
-            remote(vm.ctx_out.at[o], vm.ctx_in.at[p], sem.ctx_send.at[o], sem.ctx_recv.at[p], flat),
-            remote(vm.ctx_log, vm.ctx_logs.at[p], sem.ctx_log_send.at[o], sem.ctx_log_recv.at[p], flat),
-        )
-
     def early_copies(o, p):
         return (*ctx_copies(o, p), log_copy(o, p))
 
-    def early_start(o):
-        for copy in early_copies(o, post):
-            copy.start()
-
-    owners(early_start)
+    owners(lambda o: log_copy(o, post).start())
 
     @pl.when(owner)
     def _():
@@ -431,12 +451,14 @@
         vm.ctx_logs[post] = vm.ctx_log[...]
         vm.logs[post] = vm.log_out[...]
 
+    every = pl.ds(0, GROUPS)
+
     def seg_copy(o, p, g):
         return remote(
-            vm.seg_out.at[g, o],
-            vm.seg_in.at[g, p],
-            sem.seg_send.at[g, o],
-            sem.seg_recv.at[g, p],
+            vm.seg_out.at[o, g],
+            vm.seg_in.at[p, g],
+            sem.seg_send.at[o],
+            sem.seg_recv.at[p],
             crew * CREW + owner_of(o),
         )
 
@@ -448,26 +470,24 @@
         for b in range(blocks):
             at = slice(b * TILE, (b + 1) * TILE)
             keys = vm.key[at, lanes].astype(f32)
-            start = vm.offset[b : b + 1, lanes]
-            after = (whole - start) - vm.inclusive[at, lanes]
+            start, closing = vm.offset[b : b + 1, lanes], vm.closing[b : b + 1, lanes]
+            ahead = keys * jnp.exp(closing - vm.inclusive[at, lanes])
+            behind = keys * jnp.exp(vm.before[at, lanes])
+            vm.k_block[g, at, :] = jnp.concatenate([ahead, behind], axis=1).astype(bf16)
             both.append(
                 jnp.concatenate(
-                    [keys * jnp.exp(after), keys * jnp.exp(start + vm.before[at, lanes])], axis=1
+                    [ahead * jnp.exp((whole - start) - closing), behind * jnp.exp(start)], axis=1
                 ).astype(bf16)
             )
         state = per_head(dot_tn(vm.value[:, v_lanes], jnp.concatenate(both, axis=0)), head_k)
         for j in range(OWNERS):
             at = slice(j * UNIT, (j + 1) * UNIT)
-            vm.seg_out[g, j] = jnp.concatenate([state[at, :LANES], state[at, LANES:]], axis=0).astype(bf16)
+            vm.seg_out[j, g] = jnp.concatenate([state[at, :LANES], state[at, LANES:]], axis=0).astype(bf16)
         owners(lambda o: seg_copy(o, post, g).start())
 
     @pl.when(owner)
     def _():
-        for g in range(GROUPS):
-            vm.seg_in[g, post] = vm.seg_out[g, chip]
-
-    reduce_here(1, vm.gate_part, vm.gate_parts, vm.gate_total, vm.gate_totals, gate_spread)
-
+        vm.seg_in[post] = vm.seg_out[chip]
 
     head_k1 = iota((TILE, LANES), 1) // DK
     head_v = iota((TILE, GV), 1) // DV
@@ -498,11 +518,11 @@
             )
             v_stack = stacked(vm.value[at, v_lanes], head_v)
             vm.within[at, v_lanes] = dot(both.astype(bf16), v_stack)
-            vm.q_block[g, at, :] = jnp.concatenate(
-                [queries * jnp.exp(inclusive), queries * jnp.exp(closing - before)], axis=1
-            ).astype(bf16)
+            ahead = queries * jnp.exp(inclusive)
+            behind = queries * jnp.exp(closing - before)
+            vm.q_block[g, at, :] = jnp.concatenate([ahead, behind], axis=1).astype(bf16)
             vm.q_whole[g, at, :] = jnp.concatenate(
-                [queries * jnp.exp(start + inclusive), queries * jnp.exp((whole - start) - before)], axis=1
+                [ahead * jnp.exp(start), behind * jnp.exp((whole - start) - closing)], axis=1
             ).astype(bf16)
 
     def between(g):
@@ -512,15 +532,7 @@
         left = []
         for b in range(blocks):
             at = slice(b * TILE, (b + 1) * TILE)
-            keys = vm.key[at, lanes].astype(f32)
-            both = jnp.concatenate(
-                [
-                    keys * jnp.exp(vm.closing[b : b + 1, lanes] - vm.inclusive[at, lanes]),
-                    keys * jnp.exp(vm.before[at, lanes]),
-                ],
-                axis=1,
-            ).astype(bf16)
-            left.append(per_head(dot_tn(vm.value[at, v_lanes], both), head_k))
+            left.append(per_head(dot_tn(vm.value[at, v_lanes], vm.k_block[g, at, :]), head_k))
         forward = [jnp.zeros((DV, LANES), f32)]
         backward = [jnp.zeros((DV, LANES), f32)]
         for b in range(blocks - 1):
@@ -559,10 +571,11 @@
                 copy.wait_recv()
 
         mates(early_in)
+        vm.decay[...] = jnp.exp(vm.logs[...])
         crew_log = vm.logs[0]
         for p in range(1, CREW):
             crew_log = crew_log + vm.logs[p]
-        vm.crew_log[0] = crew_log
+        vm.crew_log[0, :GROUPS] = crew_log
         for g in range(GROUPS):
             posts = list(range(g, CREW, GROUPS))
             logs = [vm.ctx_logs[p] for p in posts]
@@ -585,6 +598,8 @@
 
     inside(1)
 
+    reduce_here(1, vm.gate_part, vm.gate_parts, vm.gate_total, vm.gate_totals, gate_spread)
+
     def crew_copy(c, slot, side):
         return remote(
             vm.crew_out.at[side],
@@ -595,34 +610,32 @@
         )
 
     def post_decay(p, g):
-        return jnp.exp(vm.logs[p, g : g + 1, :])
+        return vm.decay[p, g : g + 1, :]
 
     @pl.when(owner)
     def _():
-        for g in range(GROUPS):
-            mates(lambda p: seg_copy(0, p, g).wait_recv())
-        at = slice(0, UNIT)
+        mates(lambda p: seg_copy(0, p, every).wait_recv())
         for g in range(GROUPS):
             at = slice(g * UNIT, (g + 1) * UNIT)
-            forward = vm.seg_in[g, 0, :UNIT].astype(f32)
+            forward = vm.seg_in[0, g, :UNIT].astype(f32)
             for p in range(1, CREW):
-                forward = post_decay(p, g) * forward + vm.seg_in[g, p, :UNIT].astype(f32)
-            backward = vm.seg_in[g, CREW - 1, UNIT:].astype(f32)
+                forward = post_decay(p, g) * forward + vm.seg_in[p, g, :UNIT].astype(f32)
+            backward = vm.seg_in[CREW - 1, g, UNIT:].astype(f32)
             for p in range(CREW - 2, -1, -1):
-                backward = post_decay(p, g) * backward + vm.seg_in[g, p, UNIT:].astype(f32)
+                backward = post_decay(p, g) * backward + vm.seg_in[p, g, UNIT:].astype(f32)
             vm.crew_out[0, at, :] = forward.astype(bf16)
             vm.crew_out[1, at, :] = backward.astype(bf16)
 
         def crew_start(i):
-            c = lax.rem(crew + i, crews)
-
-            @pl.when(c > crew)
+            ahead, behind = crews - i, i - 1
+
+            @pl.when(ahead > crew)
             def _():
-                crew_copy(c, crew, 0).start()
-
-            @pl.when(c < crew)
+                crew_copy(ahead, crew, 0).start()
+
+            @pl.when(behind < crew)
             def _():
-                crew_copy(c, crew, 1).start()
+                crew_copy(behind, crew, 1).start()
 
         others(crew_start, crews)
 
@@ -631,12 +644,15 @@
     for g in range(GROUPS - 2):
         between(g)
 
-    def enter_copy(p, o, g):
+    half = GROUPS // 2
+
+    def enter_copy(p, o, h):
+        part = pl.ds(h * half, half)
         return remote(
-            vm.enter_out.at[g, p],
-            vm.enter_in.at[g, o],
-            sem.enter_send.at[g, p],
-            sem.enter_recv.at[g, o],
+            vm.enter_out.at[p, part],
+            vm.enter_in.at[o, part],
+            sem.enter_send.at[h, p],
+            sem.enter_recv.at[h, o],
             crew * CREW + p,
         )
 
@@ -648,24 +664,25 @@
                 copy.wait_recv()
 
         others(ctx_arrived, crews)
+        vm.crew_decay[...] = jnp.exp(vm.crew_logs[...])
         zero = jnp.zeros((UNIT, LANES), f32)
         forward, backward = [zero] * GROUPS, [zero] * GROUPS
         for a in range(crews):
             z = crews - 1 - a
             for g in range(GROUPS):
                 forward[g] = (
-                    jnp.exp(vm.crew_logs[a, 1, g : g + 1, :]) * forward[g]
+                    vm.crew_decay[a, 1, g : g + 1, :] * forward[g]
                     + vm.ctx_crews[a, g, :UNIT].astype(f32)
                 )
                 backward[g] = (
-                    jnp.exp(vm.crew_logs[z, 1, g : g + 1, :]) * backward[g]
+                    vm.crew_decay[z, 1, g : g + 1, :] * backward[g]
                     + vm.ctx_crews[z, g, UNIT:].astype(f32)
                 )
 
         def step_states(c, states):
             left = vm.crew_in[c].astype(f32)
             return tuple(
-                jnp.exp(vm.crew_logs[c, 0, g : g + 1, :]) * states[g] + left[g * UNIT : (g + 1) * UNIT]
+                vm.crew_decay[c, 0, g : g + 1, :] * states[g] + left[g * UNIT : (g + 1) * UNIT]
                 for g in range(GROUPS)
             )
 
@@ -683,17 +700,17 @@
         for g in range(GROUPS):
             state = forward[g]
             for p in range(CREW):
-                vm.enter_out[g, p, :UNIT] = state.astype(bf16)
+                vm.enter_out[p, g, :UNIT] = state.astype(bf16)
                 if p < CREW - 1:
-                    state = post_decay(p, g) * state + vm.seg_in[g, p, :UNIT].astype(f32)
+                    state = post_decay(p, g) * state + vm.seg_in[p, g, :UNIT].astype(f32)
             state = backward[g]
             for p in range(CREW - 1, -1, -1):
-                vm.enter_out[g, p, UNIT:] = state.astype(bf16)
+                vm.enter_out[p, g, UNIT:] = state.astype(bf16)
                 if p > 0:
-                    state = post_decay(p, g) * state + vm.seg_in[g, p, UNIT:].astype(f32)
-            mates(lambda p: enter_copy(p, chip, g).start())
-        for g in range(GROUPS):
-            vm.enter_in[g, chip] = vm.enter_out[g, post]
+                    state = post_decay(p, g) * state + vm.seg_in[p, g, UNIT:].astype(f32)
+            if g % half == half - 1:
+                mates(lambda p: enter_copy(p, chip, g // half).start())
+        vm.enter_in[chip] = vm.enter_out[post]
 
     loads["outgate_weight"].wait()
     for n in range(0, vm.outgate_weight.shape[1], COLS):
@@ -704,7 +721,7 @@
         between(g)
     head_mean = jnp.where(iota((GV, GV), 0) // DV == iota((GV, GV), 1) // DV, 1.0 / DV, 0.0).astype(bf16)
 
-    arrivals(gate_spread)
+    arrivals(1, gate_spread)
     for r in range(reducers):
         for t in range(tp_count):
             tile = summed(vm.gate_totals, r, t)
@@ -716,18 +733,17 @@
     for which in range(2):
         for r in range(reducers):
 
-            @pl.when(elsewhere(r))
+            @pl.when(elsewhere(r, which))
             def _():
                 to_reducer(r, crew, core, which).wait_send()
 
-    sent(spread)
-    sent(gate_spread)
+    sent(0, spread)
+    sent(1, gate_spread)
 
     def to_owner_sent(o):
         for copy in early_copies(o, post):
             copy.wait_send()
-        for g in range(GROUPS):
-            seg_copy(o, post, g).wait_send()
+        seg_copy(o, post, every).wait_send()
 
     owners(to_owner_sent)
 
@@ -745,8 +761,8 @@
         v_lanes = slice(g * GV, (g + 1) * GV)
         states = jnp.concatenate(
             [
-                jnp.concatenate([vm.enter_in[g, o, :UNIT] for o in range(OWNERS)], axis=0),
-                jnp.concatenate([vm.enter_in[g, o, UNIT:] for o in range(OWNERS)], axis=0),
+                jnp.concatenate([vm.enter_in[o, g, :UNIT] for o in range(OWNERS)], axis=0),
+                jnp.concatenate([vm.enter_in[o, g, UNIT:] for o in range(OWNERS)], axis=0),
             ],
             axis=1,
         )
@@ -755,16 +771,21 @@
         mean = dot((mixed * mixed).astype(bf16), head_mean)
         vm.gated[:, v_lanes] = (mixed * lax.rsqrt(mean + epsilon) * vm.silu[:, v_lanes]).astype(bf16)
 
-    for half in range(0, GROUPS, 2):
-        for g in range(half, half + 2):
-            owners(lambda o: enter_copy(post, o, g).wait_recv())
-        for g in range(half, half + 2):
-            finish(g)
+    depth = half * GV
+    owners(lambda o: enter_copy(post, o, 0).wait_recv())
+    for g in range(half):
+        finish(g)
+    for n in range(0, width, COLS):
+        at = slice(n, n + COLS)
+        vm.branch_part[:, at] = dot(vm.gated[:, :depth], vm.out_weight[:depth, at])
+    owners(lambda o: enter_copy(post, o, 1).wait_recv())
+    for g in range(half, GROUPS):
+        finish(g)
 
     square = jnp.zeros((rows, LANES), f32)
     for n in range(0, width, COLS):
         at = slice(n, n + COLS)
-        branch = dot(vm.gated[...], vm.out_weight[:, at]).astype(bf16)
+        branch = (vm.branch_part[:, at] + dot(vm.gated[:, depth:], vm.out_weight[depth:, at])).astype(bf16)
         vm.branch[:, at] = branch
         branch = branch.astype(f32)
         branch = branch * branch
@@ -780,8 +801,8 @@
 
     @pl.when(owner)
     def _():
-        for g in range(GROUPS):
-            mates(lambda p: enter_copy(p, chip, g).wait_send())
+        for h in range(2):
+            mates(lambda p: enter_copy(p, chip, h).wait_send())
 
 
 def shards(*operands):
@@ -817,6 +838,7 @@
         gate_totals=pltpu.VMEM((reducers * OWNERS, CORES, share, 1, LANES), f32),
         mods=pltpu.VMEM((SUB, width), f32),
         scaled=pltpu.VMEM((rows, width), f32),
+        down=pltpu.VMEM((width, values["down_weight"].shape[0]), bf16),
         ctx_scaled=pltpu.VMEM((ctx_rows, width), f32),
         normed=pltpu.VMEM((rows, width), bf16),
         ctx_out=pltpu.VMEM((OWNERS, *unit), bf16),
@@ -834,19 +856,23 @@
         before=pltpu.VMEM((rows, keyw), f32),
         closing=pltpu.VMEM((blocks, keyw), f32),
         offset=pltpu.VMEM((blocks + 1, keyw), f32),
-        log_out=pltpu.VMEM((SUB, LANES), f32),
-        logs=pltpu.VMEM((CREW, SUB, LANES), f32),
-        seg_out=pltpu.VMEM((GROUPS, OWNERS, *unit), bf16),
-        seg_in=pltpu.VMEM((GROUPS, CREW, *unit), bf16),
+        log_out=pltpu.VMEM((GROUPS, LANES), f32),
+        logs=pltpu.VMEM((CREW, GROUPS, LANES), f32),
+        decay=pltpu.VMEM((CREW, GROUPS, LANES), f32),
+        crew_decay=pltpu.VMEM((crews, 2, SUB, LANES), f32),
+        seg_out=pltpu.VMEM((OWNERS, GROUPS, *unit), bf16),
+        seg_in=pltpu.VMEM((CREW, GROUPS, *unit), bf16),
         crew_out=pltpu.VMEM((2, GROUPS * UNIT, LANES), bf16),
         crew_in=pltpu.VMEM((crews, GROUPS * UNIT, LANES), bf16),
         crew_log=pltpu.VMEM((2, SUB, LANES), f32),
         crew_logs=pltpu.VMEM((crews, 2, SUB, LANES), f32),
-        enter_out=pltpu.VMEM((GROUPS, CREW, *unit), bf16),
-        enter_in=pltpu.VMEM((GROUPS, OWNERS, *unit), bf16),
+        enter_out=pltpu.VMEM((CREW, GROUPS, *unit), bf16),
+        enter_in=pltpu.VMEM((OWNERS, GROUPS, *unit), bf16),
+        k_block=pltpu.VMEM((GROUPS, rows, 2 * LANES), bf16),
         q_block=pltpu.VMEM((GROUPS, rows, 2 * LANES), bf16),
         q_whole=pltpu.VMEM((GROUPS, rows, 2 * LANES), bf16),
         within=pltpu.VMEM((rows, valw), f32),
+        branch_part=pltpu.VMEM((rows, width), f32),
         branch=pltpu.VMEM((rows, width), bf16),
     )
     for name, value in zip(NAMES, args):
@@ -867,16 +893,16 @@
         ctx_log_recv=dma((CREW,)),
         log_send=dma((OWNERS,)),
         log_recv=dma((CREW,)),
-        seg_send=dma((GROUPS, OWNERS)),
-        seg_recv=dma((GROUPS, CREW)),
+        seg_send=dma((OWNERS,)),
+        seg_recv=dma((CREW,)),
         ctx_crew_send=dma((crews,)),
         ctx_crew_recv=dma((crews,)),
         crew_log_send=dma((crews,)),
         crew_log_recv=dma((crews,)),
         crew_send=dma((crews,)),
         crew_recv=dma((crews,)),
-        enter_send=dma((GROUPS, CREW)),
-        enter_recv=dma((GROUPS, OWNERS)),
+        enter_send=dma((2, CREW)),
+        enter_recv=dma((2, OWNERS)),
     )
     return pl.pallas_call(
         functools.partial(block_kernel, sp_count, tp_count),

time: 33 us -> 32 us (0.970)
  Pallas kernels: 31.9 us -> 30.8 us
    pallas_call x1, Pallas kernels: 31.9 us -> 30.8 us  [shards(): pl.pallas_call(functools.partial(block_kernel, sp_count, tp_count), out_s...]
where the time goes in v4:
time: 32 us; the launch traced here: 31.8 us
  Pallas kernels  30.8 us (96%)
  local copies, waits for them, and re-layouts  0.97 us (3%)
    pallas_call x1, Pallas kernels, shards(): pl.pallas_call(functools.partial(block_kernel, sp_count, tp_count), out_s...  30.8 us
    unnamed x1, local copies, waits for them, and re-layouts  0.97 us

profile of v4, /device:TPU:0, one launch (start us, length us, event | category | flops | bytes accessed | tf_op | source)
XLA Modules:
  0.0 31.8 jit_solution(11964776415605510286)
XLA Ops:
  0.0 30.8 %block.1 = bf16[256,2048]{1,0:T(8,128)(2,1)S(1)} custom-call(bf16[256,2048]{1,0:T(8,128)(2,1)} %refs_0_.1, bf16[64,2048]{1,0:T(8,128)(2,1)} %refs_1_.1, bf16[2048]{0:T(1024)(128)(2,1)} %refs_2_.1, bf16[2048]{0:T(1024)(128)(2,1)} %refs_3_.1, bf16[256,512]{1,0:T(8,128)(2,1)} %refs_4_.1, bf16[256,512]{1,0:T(8,128)(2,1)} %refs_5_.1, bf16[256,512]{1,0:T(8,128)(2,1)} %refs_6_.1, ...), custom_call_target="tpu_custom_call" | custom-call | tf_op jit(solution)/shard_map/block/pallas_call | solution.py:907
  30.8 1.0 %copy.19 = bf16[256,2048]{1,0:T(8,128)(2,1)} copy(bf16[256,2048]{1,0:T(8,128)(2,1)S(1)} %block.1) | data formatting | bytes 2097152

commit v5 on v4

--- a/solution.py
+++ b/solution.py
@@ -222,23 +222,17 @@
     pick = iota((STRIP, row_share), 0) == 0
     raw = jnp.where(pick, vm.cond[0:1, mine], vm.cond[1:2, mine])
     cond = (raw / (1.0 + jnp.exp(-raw))).astype(bf16)
-    for which, name in enumerate(("shift_weight", "scale_weight", "gate_weight")):
-        loads[name].wait()
-        part = dot(cond, getattr(vm, name)[...])
+    loads["shift_weight"].wait()
+    loads["scale_weight"].wait()
+    for which, weight in enumerate((vm.shift_weight, vm.scale_weight)):
+        part = dot(cond, weight[...])
         for c in range(chunks):
             at = slice(c * LANES, (c + 1) * LANES)
-            r, row = c // share, c % share
-            if which == 2:
-                vm.gate_part[r, row] = part[0:1, at]
-            else:
-                vm.part[r, row * 4 + which : row * 4 + which + 1, :] = part[0:1, at]
-                vm.part[r, row * 4 + 2 + which : row * 4 + 3 + which, :] = part[1:2, at]
+            r, row = c // share, c % share * 4 + which
+            vm.part[r, row : row + 1, :] = part[0:1, at]
+            vm.part[r, row + 2 : row + 3, :] = part[1:2, at]
     for name in LATER:
         loads[name].start()
-    @pl.when(reducer)
-    def _():
-        pl.semaphore_wait(barrier, count - 1)
-
     @pl.when(jnp.logical_not(reducer))
     def _():
         pl.semaphore_wait(barrier, reducers)
@@ -265,7 +259,20 @@
             def _():
                 to_reducer(r, crew, core, which).start()
 
+    def early_part(r):
+        return to_reducer(r, crew, 0, 0)
+
+    for r in range(reducers):
+
+        @pl.when(jnp.logical_not(elsewhere(r, 0)))
+        def _():
+            early_part(r).wait_recv()
+
     send_parts(0)
+    loads["gate_weight"].wait()
+    part = dot(cond, vm.gate_weight[...])
+    for c in range(chunks):
+        vm.gate_part[c // share, c % share] = part[0:1, c * LANES : (c + 1) * LANES]
 
     loads["context"].wait()
     xc = vm.context[...].astype(f32)
@@ -311,7 +318,8 @@
                         if c == home and k == home_core[which]:
                             term = mine[r]
                         else:
-                            to_reducer(r, c, k, which).wait_recv()
+                            if which == 1 or c != home or k != 0:
+                                to_reducer(r, c, k, which).wait_recv()
                             term = held[c, k]
                         out = term if out is None else out + term
                     total[k] = out
@@ -341,6 +349,10 @@
                 for step in range(count):
                     if step != home * CREW:
                         copy(me, 0, step).wait_send()
+
+    @pl.when(reducer)
+    def _():
+        pl.semaphore_wait(barrier, count - 1)
 
     reduce_here(0, vm.part, vm.parts, vm.total, vm.totals, spread)
     loads_needed = ("norm_gain", "decay_bias", "post_gain", "up_weight", "key_weight")
@@ -488,6 +500,52 @@
     @pl.when(owner)
     def _():
         vm.seg_in[post] = vm.seg_out[chip]
+
+    def ctx_crew_copies(c, slot):
+        flat = c * CREW + post
+        return (
+            remote(
+                vm.ctx_crews_out,
+                vm.ctx_crews.at[slot],
+                sem.ctx_crew_send.at[c],
+                sem.ctx_crew_recv.at[slot],
+                flat,
+            ),
+            remote(
+                vm.ctx_crews_log,
+                vm.ctx_crews_logs.at[slot],
+                sem.ctx_crew_log_send.at[c],
+                sem.ctx_crew_log_recv.at[slot],
+                flat,
+            ),
+        )
+
+    @pl.when(owner)
+    def _():
+        def ctx_arrived(p):
+            for copy in ctx_copies(0, p):
+                copy.wait_recv()
+
+        mates(ctx_arrived)
+        for g in range(GROUPS):
+            posts = list(range(g, CREW, GROUPS))
+            logs = [vm.ctx_logs[p] for p in posts]
+            tiles = [vm.ctx_in[p].astype(f32) for p in posts]
+            forward, backward, log_sum = tiles[0][:UNIT], tiles[-1][UNIT:], logs[0]
+            for i in range(1, len(posts)):
+                forward = jnp.exp(logs[i]) * forward + tiles[i][:UNIT]
+                backward = jnp.exp(logs[-1 - i]) * backward + tiles[-1 - i][UNIT:]
+                log_sum = log_sum + logs[i]
+            vm.ctx_crews_out[g] = jnp.concatenate([forward, backward], axis=0).astype(bf16)
+            vm.ctx_crews_log[g : g + 1, :] = log_sum
+
+        def ctx_crew_start(i):
+            for copy in ctx_crew_copies(lax.rem(crew + i, crews), crew):
+                copy.start()
+
+        others(ctx_crew_start, crews)
+        vm.ctx_crews[crew] = vm.ctx_crews_out[...]
+        vm.ctx_crews_logs[crew] = vm.ctx_crews_log[...]
 
     head_k1 = iota((TILE, LANES), 1) // DK
     head_v = iota((TILE, GV), 1) // DV
@@ -549,52 +607,24 @@
     project(vm.query_weight, vm.query)
     inside(0)
 
-    def ctx_crew_copies(c, slot):
-        flat = c * CREW + post
-        return (
-            remote(
-                vm.ctx_crews_out,
-                vm.ctx_crews.at[slot],
-                sem.ctx_crew_send.at[c],
-                sem.ctx_crew_recv.at[slot],
-                flat,
-            ),
-            remote(
-                vm.crew_log, vm.crew_logs.at[slot], sem.crew_log_send.at[c], sem.crew_log_recv.at[slot], flat
-            ),
+    def crew_log_copy(c, slot):
+        return remote(
+            vm.crew_log,
+            vm.crew_logs.at[slot],
+            sem.crew_log_send.at[c],
+            sem.crew_log_recv.at[slot],
+            c * CREW + post,
         )
 
     @pl.when(owner)
     def _():
-        def early_in(p):
-            for copy in early_copies(0, p):
-                copy.wait_recv()
-
-        mates(early_in)
+        mates(lambda p: log_copy(0, p).wait_recv())
         vm.decay[...] = jnp.exp(vm.logs[...])
         crew_log = vm.logs[0]
         for p in range(1, CREW):
             crew_log = crew_log + vm.logs[p]
-        vm.crew_log[0, :GROUPS] = crew_log
-        for g in range(GROUPS):
-            posts = list(range(g, CREW, GROUPS))
-            logs = [vm.ctx_logs[p] for p in posts]
-            tiles = [vm.ctx_in[p].astype(f32) for p in posts]
-            forward, backward, log_sum = tiles[0][:UNIT], tiles[-1][UNIT:], logs[0]
-            for i in range(1, len(posts)):
-                forward = jnp.exp(logs[i]) * forward + tiles[i][:UNIT]
-                backward = jnp.exp(logs[-1 - i]) * backward + tiles[-1 - i][UNIT:]
-                log_sum = log_sum + logs[i]
-            vm.ctx_crews_out[g] = jnp.concatenate([forward, backward], axis=0).astype(bf16)
-            vm.crew_log[1, g : g + 1, :] = log_sum
-
-        def ctx_crew_start(i):
-            for copy in ctx_crew_copies(lax.rem(crew + i, crews), crew):
-                copy.start()
-
-        others(ctx_crew_start, crews)
-        vm.ctx_crews[crew] = vm.ctx_crews_out[...]
-        vm.crew_logs[crew] = vm.crew_log[...]
+        vm.crew_log[...] = crew_log
+        others(lambda i: crew_log_copy(lax.rem(crew + i, crews), crew).start(), crews)
 
     inside(1)
 
@@ -660,29 +690,30 @@
     def _():
         def ctx_arrived(i):
             c = lax.rem(crew + i, crews)
-            for copy in ctx_crew_copies(c, c):
+            for copy in (*ctx_crew_copies(c, c), crew_log_copy(c, c)):
                 copy.wait_recv()
 
         others(ctx_arrived, crews)
         vm.crew_decay[...] = jnp.exp(vm.crew_logs[...])
+        vm.ctx_decay[...] = jnp.exp(vm.ctx_crews_logs[...])
         zero = jnp.zeros((UNIT, LANES), f32)
         forward, backward = [zero] * GROUPS, [zero] * GROUPS
         for a in range(crews):
             z = crews - 1 - a
             for g in range(GROUPS):
                 forward[g] = (
-                    vm.crew_decay[a, 1, g : g + 1, :] * forward[g]
+                    vm.ctx_decay[a, g : g + 1, :] * forward[g]
                     + vm.ctx_crews[a, g, :UNIT].astype(f32)
                 )
                 backward[g] = (
-                    vm.crew_decay[z, 1, g : g + 1, :] * backward[g]
+                    vm.ctx_decay[z, g : g + 1, :] * backward[g]
                     + vm.ctx_crews[z, g, UNIT:].astype(f32)
                 )
 
         def step_states(c, states):
             left = vm.crew_in[c].astype(f32)
             return tuple(
-                vm.crew_decay[c, 0, g : g + 1, :] * states[g] + left[g * UNIT : (g + 1) * UNIT]
+                vm.crew_decay[c, g : g + 1, :] * states[g] + left[g * UNIT : (g + 1) * UNIT]
                 for g in range(GROUPS)
             )
 
@@ -751,7 +782,7 @@
     def _():
         def crew_sent(i):
             c = lax.rem(crew + i, crews)
-            for copy in ctx_crew_copies(c, crew):
+            for copy in (*ctx_crew_copies(c, crew), crew_log_copy(c, crew)):
                 copy.wait_send()
             crew_copy(c, crew, 0).wait_send()
 
@@ -859,13 +890,16 @@
         log_out=pltpu.VMEM((GROUPS, LANES), f32),
         logs=pltpu.VMEM((CREW, GROUPS, LANES), f32),
         decay=pltpu.VMEM((CREW, GROUPS, LANES), f32),
-        crew_decay=pltpu.VMEM((crews, 2, SUB, LANES), f32),
+        crew_decay=pltpu.VMEM((crews, GROUPS, LANES), f32),
+        ctx_decay=pltpu.VMEM((crews, GROUPS, LANES), f32),
+        ctx_crews_log=pltpu.VMEM((GROUPS, LANES), f32),
+        ctx_crews_logs=pltpu.VMEM((crews, GROUPS, LANES), f32),
         seg_out=pltpu.VMEM((OWNERS, GROUPS, *unit), bf16),
         seg_in=pltpu.VMEM((CREW, GROUPS, *unit), bf16),
         crew_out=pltpu.VMEM((2, GROUPS * UNIT, LANES), bf16),
         crew_in=pltpu.VMEM((crews, GROUPS * UNIT, LANES), bf16),
-        crew_log=pltpu.VMEM((2, SUB, LANES), f32),
-        crew_logs=pltpu.VMEM((crews, 2, SUB, LANES), f32),
+        crew_log=pltpu.VMEM((GROUPS, LANES), f32),
+        crew_logs=pltpu.VMEM((crews, GROUPS, LANES), f32),
         enter_out=pltpu.VMEM((CREW, GROUPS, *unit), bf16),
         enter_in=pltpu.VMEM((OWNERS, GROUPS, *unit), bf16),
         k_block=pltpu.VMEM((GROUPS, rows, 2 * LANES), bf16),
@@ -897,6 +931,8 @@
         seg_recv=dma((CREW,)),
         ctx_crew_send=dma((crews,)),
         ctx_crew_recv=dma((crews,)),
+        ctx_crew_log_send=dma((crews,)),
+        ctx_crew_log_recv=dma((crews,)),
         crew_log_send=dma((crews,)),
         crew_log_recv=dma((crews,)),
         crew_send=dma((crews,)),

time: 32 us -> 30.6 us (0.956)
  Pallas kernels: 30.8 us -> 29.5 us
    pallas_call x1, Pallas kernels: 30.8 us -> 29.5 us  [shards(): pl.pallas_call(functools.partial(block_kernel, sp_count, tp_count), out_s...]
where the time goes in v5:
time: 30.6 us; the launch traced here: 30.4 us
  Pallas kernels  29.5 us (96%)
  local copies, waits for them, and re-layouts  0.97 us (3%)
    pallas_call x1, Pallas kernels, shards(): pl.pallas_call(functools.partial(block_kernel, sp_count, tp_count), out_s...  29.5 us
    unnamed x1, local copies, waits for them, and re-layouts  0.97 us

profile of v5, /device:TPU:0, one launch (start us, length us, event | category | flops | bytes accessed | tf_op | source)
XLA Modules:
  0.0 30.4 jit_solution(18225421975656642501)
XLA Ops:
  0.0 29.5 %block.1 = bf16[256,2048]{1,0:T(8,128)(2,1)S(1)} custom-call(bf16[256,2048]{1,0:T(8,128)(2,1)} %refs_0_.1, bf16[64,2048]{1,0:T(8,128)(2,1)} %refs_1_.1, bf16[2048]{0:T(1024)(128)(2,1)} %refs_2_.1, bf16[2048]{0:T(1024)(128)(2,1)} %refs_3_.1, bf16[256,512]{1,0:T(8,128)(2,1)} %refs_4_.1, bf16[256,512]{1,0:T(8,128)(2,1)} %refs_5_.1, bf16[256,512]{1,0:T(8,128)(2,1)} %refs_6_.1, ...), custom_call_target="tpu_custom_call" | custom-call | tf_op jit(solution)/shard_map/block/pallas_call | solution.py:943
  29.5 1.0 %copy.19 = bf16[256,2048]{1,0:T(8,128)(2,1)} copy(bf16[256,2048]{1,0:T(8,128)(2,1)S(1)} %block.1) | data formatting | bytes 2097152

commit v6 on v5

--- a/solution.py
+++ b/solution.py
@@ -182,6 +182,16 @@
             else:
                 body(at)
 
+    def landed(ref, semaphore):
+        remote(ref, ref, semaphore, semaphore, me).wait_recv()
+
+    def gone(ref, semaphore):
+        remote(ref, ref, semaphore, semaphore, me).wait_send()
+
+    def by_role(body):
+        pl.when(owner)(functools.partial(body, OWNERS - 1))
+        pl.when(jnp.logical_not(owner))(functools.partial(body, OWNERS))
+
     def owner_of(at):
         return at * CORES + CORES - 1
 
@@ -291,18 +301,12 @@
 
     reduced = reducers * OWNERS
 
-    def spread(flat, slot, step=0):
+    def spread(flat, slot):
+        return remote(vm.total, vm.totals.at[slot], sem.total_send.at[0], sem.total_recv.at[0], flat)
+
+    def gate_spread(flat, slot):
         return remote(
-            vm.total, vm.totals.at[slot], sem.total_send.at[step], sem.total_recv.at[slot], flat
-        )
-
-    def gate_spread(flat, slot, step=0):
-        return remote(
-            vm.gate_total,
-            vm.gate_totals.at[slot],
-            sem.gate_send.at[step],
-            sem.gate_recv.at[slot],
-            flat,
+            vm.gate_total, vm.gate_totals.at[slot], sem.gate_send.at[0], sem.gate_recv.at[0], flat
         )
 
     def reduce_here(which, mine, held, total, totals, copy):
@@ -327,28 +331,27 @@
                 for c in sorted(range(crews), key=lambda c: -abs(c - home)):
 
                     def send(i, carry):
-                        copy(c * CREW + mate(i), slot, c * CREW + i).start()
+                        copy(c * CREW + mate(i), slot).start()
                         return carry
 
                     lax.fori_loop(0 if c != home else 1, CREW, send, 0)
 
-    def arrivals(which, copy):
-        for i in range(reduced):
-            flat = (first_reducer + i // OWNERS) * CREW + i % OWNERS * CORES + home_core[which]
-
-            @pl.when(flat != me)
-            def _():
-                copy(me, i).wait_recv()
-
-    def sent(which, copy):
-        for r in range(reducers):
-            home = first_reducer + r
-
-            @pl.when((core == home_core[which]) & (crew == home))
-            def _():
-                for step in range(count):
-                    if step != home * CREW:
-                        copy(me, 0, step).wait_send()
+    def reduces(which):
+        return (core == home_core[which]) & middle_crew
+
+    def arrivals(which, totals, semaphore):
+        @pl.when(reduces(which))
+        def _():
+            landed(totals.at[pl.ds(0, reduced - 1)], semaphore)
+
+        @pl.when(jnp.logical_not(reduces(which)))
+        def _():
+            landed(totals, semaphore)
+
+    def sent(which, credit, semaphore):
+        @pl.when(reduces(which))
+        def _():
+            gone(credit, semaphore)
 
     @pl.when(reducer)
     def _():
@@ -358,7 +361,7 @@
     loads_needed = ("norm_gain", "decay_bias", "post_gain", "up_weight", "key_weight")
     for name in loads_needed + ("value_weight",):
         loads[name].wait()
-    arrivals(0, spread)
+    arrivals(0, vm.totals, sem.total_recv.at[0])
     def summed(totals, r, t):
         out = None
         for p in range(t, CREW, tp_count):
@@ -396,8 +399,8 @@
     def ctx_copies(o, p):
         flat = crew * CREW + owner_of(o)
         return (
-            remote(vm.ctx_out.at[o], vm.ctx_in.at[p], sem.ctx_send.at[o], sem.ctx_recv.at[p], flat),
-            remote(vm.ctx_log, vm.ctx_logs.at[p], sem.ctx_log_send.at[o], sem.ctx_log_recv.at[p], flat),
+            remote(vm.ctx_out.at[o], vm.ctx_in.at[p], sem.ctx_send.at[0], sem.ctx_recv.at[0], flat),
+            remote(vm.ctx_log, vm.ctx_logs.at[p], sem.ctx_log_send.at[0], sem.ctx_log_recv.at[0], flat),
         )
 
     def ctx_start(o):
@@ -449,7 +452,7 @@
 
     def log_copy(o, p):
         return remote(
-            vm.log_out, vm.logs.at[p], sem.log_send.at[o], sem.log_recv.at[p], crew * CREW + owner_of(o)
+            vm.log_out, vm.logs.at[p], sem.log_send.at[0], sem.log_recv.at[0], crew * CREW + owner_of(o)
         )
 
     def early_copies(o, p):
@@ -462,15 +465,13 @@
         vm.ctx_in[post] = vm.ctx_out[chip]
         vm.ctx_logs[post] = vm.ctx_log[...]
         vm.logs[post] = vm.log_out[...]
-
-    every = pl.ds(0, GROUPS)
 
     def seg_copy(o, p, g):
         return remote(
             vm.seg_out.at[o, g],
             vm.seg_in.at[p, g],
-            sem.seg_send.at[o],
-            sem.seg_recv.at[p],
+            sem.seg_send.at[0],
+            sem.seg_recv.at[0],
             crew * CREW + owner_of(o),
         )
 
@@ -507,26 +508,23 @@
             remote(
                 vm.ctx_crews_out,
                 vm.ctx_crews.at[slot],
-                sem.ctx_crew_send.at[c],
-                sem.ctx_crew_recv.at[slot],
+                sem.ctx_crew_send.at[0],
+                sem.ctx_crew_recv.at[0],
                 flat,
             ),
             remote(
                 vm.ctx_crews_log,
                 vm.ctx_crews_logs.at[slot],
-                sem.ctx_crew_log_send.at[c],
-                sem.ctx_crew_log_recv.at[slot],
+                sem.ctx_crew_log_send.at[0],
+                sem.ctx_crew_log_recv.at[0],
                 flat,
             ),
         )
 
     @pl.when(owner)
     def _():
-        def ctx_arrived(p):
-            for copy in ctx_copies(0, p):
-                copy.wait_recv()
-
-        mates(ctx_arrived)
+        landed(vm.ctx_in.at[pl.ds(0, CREW - 1)], sem.ctx_recv.at[0])
+        landed(vm.ctx_logs.at[pl.ds(0, CREW - 1)], sem.ctx_log_recv.at[0])
         for g in range(GROUPS):
             posts = list(range(g, CREW, GROUPS))
             logs = [vm.ctx_logs[p] for p in posts]
@@ -611,14 +609,14 @@
         return remote(
             vm.crew_log,
             vm.crew_logs.at[slot],
-            sem.crew_log_send.at[c],
-            sem.crew_log_recv.at[slot],
+            sem.crew_log_send.at[0],
+            sem.crew_log_recv.at[0],
             c * CREW + post,
         )
 
     @pl.when(owner)
     def _():
-        mates(lambda p: log_copy(0, p).wait_recv())
+        landed(vm.logs.at[pl.ds(0, CREW - 1)], sem.log_recv.at[0])
         vm.decay[...] = jnp.exp(vm.logs[...])
         crew_log = vm.logs[0]
         for p in range(1, CREW):
@@ -634,8 +632,8 @@
         return remote(
             vm.crew_out.at[side],
             vm.crew_in.at[slot],
-            sem.crew_send.at[c],
-            sem.crew_recv.at[slot],
+            sem.crew_send.at[0],
+            sem.crew_recv.at[0],
             c * CREW + post,
         )
 
@@ -644,7 +642,7 @@
 
     @pl.when(owner)
     def _():
-        mates(lambda p: seg_copy(0, p, every).wait_recv())
+        landed(vm.seg_in.at[pl.ds(0, CREW - 1)], sem.seg_recv.at[0])
         for g in range(GROUPS):
             at = slice(g * UNIT, (g + 1) * UNIT)
             forward = vm.seg_in[0, g, :UNIT].astype(f32)
@@ -681,19 +679,17 @@
         return remote(
             vm.enter_out.at[p, part],
             vm.enter_in.at[o, part],
-            sem.enter_send.at[h, p],
-            sem.enter_recv.at[h, o],
+            sem.enter_send.at[0],
+            sem.enter_recv.at[h],
             crew * CREW + p,
         )
 
     @pl.when(owner)
     def _():
-        def ctx_arrived(i):
-            c = lax.rem(crew + i, crews)
-            for copy in (*ctx_crew_copies(c, c), crew_log_copy(c, c)):
-                copy.wait_recv()
-
-        others(ctx_arrived, crews)
+        away = pl.ds(0, crews - 1)
+        landed(vm.ctx_crews.at[away], sem.ctx_crew_recv.at[0])
+        landed(vm.ctx_crews_logs.at[away], sem.ctx_crew_log_recv.at[0])
+        landed(vm.crew_logs.at[away], sem.crew_log_recv.at[0])
         vm.crew_decay[...] = jnp.exp(vm.crew_logs[...])
         vm.ctx_decay[...] = jnp.exp(vm.ctx_crews_logs[...])
         zero = jnp.zeros((UNIT, LANES), f32)
@@ -717,16 +713,11 @@
                 for g in range(GROUPS)
             )
 
-        def from_before(c, states):
-            crew_copy(c, c, 0).wait_recv()
-            return step_states(c, states)
-
         def from_after(i, states):
-            c = crews - 1 - i
-            crew_copy(c, c, 1).wait_recv()
-            return step_states(c, states)
-
-        forward = lax.fori_loop(0, crew, from_before, tuple(forward))
+            return step_states(crews - 1 - i, states)
+
+        landed(vm.crew_in.at[away], sem.crew_recv.at[0])
+        forward = lax.fori_loop(0, crew, step_states, tuple(forward))
         backward = lax.fori_loop(0, crews - 1 - crew, from_after, tuple(backward))
         for g in range(GROUPS):
             state = forward[g]
@@ -752,7 +743,7 @@
         between(g)
     head_mean = jnp.where(iota((GV, GV), 0) // DV == iota((GV, GV), 1) // DV, 1.0 / DV, 0.0).astype(bf16)
 
-    arrivals(1, gate_spread)
+    arrivals(1, vm.gate_totals, sem.gate_recv.at[0])
     for r in range(reducers):
         for t in range(tp_count):
             tile = summed(vm.gate_totals, r, t)
@@ -768,25 +759,24 @@
             def _():
                 to_reducer(r, crew, core, which).wait_send()
 
-    sent(0, spread)
-    sent(1, gate_spread)
-
-    def to_owner_sent(o):
-        for copy in early_copies(o, post):
-            copy.wait_send()
-        seg_copy(o, post, every).wait_send()
-
-    owners(to_owner_sent)
+    sent(0, vm.credit, sem.total_send.at[0])
+    sent(1, vm.gate_credit, sem.gate_send.at[0])
+
+    def to_owners_sent(n):
+        gone(vm.ctx_out.at[pl.ds(0, n)], sem.ctx_send.at[0])
+        gone(vm.ctx_logs.at[pl.ds(0, n)], sem.ctx_log_send.at[0])
+        gone(vm.logs.at[pl.ds(0, n)], sem.log_send.at[0])
+        gone(vm.seg_out.at[pl.ds(0, n)], sem.seg_send.at[0])
+
+    by_role(to_owners_sent)
 
     @pl.when(owner)
     def _():
-        def crew_sent(i):
-            c = lax.rem(crew + i, crews)
-            for copy in (*ctx_crew_copies(c, crew), crew_log_copy(c, crew)):
-                copy.wait_send()
-            crew_copy(c, crew, 0).wait_send()
-
-        others(crew_sent, crews)
+        away = pl.ds(0, crews - 1)
+        gone(vm.ctx_crews.at[away], sem.ctx_crew_send.at[0])
+        gone(vm.ctx_crews_logs.at[away], sem.ctx_crew_log_send.at[0])
+        gone(vm.crew_logs.at[away], sem.crew_log_send.at[0])
+        gone(vm.crew_in.at[away], sem.crew_send.at[0])
 
     def finish(g):
         v_lanes = slice(g * GV, (g + 1) * GV)
@@ -802,14 +792,18 @@
         mean = dot((mixed * mixed).astype(bf16), head_mean)
         vm.gated[:, v_lanes] = (mixed * lax.rsqrt(mean + epsilon) * vm.silu[:, v_lanes]).astype(bf16)
 
+    def entered(h):
+        part = pl.ds(h * half, half)
+        by_role(lambda n: landed(vm.enter_in.at[pl.ds(0, n), part], sem.enter_recv.at[h]))
+
     depth = half * GV
-    owners(lambda o: enter_copy(post, o, 0).wait_recv())
+    entered(0)
     for g in range(half):
         finish(g)
     for n in range(0, width, COLS):
         at = slice(n, n + COLS)
         vm.branch_part[:, at] = dot(vm.gated[:, :depth], vm.out_weight[:depth, at])
-    owners(lambda o: enter_copy(post, o, 1).wait_recv())
+    entered(1)
     for g in range(half, GROUPS):
         finish(g)
 
@@ -832,8 +826,7 @@
 
     @pl.when(owner)
     def _():
-        for h in range(2):
-            mates(lambda p: enter_copy(p, chip, h).wait_send())
+        gone(vm.enter_out.at[pl.ds(0, CREW - 1)], sem.enter_send.at[0])
 
 
 def shards(*operands):
@@ -858,6 +851,8 @@
     unit = (2 * UNIT, LANES)
     buffers = dict(
         context=pltpu.VMEM((ctx_rows, width), bf16),
+        credit=pltpu.VMEM((count - 1, CORES, part_rows, LANES), f32),
+        gate_credit=pltpu.VMEM((count - 1, CORES, share, 1, LANES), f32),
         cond=pltpu.VMEM((SUB, width), f32),
         part=pltpu.VMEM((reducers, part_rows, LANES), f32),
         parts=pltpu.VMEM((crews, CORES, part_rows, LANES), f32),
@@ -917,28 +912,28 @@
         load=dma((len(NAMES),)),
         part_send=dma((2, reducers)),
         part_recv=dma((2, crews, CORES)),
-        total_send=dma((count,)),
-        total_recv=dma((reducers * OWNERS,)),
-        gate_send=dma((count,)),
-        gate_recv=dma((reducers * OWNERS,)),
-        ctx_send=dma((OWNERS,)),
-        ctx_recv=dma((CREW,)),
-        ctx_log_send=dma((OWNERS,)),
-        ctx_log_recv=dma((CREW,)),
-        log_send=dma((OWNERS,)),
-        log_recv=dma((CREW,)),
-        seg_send=dma((OWNERS,)),
-        seg_recv=dma((CREW,)),
-        ctx_crew_send=dma((crews,)),
-        ctx_crew_recv=dma((crews,)),
-        ctx_crew_log_send=dma((crews,)),
-        ctx_crew_log_recv=dma((crews,)),
-        crew_log_send=dma((crews,)),
-        crew_log_recv=dma((crews,)),
-        crew_send=dma((crews,)),
-        crew_recv=dma((crews,)),
-        enter_send=dma((2, CREW)),
-        enter_recv=dma((2, OWNERS)),
+        total_send=dma((1,)),
+        total_recv=dma((1,)),
+        gate_send=dma((1,)),
+        gate_recv=dma((1,)),
+        ctx_send=dma((1,)),
+        ctx_recv=dma((1,)),
+        ctx_log_send=dma((1,)),
+        ctx_log_recv=dma((1,)),
+        log_send=dma((1,)),
+        log_recv=dma((1,)),
+        seg_send=dma((1,)),
+        seg_recv=dma((1,)),
+        ctx_crew_send=dma((1,)),
+        ctx_crew_recv=dma((1,)),
+        ctx_crew_log_send=dma((1,)),
+        ctx_crew_log_recv=dma((1,)),
+        crew_log_send=dma((1,)),
+        crew_log_recv=dma((1,)),
+        crew_send=dma((1,)),
+        crew_recv=dma((1,)),
+        enter_send=dma((1,)),
+        enter_recv=dma((2,)),
     )
     return pl.pallas_call(
         functools.partial(block_kernel, sp_count, tp_count),

time: 30.6 us -> 29.1 us (0.951)
  Pallas kernels: 29.5 us -> 28 us
    pallas_call x1, Pallas kernels: 29.5 us -> 28 us  [shards(): pl.pallas_call(functools.partial(block_kernel, sp_count, tp_count), out_s...]
where the time goes in v6:
time: 29.1 us; the launch traced here: 29 us
  Pallas kernels  28 us (96%)
  local copies, waits for them, and re-layouts  0.97 us (3%)
    pallas_call x1, Pallas kernels, shards(): pl.pallas_call(functools.partial(block_kernel, sp_count, tp_count), out_s...  28 us
    unnamed x1, local copies, waits for them, and re-layouts  0.97 us

profile of v6, /device:TPU:0, one launch (start us, length us, event | category | flops | bytes accessed | tf_op | source)
XLA Modules:
  0.0 29.0 jit_solution(12611340490044941414)
XLA Ops:
  0.0 28.0 %block.1 = bf16[256,2048]{1,0:T(8,128)(2,1)S(1)} custom-call(bf16[256,2048]{1,0:T(8,128)(2,1)} %refs_0_.1, bf16[64,2048]{1,0:T(8,128)(2,1)} %refs_1_.1, bf16[2048]{0:T(1024)(128)(2,1)} %refs_2_.1, bf16[2048]{0:T(1024)(128)(2,1)} %refs_3_.1, bf16[256,512]{1,0:T(8,128)(2,1)} %refs_4_.1, bf16[256,512]{1,0:T(8,128)(2,1)} %refs_5_.1, bf16[256,512]{1,0:T(8,128)(2,1)} %refs_6_.1, ...), custom_call_target="tpu_custom_call" | custom-call | tf_op jit(solution)/shard_map/block/pallas_call | solution.py:938
  28.0 1.0 %copy.19 = bf16[256,2048]{1,0:T(8,128)(2,1)} copy(bf16[256,2048]{1,0:T(8,128)(2,1)S(1)} %block.1) | data formatting | bytes 2097152

commit v7 on v6

--- a/solution.py
+++ b/solution.py
@@ -241,8 +241,11 @@
             r, row = c // share, c % share * 4 + which
             vm.part[r, row : row + 1, :] = part[0:1, at]
             vm.part[r, row + 2 : row + 3, :] = part[1:2, at]
-    for name in LATER:
-        loads[name].start()
+    def load_later():
+        for name in LATER:
+            loads[name].start()
+
+    pl.when(reducer)(load_later)
     @pl.when(jnp.logical_not(reducer))
     def _():
         pl.semaphore_wait(barrier, reducers)
@@ -255,7 +258,7 @@
             part.at[r],
             parts.at[c, k],
             sem.part_send.at[which, r],
-            sem.part_recv.at[which, c, k],
+            sem.gate_part_recv.at[0] if which == 1 else sem.part_recv.at[c, k],
             (first_reducer + r) * CREW + chip * CORES + home_core[which],
         )
 
@@ -279,6 +282,7 @@
             early_part(r).wait_recv()
 
     send_parts(0)
+    pl.when(jnp.logical_not(reducer))(load_later)
     loads["gate_weight"].wait()
     part = dot(cond, vm.gate_weight[...])
     for c in range(chunks):
@@ -316,13 +320,15 @@
             @pl.when((core == home_core[which]) & (crew == home))
             def _():
                 slot = r * OWNERS + chip
+                if which == 1:
+                    landed(vm.gate_part_credit, sem.gate_part_recv.at[0])
                 for k in range(CORES):
                     out = None
                     for c in range(crews):
                         if c == home and k == home_core[which]:
                             term = mine[r]
                         else:
-                            if which == 1 or c != home or k != 0:
+                            if which == 0 and (c != home or k != 0):
                                 to_reducer(r, c, k, which).wait_recv()
                             term = held[c, k]
                         out = term if out is None else out + term
@@ -853,6 +859,7 @@
         context=pltpu.VMEM((ctx_rows, width), bf16),
         credit=pltpu.VMEM((count - 1, CORES, part_rows, LANES), f32),
         gate_credit=pltpu.VMEM((count - 1, CORES, share, 1, LANES), f32),
+        gate_part_credit=pltpu.VMEM((crews * CORES - 1, share, 1, LANES), f32),
         cond=pltpu.VMEM((SUB, width), f32),
         part=pltpu.VMEM((reducers, part_rows, LANES), f32),
         parts=pltpu.VMEM((crews, CORES, part_rows, LANES), f32),
@@ -911,7 +918,8 @@
     semaphores = dict(
         load=dma((len(NAMES),)),
         part_send=dma((2, reducers)),
-        part_recv=dma((2, crews, CORES)),
+        part_recv=dma((crews, CORES)),
+        gate_part_recv=dma((1,)),
         total_send=dma((1,)),
         total_recv=dma((1,)),
         gate_send=dma((1,)),

time: 29.1 us -> 29.1 us (level)
  no operation moved by 1% of the time
where the time goes in v7:
time: 29.1 us; the launch traced here: 28.9 us
  Pallas kernels  27.9 us (96%)
  local copies, waits for them, and re-layouts  0.97 us (3%)
    pallas_call x1, Pallas kernels, shards(): pl.pallas_call(functools.partial(block_kernel, sp_count, tp_count), out_s...  27.9 us
    unnamed x1, local copies, waits for them, and re-layouts  0.97 us

profile of v7, /device:TPU:0, one launch (start us, length us, event | category | flops | bytes accessed | tf_op | source)
XLA Modules:
  0.0 28.9 jit_solution(6542983981730799527)
XLA Ops:
  0.0 27.9 %block.1 = bf16[256,2048]{1,0:T(8,128)(2,1)S(1)} custom-call(bf16[256,2048]{1,0:T(8,128)(2,1)} %refs_0_.1, bf16[64,2048]{1,0:T(8,128)(2,1)} %refs_1_.1, bf16[2048]{0:T(1024)(128)(2,1)} %refs_2_.1, bf16[2048]{0:T(1024)(128)(2,1)} %refs_3_.1, bf16[256,512]{1,0:T(8,128)(2,1)} %refs_4_.1, bf16[256,512]{1,0:T(8,128)(2,1)} %refs_5_.1, bf16[256,512]{1,0:T(8,128)(2,1)} %refs_6_.1, ...), custom_call_target="tpu_custom_call" | custom-call | tf_op jit(solution)/shard_map/block/pallas_call | solution.py:946
  27.9 1.0 %copy.19 = bf16[256,2048]{1,0:T(8,128)(2,1)} copy(bf16[256,2048]{1,0:T(8,128)(2,1)S(1)} %block.1) | data formatting | bytes 2097152
